TPU v7x, 256 devices: a whole 4x4x8 slice. The times are simulated.
256 devices in a mesh: sp: 32 (over z, x), fs: 4 (over y), tp: 2 (over core).
Axes of the slice: x: 4, y: 4, z: 8, core: 2. Of those that a mesh axis runs over, the one named last changes fastest.
Arguments:
- inputs: bfloat16 [4, 4096, 2048], P('fs', 'sp'), may hold values from -6 to 6
- input_norm_gain: bfloat16 [2048], replicated, may hold values from 0.099609375 to 1.8984375
- receptance_matrix: bfloat16 [2048, 1024], P('fs', 'tp'), may hold values from -0.125 to 0.125
- key_matrix: bfloat16 [2048, 1024], P('fs', 'tp'), may hold values from -0.125 to 0.125
- value_matrix: bfloat16 [2048, 1024], P('fs', 'tp'), may hold values from -0.125 to 0.125
- pooling_input_weight: bfloat16 [2048, 1024], P('fs', 'tp'), may hold values from -0.125 to 0.125
- decay_lower_matrix: bfloat16 [2048, 128], replicated, may hold values from -0.125 to 0.125
- decay_raise_matrix: bfloat16 [2, 64, 1024], P(None, None, 'tp'), may hold values from -1 to 1
- decay_offset_bias: float32 [2, 1024], P(None, 'tp'), may hold values from -13 to -3
- removal_lower_matrix: bfloat16 [2048, 128], replicated, may hold values from -0.125 to 0.125
- removal_raise_matrix: bfloat16 [2, 64, 1024], P(None, None, 'tp'), may hold values from -1 to 1
- removal_rate_bias: float32 [2, 1024], P(None, 'tp'), may hold values from -9 to 1.5
- tempo_scale: float32 [4, 2, 16, 4096], P('fs', None, 'tp', 'sp'), may hold values from 0.3 to 3.2, as said below
- sudden_decay_extra: float32 [4, 2, 16, 4096], P('fs', None, 'tp', 'sp'), may hold values from -2.8 to 0
- head_norm_gain: bfloat16 [1024], P('tp'), may hold values from 0.099609375 to 1.8984375
- group_mixing_weight: bfloat16 [4, 256, 256], P('tp'), may hold values from -0.375 to 0.375
- attention_output_matrix: bfloat16 [2048, 1024], P('fs', 'tp'), may hold values from -0.125 to 0.125
- pooling_output_matrix: bfloat16 [2048, 1024], P('fs', 'tp'), may hold values from -0.125 to 0.125
Outputs:
- mixed_out: bfloat16 [4, 4096, 2048], P('fs', ('sp', 'tp'))
Inputs may be any that keep to these rules, and one draw needn't show every extreme that they name: `tempo_scale`: positive.
All inputs are finite; a program needn't handle non-finite values.
Results may differ from a plain program's by a relative error of at most 0.017.
Values may be sent and summed in bfloat16 or wider, within the bound.
No kernel may reach another device: no remote copies, remote signals or barrier semaphores. Data moves between devices by JAX's collectives and lax.ppermute only.
A program may use at most 128 MiB of HBM per device.

v0:
```python
import jax
import jax.numpy as jnp
from jax import lax
from jax.sharding import Mesh
from jax.sharding import PartitionSpec as P

HEAD = 64
DECAY_RANK = 64
RATE_RANK = 64
POOL_GROUPS = 4
GROUP_WIDTH = 256
SP = ("sp_0", "sp_1")
SP_TP = ("sp_0", "sp_1", "tp")


norm_eps = 1e-06
head_eps = 0.00064
unit_eps = 1e-06
span_len = 32
highest = lax.Precision.HIGHEST


def filled_with(shard, identity):
    return jax.tree.map(
        lambda a, e: jnp.broadcast_to(jnp.asarray(e, a.dtype), a.shape), shard, identity
    )


def prefix_by_axis(shard, axes, combine, identity, reverse):
    before = start = filled_with(shard, identity)
    total = shard
    for axis in reversed(axes):
        peers, here = (lax.axis_size(axis), lax.axis_index(axis))
        pieces = jax.tree.map(
            lambda part, kind: lax.all_gather(part.astype(kind), axis),
            total,
            (jnp.bfloat16, jnp.bfloat16),
        )
        inside, total = (start, start)
        for k in reversed(range(peers)) if reverse else range(peers):
            passed = k > here if reverse else k < here
            total = combine(
                total, jax.tree.map(lambda part, own: part[k].astype(own.dtype), pieces, shard)
            )
            inside = jax.tree.map(lambda new, old: jnp.where(passed, new, old), total, inside)
        before = combine(inside, before)
    return before


def with_halo(cells, sides, width):
    for axis, dim in sides:
        count = lax.axis_size(axis)
        ends = count - 1
        head = lax.slice_in_dim(cells, 0, width, axis=dim)
        tail = lax.slice_in_dim(cells, cells.shape[dim] - width, cells.shape[dim], axis=dim)
        cells = jnp.concatenate(
            [
                lax.ppermute(tail, axis, [(i, (i + 1) % count) for i in range(ends)]),
                cells,
                lax.ppermute(head, axis, [((i + 1) % count, i) for i in range(ends)]),
            ],
            axis=dim,
        )
    return cells


def contract(form, left, right):
    return jnp.einsum(form, left, right, precision=highest)


def matmul(left, right):
    return contract("...ij,...jk->...ik", left, right)


def project(left, weight):
    return jnp.dot(left, weight, preferred_element_type=jnp.float32).astype(jnp.bfloat16)


def against(row_block, weight):
    return lax.dot_general(
        row_block, weight, (((1,), (1,)), ((), ())), preferred_element_type=jnp.float32
    )


def chain_combine(earlier, later):
    return (matmul(earlier[0], later[0]), matmul(earlier[1], later[0]) + later[1])


def unit_inverse(lower):
    result = jnp.eye(lower.shape[-1], dtype=jnp.float32) - lower
    power = lower
    for level in range(4):
        power = matmul(power, power)
        result = result + matmul(result, power)
    return result


def span_terms(logarithm_decay, unit, removal, written, value, recept):
    inner = jnp.cumsum(logarithm_decay, axis=-2)
    last = inner[..., -1:, :]
    ahead = unit * jnp.exp(inner - logarithm_decay)
    shrink = jnp.exp(-inner)
    remove_scaled = removal * shrink
    write_scaled = written * shrink
    query = recept * jnp.exp(inner)
    spots = jnp.arange(span_len)
    strict = spots[:, None] > spots[None, :]
    within = spots[:, None] >= spots[None, :]
    link_remove = jnp.where(strict, contract("...tk,...sk->...ts", ahead, remove_scaled), 0.0)
    link_write = jnp.where(strict, contract("...tk,...sk->...ts", ahead, write_scaled), 0.0)
    read_remove = jnp.where(within, contract("...tk,...sk->...ts", query, remove_scaled), 0.0)
    read_write = jnp.where(within, contract("...tk,...sk->...ts", query, write_scaled), 0.0)
    inverse = unit_inverse(link_remove)
    pull_map = -matmul(inverse, ahead)
    pull_base = -matmul(inverse, matmul(link_write, value))
    tail = jnp.exp(last - inner)
    remove_tail = removal * tail
    write_tail = written * tail
    transfer = jnp.eye(unit.shape[-1], dtype=jnp.float32) * jnp.exp(last) + contract(
        "...sk,...sj->...kj", pull_map, remove_tail
    )
    carried = contract("...sv,...sk->...vk", pull_base, remove_tail) + contract(
        "...sv,...sk->...vk", value, write_tail
    )
    query_eff = query + matmul(read_remove, pull_map)
    local_read = matmul(read_remove, pull_base) + matmul(read_write, value)
    return (query_eff, local_read, transfer, carried)


def shards(
    inputs,
    input_norm_gain,
    receptance_matrix,
    key_matrix,
    value_matrix,
    pooling_input_weight,
    decay_lower_matrix,
    decay_raise_matrix,
    decay_offset_bias,
    removal_lower_matrix,
    removal_raise_matrix,
    removal_rate_bias,
    tempo_scale,
    sudden_decay_extra,
    head_norm_gain,
    group_mixing_weight,
    attention_output_matrix,
    pooling_output_matrix,
):
    recept_full, key_full, value_full, pool_full, attn_full, pool_back = (
        lax.all_gather(receptance_matrix, "fs", axis=0, tiled=True),
        lax.all_gather(key_matrix, "fs", axis=0, tiled=True),
        lax.all_gather(value_matrix, "fs", axis=0, tiled=True),
        lax.all_gather(pooling_input_weight, "fs", axis=0, tiled=True),
        lax.all_gather(attention_output_matrix, "fs", axis=0, tiled=True),
        lax.all_gather(pooling_output_matrix, "fs", axis=0, tiled=True),
    )
    row_block = inputs[0].astype(jnp.float32)
    normed = (
        row_block
        * lax.rsqrt(jnp.mean(row_block * row_block, axis=-1, keepdims=True) + norm_eps)
        * input_norm_gain.astype(jnp.float32)
    ).astype(jnp.bfloat16)
    tokens = normed.shape[0]
    heads = recept_full.shape[1] // HEAD
    blocks = tokens // span_len
    receptance = project(normed, recept_full).astype(jnp.float32).reshape(tokens, heads, HEAD)
    key_rows = project(normed, key_full).astype(jnp.float32).reshape(tokens, heads, HEAD)
    val_rows = project(normed, value_full).astype(jnp.float32).reshape(tokens, heads, HEAD)
    pool_in = project(normed, pool_full)
    decay_act = jnp.tanh(project(normed, decay_lower_matrix).astype(jnp.float32)).astype(
        jnp.bfloat16
    )
    rate_latent = project(normed, removal_lower_matrix)
    unit_keys = key_rows * lax.rsqrt(
        jnp.sum(key_rows * key_rows, axis=-1, keepdims=True) + unit_eps
    )
    decays = []
    removals = []
    writes = []
    for travel_direction in range(2):
        part = decay_act[:, travel_direction * DECAY_RANK : (travel_direction + 1) * DECAY_RANK]
        decay_pre = decay_offset_bias[travel_direction] + jnp.dot(
            part, decay_raise_matrix[travel_direction], preferred_element_type=jnp.float32
        )
        decay_velocity = jnp.exp(-jax.nn.softplus(-decay_pre) - 0.5).reshape(tokens, heads, HEAD)
        decays.append(
            -decay_velocity * tempo_scale[0, travel_direction].T[:, :, None]
            + sudden_decay_extra[0, travel_direction].T[:, :, None]
        )
        latent = rate_latent[:, travel_direction * RATE_RANK : (travel_direction + 1) * RATE_RANK]
        rate = jax.nn.sigmoid(
            removal_rate_bias[travel_direction]
            + jnp.dot(
                latent, removal_raise_matrix[travel_direction], preferred_element_type=jnp.float32
            )
        )
        rate = rate.reshape(tokens, heads, HEAD)
        removals.append(unit_keys * rate)
        writes.append(key_rows * rate)

    def both_ways(forward, backward):
        stacked = jnp.stack([forward, jnp.flip(backward, axis=0)], axis=0)
        return stacked.reshape(2, blocks, span_len, heads, HEAD).transpose(0, 3, 1, 2, 4)

    query_eff, local_read, transfer, carried = span_terms(
        both_ways(decays[0], decays[1]),
        both_ways(unit_keys, unit_keys),
        both_ways(removals[0], removals[1]),
        both_ways(writes[0], writes[1]),
        both_ways(val_rows, val_rows),
        both_ways(receptance, receptance),
    )
    prefix_map, prefix_sum = lax.associative_scan(chain_combine, (transfer, carried), axis=2)
    total_map = prefix_map[:, :, -1]
    total_sum = prefix_sum[:, :, -1]
    identity_map = jnp.broadcast_to(jnp.eye(HEAD, dtype=jnp.float32), total_map.shape[1:])
    empty = jnp.zeros(total_map.shape[1:], jnp.float32)
    ahead_in = prefix_by_axis(
        (total_map[0], total_sum[0]), SP, chain_combine, (identity_map, empty), False
    )
    behind_in = prefix_by_axis(
        (total_map[1], total_sum[1]), SP, chain_combine, (identity_map, empty), True
    )
    incoming = jnp.stack([ahead_in[1], behind_in[1]], axis=0)
    ending = matmul(incoming[:, :, None], prefix_map) + prefix_sum
    starting = jnp.concatenate([incoming[:, :, None], ending[:, :, :-1]], axis=2)
    reads = contract("...tk,...vk->...tv", query_eff, starting) + local_read
    reads = reads.transpose(0, 2, 3, 1, 4).reshape(2, tokens, heads, HEAD)
    readout = reads[0] + jnp.flip(reads[1], axis=0)
    centred = readout - jnp.mean(readout, axis=-1, keepdims=True)
    spread = jnp.mean(centred * centred, axis=-1, keepdims=True)
    attn_out = (centred * lax.rsqrt(spread + head_eps)).reshape(
        tokens, heads * HEAD
    ) * head_norm_gain.astype(jnp.float32)
    attn_out = attn_out.astype(jnp.bfloat16)
    reach = 2 ** (POOL_GROUPS - 1)
    rimmed = with_halo(pool_in, ((SP, 0),), reach).astype(jnp.float32)
    position = lax.axis_index(SP) * tokens + jnp.arange(tokens)
    length = tokens * lax.axis_size(SP)
    running = rimmed
    window_sums = []
    window_counts = []
    for level in range(POOL_GROUPS):
        shift = 2**level
        running = running[:-shift] + running[shift:]
        window_sums.append(running[reach - shift : reach - shift + tokens])
        upper = jnp.minimum(position + shift, length)
        lower = jnp.maximum(position - shift, 0)
        window_counts.append((upper - lower).astype(jnp.float32))
    window_sums = jnp.stack(window_sums, axis=0)
    window_counts = jnp.stack(window_counts, axis=0)
    pool_vals = pool_in.astype(jnp.float32)
    groups_here = pool_in.shape[1] // GROUP_WIDTH
    diffs = []
    for member in range(groups_here):
        group = lax.axis_index("tp") * groups_here + member
        chosen = lax.dynamic_index_in_dim(
            window_sums[:, :, member * GROUP_WIDTH : (member + 1) * GROUP_WIDTH],
            group,
            0,
            keepdims=False,
        )
        count = lax.dynamic_index_in_dim(window_counts, group, 0, keepdims=False)
        diffs.append(
            chosen / count[:, None]
            - pool_vals[:, member * GROUP_WIDTH : (member + 1) * GROUP_WIDTH]
        )
    pool_diff = jnp.concatenate(diffs, axis=1).astype(jnp.bfloat16)
    mixed = [
        jnp.dot(
            pool_diff[:, member * GROUP_WIDTH : (member + 1) * GROUP_WIDTH],
            group_mixing_weight[member],
            preferred_element_type=jnp.float32,
        )
        for member in range(groups_here)
    ]
    pool_out = jnp.concatenate(mixed, axis=1).astype(jnp.bfloat16)
    attn_half, pool_half = (
        lax.all_to_all(attn_out, "tp", split_axis=0, concat_axis=1, tiled=True),
        lax.all_to_all(pool_out, "tp", split_axis=0, concat_axis=1, tiled=True),
    )
    attn_whole, pool_whole = (
        lax.all_gather(attn_full, "tp", axis=1, tiled=True),
        lax.all_gather(pool_back, "tp", axis=1, tiled=True),
    )
    result = against(attn_half, attn_whole) + against(pool_half, pool_whole)
    return result.astype(jnp.bfloat16)[None]


def solution(mesh):
    split = Mesh(
        mesh.devices.reshape(8, 4, mesh.shape["fs"], mesh.shape["tp"]), ("sp_0", "sp_1", "fs", "tp")
    )
    in_specs = (
        P("fs", SP, None),
        P(),
        P("fs", "tp"),
        P("fs", "tp"),
        P("fs", "tp"),
        P("fs", "tp"),
        P(),
        P(None, None, "tp"),
        P(None, "tp"),
        P(),
        P(None, None, "tp"),
        P(None, "tp"),
        P("fs", None, "tp", SP),
        P("fs", None, "tp", SP),
        P("tp"),
        P("tp", None, None),
        P("fs", "tp"),
        P("fs", "tp"),
    )
    out_specs = P("fs", SP_TP, None)
    return jax.shard_map(
        shards, mesh=split, in_specs=in_specs, out_specs=out_specs, check_vma=False
    )
```

profile of v0, /device:TPU:7, one launch (start us, length us, event | category | flops | bytes accessed | tf_op | source)
XLA Modules:
  0.0 447.5 jit_solution(15655499817770157762)
XLA Ops:
  18.1 27.2 %all-gather.19.cloned.1.call-done = bf16[2048,512]{1,0:T(8,128)(2,1)} async-done(((bf16[512,512]{1,0:T(8,128)(2,1)}), bf16[2048,512]{1,0:T(8,128)(2,1)}) %all-gather.19.cloned.1.call-update) | async-done | bytes 2097168 | tf_op jit(solution)/shard_map/all_gather | solution.py:152
  45.3 2.1 fusion.29
  47.6 32.9 %all-gather.21.cloned.1.call-done = bf16[2048,512]{1,0:T(8,128)(2,1)} async-done(((bf16[512,512]{1,0:T(8,128)(2,1)}), bf16[2048,512]{1,0:T(8,128)(2,1)}) %all-gather.21.cloned.1.call-update) | async-done | bytes 2097168 | tf_op jit(solution)/shard_map/all_gather | solution.py:153
  80.5 2.1 fusion.28
  90.6 3.0 fusion.55
  93.6 3.0 convolution_select_fusion.2
  102.9 2.2 fusion.218
  105.0 2.2 convolution_add_fusion.3
  107.2 4.0 convolution_select_fusion.1
  114.5 3.2 convolution_add_fusion.2
  117.8 1.8 convolution_negate_fusion.1
  121.9 4.2 fusion.46
  126.2 5.0 %multiply_add_fusion = f32[2,8,4,64,64]{4,3,2,1,0:T(8,128)S(1)} fusion(f32[2,8,4,32,64]{4,3,2,1,0:T(8,128)S(1)} %convolution_negate_fusion.1, f32[2,8,4,64]{3,2,1,0:T(4,128)S(1)} %copy-done.59, f32[64,64]{1,0:T(8,128)S(1)} %fusion.167, f32[2,8,4,32,64]{4,1,2,3,0:T(8,128)} %copy-done.15), kind=kOutput, calls=%fused_computation.8 | convolution fusion | flops 101187584 | bytes 2129920 | tf_op jit(solution)/shard_map/...sk,...sj->...kj/dot_general | solution.py:68
  133.2 4.0 convolution_add_fusion.1
  140.3 1.5 fusion.13
  142.5 1.5 convolution_bitcast_fusion.3
  145.5 11.3 %pad.33 = f32[2,8,4,64,64]{4,3,2,1,0:T(8,128)} pad(f32[2,8,2,64,64]{4,3,2,1,0:T(8,128)S(1)} %copy-done.30, f32[]{:T(128)} %constant.27.clone.1), padding=0_0_0x0_0_0x1_0_1x0_0_0x0_0_0 | pad | bytes 1572868 | tf_op jit(solution)/shard_map/pad | solution.py:214
  157.0 11.2 %pad.32 = f32[2,8,4,64,64]{4,3,2,1,0:T(8,128)} pad(f32[2,8,2,64,64]{4,3,2,1,0:T(8,128)S(1)} %pad_maximum_fusion.1, f32[]{:T(128)} %constant.27.clone.1), padding=0_0_0x0_0_0x0_1_1x0_0_0x0_0_0 | pad | bytes 1572868 | tf_op jit(solution)/shard_map/pad | solution.py:214
  168.2 11.2 %pad.28 = f32[2,8,4,64,64]{4,3,2,1,0:T(8,128)} pad(f32[2,8,2,64,64]{4,3,2,1,0:T(8,128)S(1)} %pad_maximum_fusion, f32[]{:T(128)} %constant.27.clone.1), padding=0_0_0x0_0_0x0_1_1x0_0_0x0_0_0 | pad | bytes 1572868 | tf_op jit(solution)/shard_map/pad | solution.py:214
  179.5 16.7 %pad.29 = f32[2,8,4,64,64]{4,3,2,1,0:T(8,128)} pad(f32[2,8,2,64,64]{4,3,2,1,0:T(8,128)} %pad_add_fusion.1, f32[]{:T(128)} %constant.27.clone.1), padding=0_0_0x0_0_0x1_0_1x0_0_0x0_0_0 | pad | bytes 1572868 | tf_op jit(solution)/shard_map/pad | solution.py:214
  196.2 2.2 add_convert_fusion
  198.4 10.7 %all-gather.6 = bf16[4,8,1,64,64]{4,3,2,1,0:T(8,128)(2,1)S(1)} all-gather(bf16[1,8,1,64,64]{4,3,2,1,0:T(8,128)(2,1)S(1)} %get-tuple-element.24), channel_id=8, replica_groups=mesh['sp_0'=8,'sp_1'=4,'fs'=4,'tp'=2] {'sp_1'}, dimensions={0}, use_global_device_ids=true | all-gather | bytes 327680 | tf_op jit(solution)/shard_map/all_gather | solution.py:35
  209.1 1.9 fusion.200
  211.0 11.9 %all-gather.4 = bf16[4,8,1,64,64]{4,3,2,1,0:T(8,128)(2,1)S(1)} all-gather(bf16[1,8,1,64,64]{4,3,2,1,0:T(8,128)(2,1)S(1)} %get-tuple-element.22), channel_id=6, replica_groups=mesh['sp_0'=8,'sp_1'=4,'fs'=4,'tp'=2] {'sp_1'}, dimensions={0}, use_global_device_ids=true | all-gather | bytes 327680 | tf_op jit(solution)/shard_map/all_gather | solution.py:35
  225.7 22.8 %all-gather.7 = bf16[64,64,64]{2,1,0:T(8,128)(2,1)S(1)} all-gather(bf16[8,64,64]{2,1,0:T(8,128)(2,1)S(1)} %get-tuple-element.46), channel_id=9, replica_groups=mesh['sp_0'=8,'sp_1'=4,'fs'=4,'tp'=2] {'sp_0'}, dimensions={0}, use_global_device_ids=true | all-gather | bytes 589824 | tf_op jit(solution)/shard_map/all_gather | solution.py:35
  249.3 22.1 %all-gather.5 = bf16[64,64,64]{2,1,0:T(8,128)(2,1)S(1)} all-gather(bf16[8,64,64]{2,1,0:T(8,128)(2,1)S(1)} %get-tuple-element.48), channel_id=7, replica_groups=mesh['sp_0'=8,'sp_1'=4,'fs'=4,'tp'=2] {'sp_0'}, dimensions={0}, use_global_device_ids=true | all-gather | bytes 589824 | tf_op jit(solution)/shard_map/all_gather | solution.py:35
  272.9 10.5 %all-gather.2 = bf16[4,8,1,64,64]{4,3,2,1,0:T(8,128)(2,1)S(1)} all-gather(bf16[1,8,1,64,64]{4,3,2,1,0:T(8,128)(2,1)S(1)} %get-tuple-element.23), channel_id=4, replica_groups=mesh['sp_0'=8,'sp_1'=4,'fs'=4,'tp'=2] {'sp_1'}, dimensions={0}, use_global_device_ids=true | all-gather | bytes 327680 | tf_op jit(solution)/shard_map/all_gather | solution.py:35
  283.4 10.2 %all-gather = bf16[4,8,1,64,64]{4,3,2,1,0:T(8,128)(2,1)S(1)} all-gather(bf16[1,8,1,64,64]{4,3,2,1,0:T(8,128)(2,1)S(1)} %get-tuple-element.21), channel_id=2, replica_groups=mesh['sp_0'=8,'sp_1'=4,'fs'=4,'tp'=2] {'sp_1'}, dimensions={0}, use_global_device_ids=true | all-gather | bytes 327680 | tf_op jit(solution)/shard_map/all_gather | solution.py:35
  295.7 20.4 %all-gather.3 = bf16[64,64,64]{2,1,0:T(8,128)(2,1)S(1)} all-gather(bf16[8,64,64]{2,1,0:T(8,128)(2,1)S(1)} %get-tuple-element.50), channel_id=5, replica_groups=mesh['sp_0'=8,'sp_1'=4,'fs'=4,'tp'=2] {'sp_0'}, dimensions={0}, use_global_device_ids=true | all-gather | bytes 589824 | tf_op jit(solution)/shard_map/all_gather | solution.py:35
  317.0 22.0 %all-gather.1 = bf16[64,64,64]{2,1,0:T(8,128)(2,1)S(1)} all-gather(bf16[8,64,64]{2,1,0:T(8,128)(2,1)S(1)} %get-tuple-element.52), channel_id=3, replica_groups=mesh['sp_0'=8,'sp_1'=4,'fs'=4,'tp'=2] {'sp_0'}, dimensions={0}, use_global_device_ids=true | all-gather | bytes 589824 | tf_op jit(solution)/shard_map/all_gather | solution.py:35
  345.3 3.0 fusion.30
  348.8 2.1 fusion.14
  350.9 1.8 copy.91
  352.7 1.9 stack.75
  354.6 1.8 rev.22
  356.3 2.0 copy.92
  363.5 3.1 convolution_select_fusion.3
  367.8 3.1 convolution_select_fusion
  372.2 2.0 convolution_add_fusion.8
  374.3 2.0 convolution_bitcast_fusion
  376.8 3.4 fusion.9
  382.6 2.1 fusion.214
  384.7 1.9 collective-permute-start.1
  386.6 5.5 %collective-permute-start = (bf16[8,512]{1,0:T(8,128)(2,1)S(1)}, bf16[8,512]{1,0:T(8,128)(2,1)S(1)}, u32[]{:S(2)}, u32[]{:S(2)}) collective-permute-start(bf16[8,512]{1,0:T(8,128)(2,1)S(1)} %get-tuple-element.34), channel_id=1, source_target_pairs={{0,8},{8,16},{16,24},{24,32},{32,40},{40,48},{48,56},{56,64},{64,7... | collective-permute-start | bytes 24584 | tf_op jit(solution)/shard_map/ppermute | solution.py:58
  392.1 34.8 %all_to_all.32 = bf16[2,64,512]{2,1,0:T(8,128)(2,1)S(1)} all-to-all(bf16[2,64,512]{2,1,0:T(8,128)(2,1)S(1)} %multiply_convert_fusion), channel_id=1, replica_groups=mesh['sp_0'=8,'sp_1'=4,'fs'=4,'tp'=2] {'tp'}, dimensions={0} | all-to-all | bytes 262144 | tf_op jit(solution)/shard_map/all_to_all | solution.py:280
  428.6 3.9 all_to_all.33
  432.5 3.6 fusion.222
  436.1 4.3 fusion.1
  (322 shorter events, 65.2 us)
Async XLA Ops:
  6.5 5.0 %copy-start = (bf16[2048,128]{1,0:T(8,128)(2,1)S(1)}, bf16[2048,128]{1,0:T(8,128)(2,1)}, u32[]{:S(2)}) copy-start(bf16[2048,128]{1,0:T(8,128)(2,1)} %param.24) | copy-start | bytes 1572868
  6.5 4.7 %copy-start.68 = (f32[2,512]{1,0:T(2,128)S(1)}, f32[2,512]{1,0:T(2,128)}, u32[]{:S(2)}) copy-start(f32[2,512]{1,0:T(2,128)} %param.26) | copy-start | bytes 12292
  6.5 4.7 %copy-start.67 = (bf16[2048]{0:T(1024)(128)(2,1)S(1)}, bf16[2048]{0:T(1024)(128)(2,1)}, u32[]{:S(2)}) copy-start(bf16[2048]{0:T(1024)(128)(2,1)} %param.19) | copy-start | bytes 12292
  6.5 4.7 %copy-start.5 = (bf16[1,128,2048]{2,1,0:T(8,128)(2,1)S(1)}, bf16[1,128,2048]{2,1,0:T(8,128)(2,1)}, u32[]{:S(2)}) copy-start(bf16[1,128,2048]{2,1,0:T(8,128)(2,1)} %param.18) | copy-start | bytes 1572868
  6.5 38.7 %all-gather.19.cloned.1.call-start = ((), (), s32[]{:S(2)}) async-start(), calls=%async_computation.3 | async-start | bytes 2621440 | tf_op jit(solution)/shard_map/all_gather | solution.py:152
  7.3 73.2 %all-gather.21.cloned.1.call-start = ((), (), s32[]{:S(2)}) async-start(), calls=%async_computation.4 | async-start | bytes 2621440 | tf_op jit(solution)/shard_map/all_gather | solution.py:153
  8.0 3.9 copy-start.74
  8.0 337.3 %all-gather.17.cloned.1.call-start = ((), (), s32[]{:S(2)}) async-start(), calls=%async_computation.2 | async-start | bytes 2621440 | tf_op jit(solution)/shard_map/all_gather | solution.py:151
  8.8 339.5 %all-gather.23.cloned.1.call-start = ((), (), s32[]{:S(2)}) async-start(), calls=%async_computation.5 | async-start | bytes 2621440 | tf_op jit(solution)/shard_map/all_gather | solution.py:155
  9.3 372.2 %all-gather.29.cloned.1.call-start = ((), (), s32[]{:S(2)}) async-start(), calls=%async_computation.8 | async-start | bytes 2621440 | tf_op jit(solution)/shard_map/all_gather | solution.py:156
  10.0 372.2 %all-gather.27.cloned.1.call-start = ((), (), s32[]{:S(2)}) async-start(), calls=%async_computation.7 | async-start | bytes 2621440 | tf_op jit(solution)/shard_map/all_gather | solution.py:154
  10.5 422.0 %all-gather.25.cloned.1.call-start = ((), (), s32[]{:S(2)}) async-start(), calls=%async_computation.6 | async-start | bytes 6291456 | tf_op jit(solution)/shard_map/all_gather | solution.py:284
  11.5 69.0 %copy-start.62 = (f32[128]{0:T(128)}, f32[128]{0:T(128)S(1)}, u32[]{:S(2)}) copy-start(f32[128]{0:T(128)S(1)} %add_rsqrt_fusion.2) | copy-start | bytes 1540
  93.6 4.2 copy-start.9
  93.6 13.6 %copy-start.7 = (f32[2,8,4,32,64]{4,1,2,3,0:T(8,128)}, f32[2,8,4,32,64]{4,1,2,3,0:T(8,128)S(1)}, u32[]{:S(2)}) copy-start(f32[2,8,4,32,64]{4,1,2,3,0:T(8,128)S(1)} %get-tuple-element.12) | copy-start | bytes 1572868
  93.6 28.3 %copy-start.15 = (f32[2,8,4,32,64]{4,1,2,3,0:T(8,128)}, f32[2,8,4,32,64]{4,1,2,3,0:T(8,128)S(1)}, u32[]{:S(2)}) copy-start(f32[2,8,4,32,64]{4,1,2,3,0:T(8,128)S(1)} %get-tuple-element.16) | copy-start | bytes 1572868
  114.5 17.9 %copy-start.22 = (f32[1,4,32,8,64]{4,2,1,3,0:T(8,128)}, f32[1,4,32,8,64]{4,2,1,3,0:T(8,128)S(1)}, u32[]{:S(2)}) copy-start(f32[1,4,32,8,64]{4,2,1,3,0:T(8,128)S(1)} %copy.129) | copy-start | bytes 786436
  119.5 6.6 %copy-start.11 = (f32[2,8,4,32,64]{4,3,2,1,0:T(8,128)}, f32[2,8,4,32,64]{4,3,2,1,0:T(8,128)S(1)}, u32[]{:S(2)}) copy-start(f32[2,8,4,32,64]{4,3,2,1,0:T(8,128)S(1)} %convolution_negate_fusion.1) | copy-start | bytes 1572868
  121.9 4.2 copy-start.13
  121.9 4.2 copy-start.59
  131.2 11.3 %copy-start.2 = (f32[2,8,4,64,64]{4,3,2,1,0:T(8,128)}, f32[2,8,4,64,64]{4,3,2,1,0:T(8,128)S(1)}, u32[]{:S(2)}) copy-start(f32[2,8,4,64,64]{4,3,2,1,0:T(8,128)S(1)} %multiply_add_fusion) | copy-start | bytes 3145732
  137.2 4.6 %copy-start.16 = (f32[2,8,4,64,64]{4,3,2,1,0:T(8,128)}, f32[2,8,4,64,64]{4,3,2,1,0:T(8,128)S(1)}, u32[]{:S(2)}) copy-start(f32[2,8,4,64,64]{4,3,2,1,0:T(8,128)S(1)} %convolution_add_fusion.1) | copy-start | bytes 3145732
  145.5 11.3 %slice-start.1 = ((f32[2,8,4,64,64]{4,3,2,1,0:T(8,128)}), f32[2,8,1,64,64]{4,3,2,1,0:T(8,128)S(1)}, s32[]{:S(2)}) async-start(f32[2,8,4,64,64]{4,3,2,1,0:T(8,128)} %copy-done.16), calls=%async_computation.11 | async-start | bytes 1048576 | tf_op jit(solution)/shard_map/slice | solution.py:214
  145.5 11.3 %copy-start.53 = (f32[2,8,1,64,64]{4,3,2,1,0:T(8,128)S(1)}, f32[2,8,1,64,64]{4,3,2,1,0:T(8,128)}, u32[]{:S(2)}) copy-start(f32[2,8,1,64,64]{4,3,2,1,0:T(8,128)} %fusion.13) | copy-start | bytes 786436
  156.9 11.2 %slice-start = ((f32[2,8,4,64,64]{4,3,2,1,0:T(8,128)}), f32[2,8,1,64,64]{4,3,2,1,0:T(8,128)S(1)}, s32[]{:S(2)}) async-start(f32[2,8,4,64,64]{4,3,2,1,0:T(8,128)} %copy-done.2), calls=%async_computation.10 | async-start | bytes 1048576 | tf_op jit(solution)/shard_map/slice | solution.py:214
  156.9 11.2 %copy-start.54 = (f32[2,8,1,64,64]{4,3,2,1,0:T(8,128)S(1)}, f32[2,8,1,64,64]{4,3,2,1,0:T(8,128)}, u32[]{:S(2)}) copy-start(f32[2,8,1,64,64]{4,3,2,1,0:T(8,128)} %convolution_bitcast_fusion.3) | copy-start | bytes 786436
  179.5 16.7 %copy-start.3 = (f32[2,8,4,64,64]{4,3,2,1,0:T(8,128)S(1)}, f32[2,8,4,64,64]{4,3,2,1,0:T(8,128)}, u32[]{:S(2)}) copy-start(f32[2,8,4,64,64]{4,3,2,1,0:T(8,128)} %pad.33) | copy-start | bytes 3145732
  196.2 12.9 %copy-start.18 = (f32[2,8,4,64,64]{4,3,2,1,0:T(8,128)S(1)}, f32[2,8,4,64,64]{4,3,2,1,0:T(8,128)}, u32[]{:S(2)}) copy-start(f32[2,8,4,64,64]{4,3,2,1,0:T(8,128)} %pad.28) | copy-start | bytes 3145732
  196.2 12.9 %copy-start.19 = (f32[2,8,4,64,64]{4,3,2,1,0:T(8,128)S(1)}, f32[2,8,4,64,64]{4,3,2,1,0:T(8,128)}, u32[]{:S(2)}) copy-start(f32[2,8,4,64,64]{4,3,2,1,0:T(8,128)} %pad.29) | copy-start | bytes 3145732
  224.4 24.6 %copy-start.33 = (f32[8,64,64]{2,1,0:T(8,128)}, f32[8,64,64]{2,1,0:T(8,128)S(1)}, u32[]{:S(2)}) copy-start(f32[8,64,64]{2,1,0:T(8,128)S(1)} %convolution_add_fusion.19) | copy-start | bytes 393220
  224.7 24.6 %copy-start.34 = (f32[8,64,64]{2,1,0:T(8,128)}, f32[8,64,64]{2,1,0:T(8,128)S(1)}, u32[]{:S(2)}) copy-start(f32[8,64,64]{2,1,0:T(8,128)S(1)} %convolution_add_fusion.18) | copy-start | bytes 393220
  294.2 22.2 %copy-start.45 = (f32[8,64,64]{2,1,0:T(8,128)}, f32[8,64,64]{2,1,0:T(8,128)S(1)}, u32[]{:S(2)}) copy-start(f32[8,64,64]{2,1,0:T(8,128)S(1)} %convolution_add_fusion.33) | copy-start | bytes 393220
  316.2 25.2 %copy-start.26 = (bf16[64,64,64]{2,1,0:T(8,128)(2,1)}, bf16[64,64,64]{2,1,0:T(8,128)(2,1)S(1)}, u32[]{:S(2)}) copy-start(bf16[64,64,64]{2,1,0:T(8,128)(2,1)S(1)} %all-gather.3) | copy-start | bytes 1572868
  348.3 87.8 %all-gather.31.cloned.1.call-start = ((), (), s32[]{:S(2)}) async-start(), calls=%async_computation.9 | async-start | bytes 6291456 | tf_op jit(solution)/shard_map/all_gather | solution.py:285
  358.3 2.6 copy-start.44
  358.3 2.6 copy-start.49
  358.3 2.6 copy-start.56
  358.3 4.0 copy-start.57
  359.6 3.1 copy-start.32
  359.6 3.1 copy-start.46
  359.7 3.1 copy-start.55
  363.5 3.1 copy-start.14
  367.8 3.1 copy-start.21
  367.8 3.1 copy-start.23
  382.0 10.1 %copy-start.64 = (f32[512]{0:T(512)S(1)}, f32[512]{0:T(512)}, u32[]{:S(2)}) copy-start(f32[512]{0:T(512)} %convert_element_type.431) | copy-start | bytes 6148
  384.7 42.3 %collective-permute-start.1 = (bf16[8,512]{1,0:T(8,128)(2,1)S(1)}, bf16[8,512]{1,0:T(8,128)(2,1)S(1)}, u32[]{:S(2)}, u32[]{:S(2)}) collective-permute-start(bf16[8,512]{1,0:T(8,128)(2,1)S(1)} %get-tuple-element.35), channel_id=1, source_target_pairs={{8,0},{16,8},{24,16},{32,24},{40,32},{48,40},{56,48},{64,56},{72,6... | collective-permute-start | bytes 24584 | tf_op jit(solution)/shard_map/ppermute | solution.py:60
  386.6 40.3 %collective-permute-start = (bf16[8,512]{1,0:T(8,128)(2,1)S(1)}, bf16[8,512]{1,0:T(8,128)(2,1)S(1)}, u32[]{:S(2)}, u32[]{:S(2)}) collective-permute-start(bf16[8,512]{1,0:T(8,128)(2,1)S(1)} %get-tuple-element.34), channel_id=1, source_target_pairs={{0,8},{8,16},{16,24},{24,32},{32,40},{40,48},{48,56},{56,64},{64,7... | collective-permute-start | bytes 24584 | tf_op jit(solution)/shard_map/ppermute | solution.py:58
  436.1 4.4 copy-start.1
  (40 other events, 64.4 us)
Sparse Core Ops, SparseCore 0:
  9.2 36.0 all-gather.18
  47.1 33.3 all-gather.20
  82.3 33.3 all-gather.16
  117.4 33.3 all-gather.22
  152.5 33.3 all-gather.28
  187.5 33.3 all-gather.26
  348.4 46.8 all-gather.24
  397.2 31.7 all-gather.30
where the time goes:
time: 453 us; the launch traced here: 448 us
  blocking collectives  169 us (37%)
  matrix products  97.2 us (21%)
  local copies, waits for them, and re-layouts  78.5 us (17%)
  waiting for transfers between devices  63.8 us (14%)
  between operations  15.5 us (3%)
  other arithmetic  15.2 us (3%)
  starting transfers between devices  8.1 us (2%)
    all_gather x8, blocking collectives, prefix_by_axis(): lax.all_gather(part.astype(kind), axis)  131 us
    dot_general x67, matrix products, contract(): return jnp.einsum(form, left, right, precision=highest)  77.7 us
    pad x4, local copies, waits for them, and re-layouts, shards(): lax.associative_scan(chain_combine, (transfer, carried), axis=2)  50.4 us
    all_to_all x1, blocking collectives, shards(): lax.all_to_all(attn_out, 'tp', split_axis=0, concat_axis=1, tiled=True)  34.8 us
    all_gather x1, waiting for transfers between devices, shards(): lax.all_gather(value_matrix, 'fs', axis=0, tiled=True)  32.9 us
    all_gather x1, waiting for transfers between devices, shards(): lax.all_gather(key_matrix, 'fs', axis=0, tiled=True)  27.2 us
    dot_general x6, matrix products, project(): jnp.dot(left, weight, preferred_element_type=jnp.float32)  9.99 us
    rev x12, local copies, waits for them, and re-layouts, both_ways(): stacked = jnp.stack([forward, jnp.flip(backward, axis=0)], axis=0)  9.63 us
  transfers between devices with their start and end apart: 10, of which 2 were waited for; matrix products, arithmetic and copies ran while one was open for 40% of the time, Pallas kernels for 0%

commit v1 on v0

v1 whole, which is shorter than its diff:
```python
import functools

import jax
import jax.numpy as jnp
from jax import lax
from jax.experimental import pallas as pl
from jax.experimental.pallas import tpu as pltpu
from jax.sharding import Mesh
from jax.sharding import PartitionSpec as P

SP = ("sp_0", "sp_1")
SP_TP = ("sp_0", "sp_1", "tp")
N_FS, N_X, N_Z = 4, 4, 8
TOK = 128
BLK = 32
N_BLK = TOK // BLK
PAIRS = 4
REACH = 8

norm_eps = 1e-06
head_eps = 0.00064
unit_eps = 1e-06
half_root = 0.6065306597126334
cap = 80.0

f32 = jnp.float32
bf16 = jnp.bfloat16
highest = lax.Precision.HIGHEST


def call(body, outs, scratch=(), flops=0, name=None):
    def run(scalars, *arrays):
        return pl.pallas_call(
            body,
            out_shape=[jax.ShapeDtypeStruct(s, d) for s, d in outs],
            in_specs=[pl.BlockSpec(memory_space=pltpu.SMEM)]
            + [pl.BlockSpec(memory_space=pltpu.VMEM)] * len(arrays),
            out_specs=[pl.BlockSpec(memory_space=pltpu.VMEM)] * len(outs),
            scratch_shapes=list(scratch),
            compiler_params=pltpu.CompilerParams(vmem_limit_bytes=48 << 20),
            cost_estimate=pl.CostEstimate(flops=flops, transcendentals=0, bytes_accessed=1 << 20),
            name=name,
        )(scalars, *arrays)

    return run


def dot(a, b):
    return jnp.dot(a, b, preferred_element_type=f32)


def dot_t(a, b):
    return lax.dot_general(a, b, (((1,), (1,)), ((), ())), preferred_element_type=f32)


def dot_0(a, b):
    return lax.dot_general(a, b, (((0,), (0,)), ((), ())), preferred_element_type=f32)


def iota2(shape):
    return (
        lax.broadcasted_iota(jnp.int32, shape, 0),
        lax.broadcasted_iota(jnp.int32, shape, 1),
    )


def roll64(a):
    return pltpu.roll(a, 64, axis=1)


def head_sum(a):
    row, lane = iota2((128, 128))
    same = jnp.where((row // 64) == (lane // 64), 1.0, 0.0).astype(f32)
    return jnp.dot(a, same, precision=highest, preferred_element_type=f32)


def mid_rows(way):
    return [i * BLK + (BLK // 2 - 1 if way == 0 else BLK // 2) for i in range(N_BLK)]


def both_heads(block, lane):
    zero = jnp.zeros_like(block)
    low = lane < 64
    return jnp.concatenate(
        [jnp.where(low, block, zero), jnp.where(low, zero, block)], axis=0
    ).astype(bf16)


def matmul_body(_, a0, a1, a2, a3, w1, w2, p0, p1, p2, p3):
    rows = jnp.concatenate([a0[...], a1[...], a2[...], a3[...]], axis=0)
    for half, w in enumerate((w1, w2)):
        got = dot(rows, w[...])
        cols = slice(half * 512, (half + 1) * 512)
        p0[:, cols] = got[:TOK]
        p1[:, cols] = got[TOK : 2 * TOK].astype(bf16)
        p2[:, cols] = got[2 * TOK : 3 * TOK].astype(bf16)
        p3[:, cols] = got[3 * TOK :].astype(bf16)


def maps_body(
    scal, own, r1, r2, r3, inv, act, lat, draise, dbias, rraise, rbias, tempo, sudden,
    o0, o1, o2, o3, right_out, reach_out, xy_out, maps,
):
    here = scal[0]
    row, lane = iota2((TOK, TOK))
    low = lane < 64
    wide_lane = lax.broadcasted_iota(jnp.int32, (TOK, 256), 1)
    wide_low = (wide_lane % 128) < 64
    eye = row == lane
    eye_bf = jnp.where(eye, 1.0, 0.0).astype(bf16)
    level_masks = []
    for level in range(7):
        size = 2**level
        hit = ((row // (2 * size)) == (lane // (2 * size))) & ((row // size) != (lane // size))
        level_masks.append(jnp.where(hit, 1.0, 0.0).astype(bf16))
    scale = inv[...]
    for pair in range(PAIRS):
        cols = slice(pair * 128, (pair + 1) * 128)
        vcols = slice(512 + pair * 128, 512 + (pair + 1) * 128)

        def total(c):
            got = own[:, c] + r1[:, c].astype(f32) + r2[:, c].astype(f32) + r3[:, c].astype(f32)
            return (got * scale).astype(bf16).astype(f32)

        key = total(cols)
        val = total(vcols)
        square = head_sum(key * key) + unit_eps
        inverse = lax.rsqrt(square)
        unit = key * inverse
        strong = val * (square * inverse)
        links = []
        sides = []
        tails = []
        ends = []
        for way in range(2):
            mine = (lane // 64) == way
            pre = dbias[way : way + 1, cols] + dot(
                jnp.where(mine, act[...], jnp.zeros_like(act[...])), draise[:, cols]
            )
            rate = jax.nn.sigmoid(
                rbias[way : way + 1, cols]
                + dot(jnp.where(mine, lat[...], jnp.zeros_like(lat[...])), rraise[:, cols])
            )
            at = way * 8 + pair * 2
            pace = jnp.where(low, tempo[:, at : at + 1], tempo[:, at + 1 : at + 2])
            jump = jnp.where(low, sudden[:, at : at + 1], sudden[:, at + 1 : at + 2])
            g = -half_root * jax.nn.sigmoid(pre) * pace + jump
            tri = (row >= lane) if way == 0 else (row <= lane)
            reach = jnp.dot(
                jnp.where(tri, 1.0, 0.0).astype(f32), g, precision=highest, preferred_element_type=f32
            )
            reach_out[way, :, cols] = reach
            removal = unit * rate
            before = reach - g
            pieces = []
            for i, mid_row in enumerate(mid_rows(way)):
                mid = reach[mid_row : mid_row + 1, :]
                rows = slice(i * BLK, (i + 1) * BLK)
                left = unit[rows] * jnp.exp(before[rows] - mid)
                right = (removal * jnp.exp(jnp.minimum(mid - reach, cap))).astype(bf16)
                right_out[way * PAIRS + pair, i] = right
                pieces.append(dot_t(both_heads(left, lane[:BLK]), right))
            strict = (row > lane) if way == 0 else (row < lane)
            for head in range(2):
                link = jnp.concatenate(
                    [piece[head * BLK : (head + 1) * BLK] for piece in pieces], axis=0
                )
                links.append(jnp.where(strict, link, 0.0).astype(bf16))
            sides.append(
                jnp.concatenate([strong, unit * jnp.exp(before)], axis=1).astype(bf16)
            )
            end = reach[TOK - 1 :, :] if way == 0 else reach[:1, :]
            tails.append((removal * jnp.exp(end - reach)).astype(bf16))
            ends.append(end)
        solved = [eye_bf - link * level_masks[0] for link in links]
        for level in range(1, 7):
            inner = [
                dot(link * level_masks[level], t).astype(bf16) for link, t in zip(links, solved)
            ]
            solved = [t - dot(t, part).astype(bf16) for t, part in zip(solved, inner)]
        for way in range(2):
            first = dot(solved[2 * way], sides[way])
            second = dot(solved[2 * way + 1], sides[way])
            xy = jnp.where(wide_low, first, second).astype(bf16)
            xy_out[way * PAIRS + pair] = xy
            got = dot_0(tails[way], xy)
            carry = got[:, :128]
            turn = jnp.where(eye, jnp.exp(ends[way]) - 1.0, 0.0) - got[:, 128:]
            packed = jnp.where(
                row < 64,
                jnp.where(low, carry, roll64(turn)),
                jnp.where(low, roll64(carry), turn),
            )
            maps[pair, way] = packed.astype(bf16)
    for s, out in enumerate((o0, o1, o2, o3)):
        out[...] = maps[(here + s) & 3]


def read_body(_, own, r1, r2, r3, inv, right, reach_in, xy_in, qeff, local):
    row, lane = iota2((TOK, TOK))
    wide_low = (lax.broadcasted_iota(jnp.int32, (TOK, 256), 1) % 128) < 64
    scale = inv[...]
    for pair in range(PAIRS):
        c = slice(pair * 128, (pair + 1) * 128)
        got = own[:, c] + r1[:, c].astype(f32) + r2[:, c].astype(f32) + r3[:, c].astype(f32)
        query = (got * scale).astype(bf16).astype(f32)
        base = None
        for way in range(2):
            reach = reach_in[way, :, c]
            pieces = []
            for i, mid_row in enumerate(mid_rows(way)):
                mid = reach[mid_row : mid_row + 1, :]
                rows = slice(i * BLK, (i + 1) * BLK)
                left = query[rows] * jnp.exp(reach[rows] - mid)
                pieces.append(
                    dot_t(both_heads(left, lane[:BLK]), right[way * PAIRS + pair, i])
                )
            within = (row >= lane) if way == 0 else (row <= lane)
            xy = xy_in[way * PAIRS + pair]
            pulls = []
            for head in range(2):
                link = jnp.concatenate(
                    [piece[head * BLK : (head + 1) * BLK] for piece in pieces], axis=0
                )
                pulls.append(dot(jnp.where(within, link, 0.0).astype(bf16), xy))
            pull = jnp.where(wide_low, pulls[0], pulls[1])
            base = pull[:, :128] if base is None else base + pull[:, :128]
            qeff[pair, :, way * 128 : (way + 1) * 128] = (
                query * jnp.exp(reach) - pull[:, 128:]
            ).astype(bf16)
        local[:, c] = base


def spread(packed, row, lane):
    moved = roll64(packed)
    return jnp.where(
        row < 64,
        jnp.where(lane < 64, moved, 0.0),
        jnp.where(lane < 64, 0.0, packed),
    ).astype(bf16)


def chain_body(scal, a0, a1, a2, a3, *rest):
    sends, before, maps = rest[:7], rest[7], rest[8]
    here, level = scal[0], scal[1]
    row, lane = iota2((TOK, TOK))
    ident = jnp.where((lane - 64) == (row % 64), 1.0, 0.0).astype(f32)
    for s, a in enumerate((a0, a1, a2, a3)):
        maps[s] = a[...]
    totals = []
    for way in range(2):
        state = None
        for step in range(N_X):
            at = step if way == 0 else N_X - 1 - step
            got = maps[(here - at) & 3, way].astype(f32)
            if state is None:
                state = got + ident
            else:
                state = (
                    state
                    + dot(spread(got, row, lane), state.astype(bf16))
                    + jnp.where(lane < 64, got, 0.0)
                )
            if step < N_X - 1:
                before[step, way] = (state - ident).astype(bf16)
        totals.append((state - ident))
    for s, send in enumerate(sends, start=1):
        send[...] = jnp.where(level + s < N_Z, totals[0], totals[1]).astype(bf16)


def apply_body(scal, *refs):
    got, before, outs, states = refs[:7], refs[7], refs[8:12], refs[12]
    here, level = scal[0], scal[1]
    row, lane = iota2((TOK, TOK))

    def step(state, packed):
        packed = packed.astype(f32)
        fresh = jnp.where(lane < 64, packed, 0.0)
        if state is None:
            return fresh
        return state + dot(spread(packed, row, lane), state.astype(bf16)) + fresh

    enter = []
    for way in range(2):
        state = jnp.zeros((TOK, TOK), f32)
        for k in range(1, N_Z):
            s = N_Z - k if way == 0 else k
            used = (s <= level) if way == 0 else (s > level)
            state = step(state, jnp.where(used, got[s - 1][...].astype(f32), 0.0))
        enter.append(state)
    for at in range(N_X):
        f = enter[0] if at == 0 else step(enter[0], before[at - 1, 0])
        back = N_X - 1 - at
        b = enter[1] if back == 0 else step(enter[1], before[back - 1, 1])
        states[at] = jnp.where(lane < 64, f, roll64(b)).astype(bf16)
    for s, out in enumerate(outs):
        out[...] = states[(here + s) & 3]


def final_body(
    scal, z0, z1, z2, z3, qeff, local, hgain, w0, w1, w2, w3, pool, keep, give, states, total
):
    here, seq, core = scal[0], scal[2], scal[3]
    row, lane = iota2((TOK, TOK))
    low = lane < 64
    top = row < 64
    for s, z in enumerate((z0, z1, z2, z3)):
        states[s] = z[...]
    cols = []
    for pair in range(PAIRS):
        c = slice(pair * 128, (pair + 1) * 128)
        packed = states[(here - pair) & 3].astype(f32)
        moved = roll64(packed)
        ahead = jnp.where(top, jnp.where(low, packed, 0.0), jnp.where(low, 0.0, moved))
        behind = jnp.where(top, jnp.where(low, moved, 0.0), jnp.where(low, 0.0, packed))
        block = jnp.concatenate([ahead, behind], axis=0).astype(bf16)
        read = dot(qeff[pair], block) + local[:, c]
        centred = read - head_sum(read) * (1.0 / 64.0)
        var = head_sum(centred * centred) * (1.0 / 64.0)
        cols.append(
            (centred * lax.rsqrt(var + head_eps) * hgain[:, c].astype(f32)).astype(bf16)
        )
    attn = jnp.concatenate(cols, axis=1)
    for s, w in enumerate((w0, w1, w2, w3)):
        at = pl.multiple_of(((seq - s) & 3) * 512, 512)
        total[:, pl.ds(at, 512)] = dot_t(attn, w[...]) + pool[:, pl.ds(at, 512)]
    mine = pl.multiple_of(core * 64, 64)
    other = pl.multiple_of((1 - core) * 64, 64)
    keep[...] = total[pl.ds(mine, 64), :]
    give[...] = total[pl.ds(other, 64), :].astype(bf16)


def pool_body(scal, pool_in, head, tail, mix, w0, w1, w2, w3, out):
    seq, core, span = scal[2], scal[3], scal[4]
    here = pool_in[...].astype(f32)
    cells = jnp.concatenate([tail[...].astype(f32), here, head[...].astype(f32)], axis=0)
    spot = lax.broadcasted_iota(jnp.int32, (TOK, 256), 0) + span * TOK
    length = TOK * N_X * N_Z
    sums = []
    running = cells
    for level in range(4):
        shift = 2**level
        size = running.shape[0]
        running = running[: size - shift] + running[shift:]
        sums.append(running[REACH - shift : REACH - shift + TOK])
    mixed = []
    for member in range(2):
        c = slice(member * 256, (member + 1) * 256)
        upper = core == 1
        chosen = jnp.where(upper, sums[member + 2][:, c], sums[member][:, c])
        half = jnp.where(upper, 2 ** (member + 2), 2**member)
        count = (jnp.minimum(spot + half, length) - jnp.maximum(spot - half, 0)).astype(f32)
        diff = (chosen / count - here[:, c]).astype(bf16)
        mixed.append(dot(diff, mix[member]).astype(bf16))
    pooled = jnp.concatenate(mixed, axis=1)
    for s, w in enumerate((w0, w1, w2, w3)):
        at = pl.multiple_of(((seq - s) & 3) * 512, 512)
        out[:, pl.ds(at, 512)] = dot_t(pooled, w[...])


def shift_by(a, axis, s, n):
    return lax.ppermute(a, axis, [(i, (i + s) % n) for i in range(n)])


def shards(
    inputs,
    input_norm_gain,
    receptance_matrix,
    key_matrix,
    value_matrix,
    pooling_input_weight,
    decay_lower_matrix,
    decay_raise_matrix,
    decay_offset_bias,
    removal_lower_matrix,
    removal_raise_matrix,
    removal_rate_bias,
    tempo_scale,
    sudden_decay_extra,
    head_norm_gain,
    group_mixing_weight,
    attention_output_matrix,
    pooling_output_matrix,
):
    seq = lax.axis_index("fs")
    core = lax.axis_index("tp")
    level = lax.axis_index("sp_0")
    here = lax.axis_index("sp_1")
    span = level * N_X + here
    scal = jnp.stack([here, level, seq, core, span]).astype(jnp.int32)
    tokens = inputs[0]
    wide = tokens.astype(f32)
    gained = (wide * input_norm_gain.astype(f32)).astype(bf16)

    def block(s):
        return lax.dynamic_slice(gained, (0, ((seq + s) % N_FS) * 512), (TOK, 512))

    rows = [block(0)] + [None] * 3
    for s in (2, 1, 3):
        rows[s] = shift_by(block(s), "fs", s, N_FS)
    inv = lax.rsqrt(jnp.mean(wide * wide, axis=-1, keepdims=True) + norm_eps)
    act = jnp.tanh((dot(gained, decay_lower_matrix) * inv).astype(bf16).astype(f32)).astype(bf16)
    lat = (dot(gained, removal_lower_matrix) * inv).astype(bf16)
    tempo = tempo_scale[0].reshape(16, TOK).T
    sudden = sudden_decay_extra[0].reshape(16, TOK).T

    part_shapes = [((TOK, 1024), f32)] + [((TOK, 1024), bf16)] * 3

    def partials(first, second, name):
        got = call(matmul_body, part_shapes, flops=1 << 29, name=name)(scal, *rows, first, second)
        back = [None] * 4
        back[0] = got[0]
        for s in (2, 1, 3):
            back[s] = shift_by(got[s], "fs", N_FS - s, N_FS)
        return back

    kv = partials(key_matrix, value_matrix, "project_kv")
    qp = partials(receptance_matrix, pooling_input_weight, "project_qp")

    outs = call(
        maps_body,
        [((2, TOK, TOK), bf16)] * 4
        + [((8, N_BLK, TOK, TOK), bf16), ((2, TOK, 512), f32), ((8, TOK, 256), bf16)],
        scratch=[pltpu.VMEM((PAIRS, 2, TOK, TOK), bf16)],
        flops=1 << 33,
        name="maps",
    )(
        scal, *kv, inv, act, lat,
        decay_raise_matrix.reshape(128, 512), decay_offset_bias,
        removal_raise_matrix.reshape(128, 512), removal_rate_bias,
        tempo, sudden,
    )
    maps, (right, reach, xy) = outs[:4], outs[4:]
    got = [maps[0]] + [shift_by(maps[s], "sp_1", s, N_X) for s in (1, 2, 3)]

    attn_own, pool_own, _ = lax.optimization_barrier(
        (attention_output_matrix, pooling_output_matrix, kv[1])
    )
    attn_w = [attn_own] + [shift_by(attn_own, "fs", s, N_FS) for s in (1, 2, 3)]
    pool_w = [pool_own] + [shift_by(pool_own, "fs", s, N_FS) for s in (1, 2, 3)]

    pool_sum = qp[0][:, 512:]
    for s in (1, 2, 3):
        pool_sum = pool_sum + qp[s][:, 512:].astype(f32)
    pool_in = (pool_sum * inv).astype(bf16)
    n_sp = N_X * N_Z
    tail = lax.ppermute(pool_in[TOK - REACH :], SP, [(i, i + 1) for i in range(n_sp - 1)])
    head = lax.ppermute(pool_in[:REACH], SP, [(i + 1, i) for i in range(n_sp - 1)])

    qeff, local = call(
        read_body,
        [((PAIRS, TOK, 256), bf16), ((TOK, 512), f32)],
        flops=1 << 31,
        name="reads",
    )(scal, *qp, inv, right, reach, xy)

    outs = call(
        chain_body,
        [((TOK, TOK), bf16)] * 7 + [((3, 2, TOK, TOK), bf16)],
        scratch=[pltpu.VMEM((N_X, 2, TOK, TOK), bf16)],
        flops=1 << 29,
        name="chain",
    )(scal, *got)
    sends, before = outs[:7], outs[7]
    passed = [shift_by(sends[s - 1], "sp_0", s, N_Z) for s in range(1, N_Z)]

    (pool_part,) = call(pool_body, [((TOK, 2048), f32)], flops=1 << 30, name="pool")(
        scal, pool_in, head, tail, group_mixing_weight, *pool_w
    )

    states = call(
        apply_body,
        [((TOK, TOK), bf16)] * 4,
        scratch=[pltpu.VMEM((N_X, TOK, TOK), bf16)],
        flops=1 << 29,
        name="enter",
    )(scal, *passed, before)
    enter = [states[0]] + [shift_by(states[s], "sp_1", s, N_X) for s in (1, 2, 3)]

    keep, give = call(
        final_body,
        [((64, 2048), f32), ((64, 2048), bf16)],
        scratch=[pltpu.VMEM((N_X, TOK, TOK), bf16), pltpu.VMEM((TOK, 2048), f32)],
        flops=1 << 30,
        name="final",
    )(scal, *enter, qeff, local, head_norm_gain.reshape(1, 512), *attn_w, pool_part)
    taken = lax.ppermute(give, "tp", [(0, 1), (1, 0)])
    return (keep + taken.astype(f32)).astype(bf16)[None]


def solution(mesh):
    split = Mesh(
        mesh.devices.reshape(8, 4, mesh.shape["fs"], mesh.shape["tp"]), ("sp_0", "sp_1", "fs", "tp")
    )
    in_specs = (
        P("fs", SP, None),
        P(),
        P("fs", "tp"),
        P("fs", "tp"),
        P("fs", "tp"),
        P("fs", "tp"),
        P(),
        P(None, None, "tp"),
        P(None, "tp"),
        P(),
        P(None, None, "tp"),
        P(None, "tp"),
        P("fs", None, "tp", SP),
        P("fs", None, "tp", SP),
        P("tp"),
        P("tp", None, None),
        P("fs", "tp"),
        P("fs", "tp"),
    )
    out_specs = P("fs", SP_TP, None)
    return jax.shard_map(
        shards, mesh=split, in_specs=in_specs, out_specs=out_specs, check_vma=False
    )
```

time: 453 us -> 128 us (0.28)
  blocking collectives: 169 us -> 0 us
  matrix products: 97.2 us -> 0.6 us
  local copies, waits for them, and re-layouts: 78.5 us -> 4 us
  starting transfers between devices: 8.1 us -> 45.5 us
  Pallas kernels: 0 us -> 25.7 us
  waiting for transfers between devices: 63.8 us -> 48.2 us
  between operations: 15.5 us -> 0.22 us
  other arithmetic: 15.2 us -> 2.12 us
    all_gather x8 -> x0, blocking collectives: 131 us -> none  [prefix_by_axis(): lax.all_gather(part.astype(kind), axis)]
    dot_general x81 -> x2, matrix products: 97.2 us -> 0.6 us  [dot(): return jnp.dot(a, b, preferred_element_type=f32)]
    all_gather x8 -> x0, waiting for transfers between devices: 60.2 us -> none  [the longest x1 32.9 us: shards(): lax.all_gather(value_matrix, 'fs', axis=0, tiled=True)]
    pad x4 -> x0, local copies, waits for them, and re-layouts: 50.4 us -> none  [shards(): lax.associative_scan(chain_combine, (transfer, carried), axis=2)]
    ppermute x2 -> x31, waiting for transfers between devices: 0.01 us -> 48.2 us  [the longest x28 40.4 us: shift_by(): return lax.ppermute(a, axis, [(i, (i + s) % n) for i in range(n)])]
    all_to_all x2 -> x0, blocking collectives: 38.6 us -> none  [the longest x1 34.8 us: shards(): lax.all_to_all(attn_out, 'tp', split_axis=0, concat_axis=1, tiled=True)]
    ppermute x2 -> x31, starting transfers between devices: 7.39 us -> 45.5 us  [the longest x28 38.5 us: shift_by(): return lax.ppermute(a, axis, [(i, (i + s) % n) for i in range(n)])]
    pallas_call x0 -> x8, Pallas kernels: none -> 25.7 us  [run(): pl.pallas_call(body, out_shape=[jax.ShapeDtypeStruct(s, d) for s, d in ou...]
  transfers between devices with their start and end apart: 10 -> 31, of which waited for: 2 -> 13; matrix products, arithmetic and copies ran while one was open for 40% -> 1% of each run, Pallas kernels for 0% -> 17%
where the time goes in v1:
time: 128 us; the launch traced here: 126 us
  waiting for transfers between devices  48.2 us (38%)
  starting transfers between devices  45.5 us (36%)
  Pallas kernels  25.7 us (20%)
  local copies, waits for them, and re-layouts  4 us (3%)
  other arithmetic  2.12 us (2%)
    ppermute x28, waiting for transfers between devices, shift_by(): return lax.ppermute(a, axis, [(i, (i + s) % n) for i in range(n)])  40.4 us
    ppermute x28, starting transfers between devices, shift_by(): return lax.ppermute(a, axis, [(i, (i + s) % n) for i in range(n)])  38.5 us
    pallas_call x8, Pallas kernels, run(): pl.pallas_call(body, out_shape=[jax.ShapeDtypeStruct(s, d) for s, d in ou...  25.7 us
    ppermute x1, waiting for transfers between devices, shards(): lax.ppermute(pool_in[:REACH], SP, [(i + 1, i) for i in range(n_sp - 1)])  3.88 us
    unnamed x34, local copies, waits for them, and re-layouts  3.55 us
    ppermute x1, starting transfers between devices, shards(): lax.ppermute(pool_in[:REACH], SP, [(i + 1, i) for i in range(n_sp - 1)])  3.03 us
    ppermute x1, waiting for transfers between devices, shards(): lax.ppermute(pool_in[TOK - REACH:], SP, [(i, i + 1) for i in range(n_sp -...  2.76 us
  transfers between devices with their start and end apart: 31, of which 13 were waited for; matrix products, arithmetic and copies ran while one was open for 1% of the time, Pallas kernels for 17%

profile of v1, /device:TPU:7, one launch (start us, length us, event | category | flops | bytes accessed | tf_op | source)
XLA Modules:
  0.0 126.3 jit_solution(6961517494819196403)
XLA Ops:
  0.0 0.7 copy-done.15
  0.8 1.3 %fusion.6 = (f32[128]{0:T(128)S(1)}, bf16[128,2048]{1,0:T(8,128)(2,1)S(1)}) fusion(bf16[1,128,2048]{2,1,0:T(8,128)(2,1)} %param.18, f32[2048]{0:T(1024)S(1)} %convert_element_type.44), kind=kLoop, calls=%fused_computation.10 | loop fusion | flops 1310592 | bytes 1057280 | tf_op jit(solution)/shard_map/reduce_sum | solution.py:401
  2.1 1.4 %collective-permute-start = (bf16[128,512]{1,0:T(8,128)(2,1)S(1)}, bf16[128,512]{1,0:T(8,128)(2,1)S(1)}, u32[]{:S(2)}, u32[]{:S(2)}) collective-permute-start(bf16[128,512]{1,0:T(8,128)(2,1)S(1)} %get-tuple-element.75), channel_id=1, source_target_pairs={{0,2},{2,4},{4,6},{6,0},{1,3},{3,5},{5,7},{7,1},{8,10},{10,12},{12... | collective-permute-start | bytes 393224 | tf_op jit(solution)/shard_map/ppermute | solution.py:362
  3.5 2.6 %collective-permute-start.1 = (bf16[128,512]{1,0:T(8,128)(2,1)S(1)}, bf16[128,512]{1,0:T(8,128)(2,1)S(1)}, u32[]{:S(2)}, u32[]{:S(2)}) collective-permute-start(bf16[128,512]{1,0:T(8,128)(2,1)S(1)} %get-tuple-element.74), channel_id=1, source_target_pairs={{0,4},{2,6},{4,0},{6,2},{1,5},{3,7},{5,1},{7,3},{8,12},{10,14},{12... | collective-permute-start | bytes 393224 | tf_op jit(solution)/shard_map/ppermute | solution.py:362
  6.1 1.1 collective-permute-start.2
  9.1 2.7 %collective-permute-done.1.a2 = bf16[128,512]{1,0:T(8,128)(2,1)S(1)} collective-permute-done((bf16[128,512]{1,0:T(8,128)(2,1)S(1)}, bf16[128,512]{1,0:T(8,128)(2,1)S(1)}, u32[]{:S(2)}, u32[]{:S(2)}) %collective-permute-start.1) | collective-permute-done | bytes 131104 | tf_op jit(solution)/shard_map/ppermute | solution.py:362
  11.8 1.2 project_kv.1
  13.1 2.3 %collective-permute-start.3 = (bf16[128,1024]{1,0:T(8,128)(2,1)S(1)}, bf16[128,1024]{1,0:T(8,128)(2,1)S(1)}, u32[]{:S(2)}, u32[]{:S(2)}) collective-permute-start(bf16[128,1024]{1,0:T(8,128)(2,1)S(1)} %get-tuple-element.39), channel_id=1, source_target_pairs={{0,6},{2,0},{4,2},{6,4},{1,7},{3,1},{5,3},{7,5},{8,14},{10,8},{12,... | collective-permute-start | bytes 786440 | tf_op jit(solution)/shard_map/ppermute | solution.py:362
  15.4 0.8 collective-permute-start.4
  16.5 0.7 copy-done.3
  17.4 1.2 project_qp.1
  18.6 1.9 %collective-permute-start.19 = (bf16[128,1024]{1,0:T(8,128)(2,1)S(1)}, bf16[128,1024]{1,0:T(8,128)(2,1)S(1)}, u32[]{:S(2)}, u32[]{:S(2)}) collective-permute-start(bf16[128,1024]{1,0:T(8,128)(2,1)S(1)} %get-tuple-element.59), channel_id=1, source_target_pairs={{0,6},{2,0},{4,2},{6,4},{1,7},{3,1},{5,3},{7,5},{8,14},{10,8},{12,... | collective-permute-start | bytes 786440 | tf_op jit(solution)/shard_map/ppermute | solution.py:362
  20.5 1.0 collective-permute-start.20
  21.8 1.6 %collective-permute-done.4.r2 = bf16[128,1024]{1,0:T(8,128)(2,1)S(1)} collective-permute-done((bf16[128,1024]{1,0:T(8,128)(2,1)S(1)}, bf16[128,1024]{1,0:T(8,128)(2,1)S(1)}, u32[]{:S(2)}, u32[]{:S(2)}) %collective-permute-start.4) | collective-permute-done | bytes 262176 | tf_op jit(solution)/shard_map/ppermute | solution.py:362
  23.3 9.2 %collective-permute-done.5.r3 = bf16[128,1024]{1,0:T(8,128)(2,1)S(1)} collective-permute-done((bf16[128,1024]{1,0:T(8,128)(2,1)S(1)}, bf16[128,1024]{1,0:T(8,128)(2,1)S(1)}, u32[]{:S(2)}, u32[]{:S(2)}) %collective-permute-start.5) | collective-permute-done | bytes 262176 | tf_op jit(solution)/shard_map/ppermute | solution.py:362
  32.5 0.7 copy-done.11
  33.2 13.0 %maps.1 = (bf16[2,128,128]{2,1,0:T(8,128)(2,1)S(1)}, bf16[2,128,128]{2,1,0:T(8,128)(2,1)S(1)}, bf16[2,128,128]{2,1,0:T(8,128)(2,1)S(1)}, bf16[2,128,128]{2,1,0:T...) custom-call(s32[5]{0:T(128)S(1)} %stack.23._.scal, ...), custom_call_target="tpu_custom_call" | custom-call | flops 8589934592 | bytes 1048576 | tf_op jit(solution)/shard_map/maps/pallas_call | solution.py:33
  46.3 2.3 %collective-permute-start.7 = (bf16[2,128,128]{2,1,0:T(8,128)(2,1)S(1)}, bf16[2,128,128]{2,1,0:T(8,128)(2,1)S(1)}, u32[]{:S(2)}, u32[]{:S(2)}) collective-permute-start(bf16[2,128,128]{2,1,0:T(8,128)(2,1)S(1)} %get-tuple-element.44), channel_id=1, source_target_pairs={{0,16},{8,24},{16,0},{24,8},{1,17},{9,25},{17,1},{25,9},{2,18},{10... | collective-permute-start | bytes 196616 | tf_op jit(solution)/shard_map/ppermute | solution.py:362
  48.6 0.8 collective-permute-done.6.a1
  49.9 1.1 collective-permute-done.7.a2
  51.0 3.2 %collective-permute-done.8.a3 = bf16[2,128,128]{2,1,0:T(8,128)(2,1)S(1)} collective-permute-done((bf16[2,128,128]{2,1,0:T(8,128)(2,1)S(1)}, bf16[2,128,128]{2,1,0:T(8,128)(2,1)S(1)}, u32[]{:S(2)}, u32[]{:S(2)}) %collective-permute-start.8) | collective-permute-done | bytes 65568 | tf_op jit(solution)/shard_map/ppermute | solution.py:362
  54.2 1.2 chain.1
  55.4 1.2 collective-permute-start.9
  56.6 3.0 %collective-permute-start.10 = (bf16[128,128]{1,0:T(8,128)(2,1)S(1)}, bf16[128,128]{1,0:T(8,128)(2,1)S(1)}, u32[]{:S(2)}, u32[]{:S(2)}) collective-permute-start(bf16[128,128]{1,0:T(8,128)(2,1)S(1)} %get-tuple-element.47), channel_id=1, source_target_pairs={{0,64},{32,96},{64,128},{96,160},{128,192},{160,224},{192,0},{224,... | collective-permute-start | bytes 98312 | tf_op jit(solution)/shard_map/ppermute | solution.py:362
  59.6 3.8 %collective-permute-start.11 = (bf16[128,128]{1,0:T(8,128)(2,1)S(1)}, bf16[128,128]{1,0:T(8,128)(2,1)S(1)}, u32[]{:S(2)}, u32[]{:S(2)}) collective-permute-start(bf16[128,128]{1,0:T(8,128)(2,1)S(1)} %get-tuple-element.48), channel_id=1, source_target_pairs={{0,96},{32,128},{64,160},{96,192},{128,224},{160,0},{192,32},{224,... | collective-permute-start | bytes 98312 | tf_op jit(solution)/shard_map/ppermute | solution.py:362
  63.4 0.9 collective-permute-start.12
  64.3 4.2 %collective-permute-start.13 = (bf16[128,128]{1,0:T(8,128)(2,1)S(1)}, bf16[128,128]{1,0:T(8,128)(2,1)S(1)}, u32[]{:S(2)}, u32[]{:S(2)}) collective-permute-start(bf16[128,128]{1,0:T(8,128)(2,1)S(1)} %get-tuple-element.50), channel_id=1, source_target_pairs={{0,160},{32,192},{64,224},{96,0},{128,32},{160,64},{192,96},{224,1... | collective-permute-start | bytes 98312 | tf_op jit(solution)/shard_map/ppermute | solution.py:362
  68.4 2.4 %collective-permute-start.14 = (bf16[128,128]{1,0:T(8,128)(2,1)S(1)}, bf16[128,128]{1,0:T(8,128)(2,1)S(1)}, u32[]{:S(2)}, u32[]{:S(2)}) collective-permute-start(bf16[128,128]{1,0:T(8,128)(2,1)S(1)} %get-tuple-element.51), channel_id=1, source_target_pairs={{0,192},{32,224},{64,0},{96,32},{128,64},{160,96},{192,128},{224,1... | collective-permute-start | bytes 98312 | tf_op jit(solution)/shard_map/ppermute | solution.py:362
  70.8 0.7 collective-permute-start.15
  71.7 0.9 collective-permute-start.28
  72.6 2.0 %collective-permute-start.29 = (bf16[512,512]{1,0:T(8,128)(2,1)S(1)}, bf16[512,512]{1,0:T(8,128)(2,1)S(1)}, u32[]{:S(2)}, u32[]{:S(2)}) collective-permute-start(bf16[512,512]{1,0:T(8,128)(2,1)S(1)} %copy-done.5), channel_id=1, source_target_pairs={{0,6},{2,0},{4,2},{6,4},{1,7},{3,1},{5,3},{7,5},{8,14},{10,8},{12,... | collective-permute-start | bytes 1572872 | tf_op jit(solution)/shard_map/ppermute | solution.py:362
  74.6 2.5 %enter.1 = (bf16[128,128]{1,0:T(8,128)(2,1)S(1)}, bf16[128,128]{1,0:T(8,128)(2,1)S(1)}, bf16[128,128]{1,0:T(8,128)(2,1)S(1)}, bf16[128,128]{1,0:T(8,128)(2,1)S(1)}) custom-call(s32[5]{0:T(128)S(1)} %stack.23._.scal, bf16[128,128]{1,0:T(8,128)(2,1)S(1)} %collective-permute-done.9.refs_0_, bf16[128,128]{1,0:T(8,128)(2,1)S(1)} %collective-permute-done.10.refs_1_, ...), custom_call_target="tpu_custom_call" | custom-call | flops 536870912 | bytes 1048576 | tf_op jit(solution)/shard_map/enter/pallas_call | solution.py:33
  77.7 3.0 %collective-permute-start.25 = (bf16[8,512]{1,0:T(8,128)(2,1)S(1)}, bf16[8,512]{1,0:T(8,128)(2,1)S(1)}, u32[]{:S(2)}, u32[]{:S(2)}) collective-permute-start(bf16[8,512]{1,0:T(8,128)(2,1)S(1)} %get-tuple-element.78), channel_id=1, source_target_pairs={{8,0},{16,8},{24,16},{32,24},{40,32},{48,40},{56,48},{64,56},{72,6... | collective-permute-start | bytes 24584 | tf_op jit(solution)/shard_map/ppermute | solution.py:448
  80.7 3.9 %collective-permute-done.25.head = bf16[8,512]{1,0:T(8,128)(2,1)S(1)} collective-permute-done((bf16[8,512]{1,0:T(8,128)(2,1)S(1)}, bf16[8,512]{1,0:T(8,128)(2,1)S(1)}, u32[]{:S(2)}, u32[]{:S(2)}) %collective-permute-start.25) | collective-permute-done | bytes 8224 | tf_op jit(solution)/shard_map/ppermute | solution.py:448
  84.6 1.9 %collective-permute-start.26 = (bf16[8,512]{1,0:T(8,128)(2,1)S(1)}, bf16[8,512]{1,0:T(8,128)(2,1)S(1)}, u32[]{:S(2)}, u32[]{:S(2)}) collective-permute-start(bf16[8,512]{1,0:T(8,128)(2,1)S(1)} %get-tuple-element.77), channel_id=1, source_target_pairs={{0,8},{8,16},{16,24},{24,32},{32,40},{40,48},{48,56},{56,64},{64,7... | collective-permute-start | bytes 24584 | tf_op jit(solution)/shard_map/ppermute | solution.py:447
  86.5 2.8 %collective-permute-done.26.tail = bf16[8,512]{1,0:T(8,128)(2,1)S(1)} collective-permute-done((bf16[8,512]{1,0:T(8,128)(2,1)S(1)}, bf16[8,512]{1,0:T(8,128)(2,1)S(1)}, u32[]{:S(2)}, u32[]{:S(2)}) %collective-permute-start.26) | collective-permute-done | bytes 8224 | tf_op jit(solution)/shard_map/ppermute | solution.py:447
  89.3 3.0 %collective-permute-start.23 = (bf16[512,512]{1,0:T(8,128)(2,1)S(1)}, bf16[512,512]{1,0:T(8,128)(2,1)S(1)}, u32[]{:S(2)}, u32[]{:S(2)}) collective-permute-start(bf16[512,512]{1,0:T(8,128)(2,1)S(1)} %copy-done.6), channel_id=1, source_target_pairs={{0,4},{2,6},{4,0},{6,2},{1,5},{3,7},{5,1},{7,3},{8,12},{10,14},{12... | collective-permute-start | bytes 1572872 | tf_op jit(solution)/shard_map/ppermute | solution.py:362
  92.9 2.2 %reads.1 = (bf16[4,128,256]{2,1,0:T(8,128)(2,1)S(1)}, f32[128,512]{1,0:T(8,128)S(1)}) custom-call(s32[5]{0:T(128)S(1)} %stack.23._.scal, f32[128,1024]{1,0:T(8,128)S(1)} %get-tuple-element.58.own, bf16[128,1024]{1,0:T(8,128)(2,1)S(1)} %collective-permute-done.19.r1, bf16[128,1024]{1,0:T(8,128)(2,1)S(1)} %collective-permute-done.20.r2, ...), custom_call_target="tpu_custom_call" | custom-call | flops 2147483648 | bytes 1048576 | tf_op jit(solution)/shard_map/reads/pallas_call | solution.py:33
  95.4 5.5 %collective-permute-done.29.w3 = bf16[512,512]{1,0:T(8,128)(2,1)S(1)} collective-permute-done((bf16[512,512]{1,0:T(8,128)(2,1)S(1)}, bf16[512,512]{1,0:T(8,128)(2,1)S(1)}, u32[]{:S(2)}, u32[]{:S(2)}) %collective-permute-start.29) | collective-permute-done | bytes 524320 | tf_op jit(solution)/shard_map/ppermute | solution.py:362
  100.9 0.8 collective-permute-start.18
  101.7 1.5 %pool.1 = f32[128,2048]{1,0:T(8,128)S(1)} custom-call(s32[5]{0:T(128)S(1)} %stack.23._.scal, bf16[128,512]{1,0:T(8,128)(2,1)S(1)} %multiply_convert_fusion.pool_in, bf16[8,512]{1,0:T(8,128)(2,1)S(1)} %collective-permute-done.25.head, bf16[8,512]{1,0:T(8,128)(2,1)S(1)} %collective-permute-done.26.tail, bf16[2,256,256]{2,1,0:T(8,128)(2,1)S(1)} %copy-done.7, ...), custom_call_target="tpu_custom_call" | custom-call | flops 1073741824 | bytes 1048576 | tf_op jit(solution)/shard_map/pool/pallas_call | solution.py:33
  103.2 2.0 %collective-permute-done.18.z3 = bf16[128,128]{1,0:T(8,128)(2,1)S(1)} collective-permute-done((bf16[128,128]{1,0:T(8,128)(2,1)S(1)}, bf16[128,128]{1,0:T(8,128)(2,1)S(1)}, u32[]{:S(2)}, u32[]{:S(2)}) %collective-permute-start.18) | collective-permute-done | bytes 32800 | tf_op jit(solution)/shard_map/ppermute | solution.py:362
  105.2 1.8 %collective-permute-done.23.w2 = bf16[512,512]{1,0:T(8,128)(2,1)S(1)} collective-permute-done((bf16[512,512]{1,0:T(8,128)(2,1)S(1)}, bf16[512,512]{1,0:T(8,128)(2,1)S(1)}, u32[]{:S(2)}, u32[]{:S(2)}) %collective-permute-start.23) | collective-permute-done | bytes 524320 | tf_op jit(solution)/shard_map/ppermute | solution.py:362
  107.0 12.6 %collective-permute-done.24.w3 = bf16[512,512]{1,0:T(8,128)(2,1)S(1)} collective-permute-done((bf16[512,512]{1,0:T(8,128)(2,1)S(1)}, bf16[512,512]{1,0:T(8,128)(2,1)S(1)}, u32[]{:S(2)}, u32[]{:S(2)}) %collective-permute-start.24) | collective-permute-done | bytes 524320 | tf_op jit(solution)/shard_map/ppermute | solution.py:362
  119.5 2.8 %final.1 = (f32[64,2048]{1,0:T(8,128)S(1)}, bf16[64,2048]{1,0:T(8,128)(2,1)S(1)}) custom-call(s32[5]{0:T(128)S(1)} %stack.23._.scal, bf16[128,128]{1,0:T(8,128)(2,1)S(1)} %get-tuple-element.54.z0, bf16[128,128]{1,0:T(8,128)(2,1)S(1)} %collective-permute-done.16.z1, bf16[128,128]{1,0:T(8,128)(2,1)S(1)} %collective-permute-done.17.z2, ...), custom_call_target="tpu_custom_call" | custom-call | flops 1073741824 | bytes 1048576 | tf_op jit(solution)/shard_map/final/pallas_call | solution.py:33
  122.4 2.1 %collective-permute-start.30 = (bf16[64,2048]{1,0:T(8,128)(2,1)S(1)}, bf16[64,2048]{1,0:T(8,128)(2,1)S(1)}, u32[]{:S(2)}, u32[]{:S(2)}) collective-permute-start(bf16[64,2048]{1,0:T(8,128)(2,1)S(1)} %get-tuple-element.70), channel_id=1, source_target_pairs={{0,1},{1,0},{2,3},{3,2},{4,5},{5,4},{6,7},{7,6},{8,9},{9,8},{10,11... | collective-permute-start | bytes 786440 | tf_op jit(solution)/shard_map/ppermute | solution.py:487
  124.4 1.2 collective-permute-done.30
  125.6 0.8 fusion.7
  (70 shorter events, 4.9 us)
Async XLA Ops:
  0.0 8.8 %copy-start = (bf16[2048,128]{1,0:T(8,128)(2,1)S(1)}, bf16[2048,128]{1,0:T(8,128)(2,1)}, u32[]{:S(2)}) copy-start(bf16[2048,128]{1,0:T(8,128)(2,1)} %param.24) | copy-start | bytes 1572868
  0.0 0.7 copy-start.15
  2.1 7.0 %collective-permute-start = (bf16[128,512]{1,0:T(8,128)(2,1)S(1)}, bf16[128,512]{1,0:T(8,128)(2,1)S(1)}, u32[]{:S(2)}, u32[]{:S(2)}) collective-permute-start(bf16[128,512]{1,0:T(8,128)(2,1)S(1)} %get-tuple-element.75), channel_id=1, source_target_pairs={{0,2},{2,4},{4,6},{6,0},{1,3},{3,5},{5,7},{7,1},{8,10},{10,12},{12... | collective-permute-start | bytes 393224 | tf_op jit(solution)/shard_map/ppermute | solution.py:362
  3.5 8.3 %collective-permute-start.1 = (bf16[128,512]{1,0:T(8,128)(2,1)S(1)}, bf16[128,512]{1,0:T(8,128)(2,1)S(1)}, u32[]{:S(2)}, u32[]{:S(2)}) collective-permute-start(bf16[128,512]{1,0:T(8,128)(2,1)S(1)} %get-tuple-element.74), channel_id=1, source_target_pairs={{0,4},{2,6},{4,0},{6,2},{1,5},{3,7},{5,1},{7,3},{8,12},{10,14},{12... | collective-permute-start | bytes 393224 | tf_op jit(solution)/shard_map/ppermute | solution.py:362
  6.1 5.7 %collective-permute-start.2 = (bf16[128,512]{1,0:T(8,128)(2,1)S(1)}, bf16[128,512]{1,0:T(8,128)(2,1)S(1)}, u32[]{:S(2)}, u32[]{:S(2)}) collective-permute-start(bf16[128,512]{1,0:T(8,128)(2,1)S(1)} %get-tuple-element.73), channel_id=1, source_target_pairs={{0,6},{2,0},{4,2},{6,4},{1,7},{3,1},{5,3},{7,5},{8,14},{10,8},{12,... | collective-permute-start | bytes 393224 | tf_op jit(solution)/shard_map/ppermute | solution.py:362
  7.2 0.7 copy-start.13
  7.9 0.7 copy-start.14
  8.8 3.1 %copy-start.1 = (bf16[512,512]{1,0:T(8,128)(2,1)S(1)}, bf16[512,512]{1,0:T(8,128)(2,1)}, u32[]{:S(2)}) copy-start(bf16[512,512]{1,0:T(8,128)(2,1)} %w1.2) | copy-start | bytes 1572868
  8.8 3.1 %copy-start.2 = (bf16[512,512]{1,0:T(8,128)(2,1)S(1)}, bf16[512,512]{1,0:T(8,128)(2,1)}, u32[]{:S(2)}) copy-start(bf16[512,512]{1,0:T(8,128)(2,1)} %w2.2) | copy-start | bytes 1572868
  11.8 4.4 %copy-start.12 = (bf16[2048,128]{1,0:T(8,128)(2,1)S(1)}, bf16[2048,128]{1,0:T(8,128)(2,1)}, u32[]{:S(2)}) copy-start(bf16[2048,128]{1,0:T(8,128)(2,1)} %param.27) | copy-start | bytes 1572868
  13.1 8.4 %collective-permute-start.3 = (bf16[128,1024]{1,0:T(8,128)(2,1)S(1)}, bf16[128,1024]{1,0:T(8,128)(2,1)S(1)}, u32[]{:S(2)}, u32[]{:S(2)}) collective-permute-start(bf16[128,1024]{1,0:T(8,128)(2,1)S(1)} %get-tuple-element.39), channel_id=1, source_target_pairs={{0,6},{2,0},{4,2},{6,4},{1,7},{3,1},{5,3},{7,5},{8,14},{10,8},{12,... | collective-permute-start | bytes 786440 | tf_op jit(solution)/shard_map/ppermute | solution.py:362
  15.4 7.9 %collective-permute-start.4 = (bf16[128,1024]{1,0:T(8,128)(2,1)S(1)}, bf16[128,1024]{1,0:T(8,128)(2,1)S(1)}, u32[]{:S(2)}, u32[]{:S(2)}) collective-permute-start(bf16[128,1024]{1,0:T(8,128)(2,1)S(1)} %get-tuple-element.40), channel_id=1, source_target_pairs={{0,4},{2,6},{4,0},{6,2},{1,5},{3,7},{5,1},{7,3},{8,12},{10,14},{12... | collective-permute-start | bytes 786440 | tf_op jit(solution)/shard_map/ppermute | solution.py:362
  16.2 1.0 copy-start.3
  16.2 1.2 copy-start.4
  16.2 16.3 %collective-permute-start.5 = (bf16[128,1024]{1,0:T(8,128)(2,1)S(1)}, bf16[128,1024]{1,0:T(8,128)(2,1)S(1)}, u32[]{:S(2)}, u32[]{:S(2)}) collective-permute-start(bf16[128,1024]{1,0:T(8,128)(2,1)S(1)} %get-tuple-element.41), channel_id=1, source_target_pairs={{0,2},{2,4},{4,6},{6,0},{1,3},{3,5},{5,7},{7,1},{8,10},{10,12},{12... | collective-permute-start | bytes 786440 | tf_op jit(solution)/shard_map/ppermute | solution.py:362
  17.4 15.1 %copy-start.8 = (bf16[2,64,512]{2,1,0:T(8,128)(2,1)S(1)}, bf16[2,64,512]{2,1,0:T(8,128)(2,1)}, u32[]{:S(2)}) copy-start(bf16[2,64,512]{2,1,0:T(8,128)(2,1)} %param.25) | copy-start | bytes 393220
  17.4 15.1 %copy-start.9 = (bf16[2,64,512]{2,1,0:T(8,128)(2,1)S(1)}, bf16[2,64,512]{2,1,0:T(8,128)(2,1)}, u32[]{:S(2)}) copy-start(bf16[2,64,512]{2,1,0:T(8,128)(2,1)} %param.28) | copy-start | bytes 393220
  18.6 41.0 %collective-permute-start.19 = (bf16[128,1024]{1,0:T(8,128)(2,1)S(1)}, bf16[128,1024]{1,0:T(8,128)(2,1)S(1)}, u32[]{:S(2)}, u32[]{:S(2)}) collective-permute-start(bf16[128,1024]{1,0:T(8,128)(2,1)S(1)} %get-tuple-element.59), channel_id=1, source_target_pairs={{0,6},{2,0},{4,2},{6,4},{1,7},{3,1},{5,3},{7,5},{8,14},{10,8},{12,... | collective-permute-start | bytes 786440 | tf_op jit(solution)/shard_map/ppermute | solution.py:362
  20.5 42.8 %collective-permute-start.20 = (bf16[128,1024]{1,0:T(8,128)(2,1)S(1)}, bf16[128,1024]{1,0:T(8,128)(2,1)S(1)}, u32[]{:S(2)}, u32[]{:S(2)}) collective-permute-start(bf16[128,1024]{1,0:T(8,128)(2,1)S(1)} %get-tuple-element.60), channel_id=1, source_target_pairs={{0,4},{2,6},{4,0},{6,2},{1,5},{3,7},{5,1},{7,3},{8,12},{10,14},{12... | collective-permute-start | bytes 786440 | tf_op jit(solution)/shard_map/ppermute | solution.py:362
  21.5 41.9 %collective-permute-start.21 = (bf16[128,1024]{1,0:T(8,128)(2,1)S(1)}, bf16[128,1024]{1,0:T(8,128)(2,1)S(1)}, u32[]{:S(2)}, u32[]{:S(2)}) collective-permute-start(bf16[128,1024]{1,0:T(8,128)(2,1)S(1)} %get-tuple-element.61), channel_id=1, source_target_pairs={{0,2},{2,4},{4,6},{6,0},{1,3},{3,5},{5,7},{7,1},{8,10},{10,12},{12... | collective-permute-start | bytes 786440 | tf_op jit(solution)/shard_map/ppermute | solution.py:362
  32.5 0.7 copy-start.11
  32.5 0.7 copy-start.10
  46.2 3.2 %collective-permute-start.6 = (bf16[2,128,128]{2,1,0:T(8,128)(2,1)S(1)}, bf16[2,128,128]{2,1,0:T(8,128)(2,1)S(1)}, u32[]{:S(2)}, u32[]{:S(2)}) collective-permute-start(bf16[2,128,128]{2,1,0:T(8,128)(2,1)S(1)} %get-tuple-element.43), channel_id=1, source_target_pairs={{0,8},{8,16},{16,24},{24,0},{1,9},{9,17},{17,25},{25,1},{2,10},{10... | collective-permute-start | bytes 196616 | tf_op jit(solution)/shard_map/ppermute | solution.py:362
  46.3 4.7 %collective-permute-start.7 = (bf16[2,128,128]{2,1,0:T(8,128)(2,1)S(1)}, bf16[2,128,128]{2,1,0:T(8,128)(2,1)S(1)}, u32[]{:S(2)}, u32[]{:S(2)}) collective-permute-start(bf16[2,128,128]{2,1,0:T(8,128)(2,1)S(1)} %get-tuple-element.44), channel_id=1, source_target_pairs={{0,16},{8,24},{16,0},{24,8},{1,17},{9,25},{17,1},{25,9},{2,18},{10... | collective-permute-start | bytes 196616 | tf_op jit(solution)/shard_map/ppermute | solution.py:362
  49.4 4.8 %collective-permute-start.8 = (bf16[2,128,128]{2,1,0:T(8,128)(2,1)S(1)}, bf16[2,128,128]{2,1,0:T(8,128)(2,1)S(1)}, u32[]{:S(2)}, u32[]{:S(2)}) collective-permute-start(bf16[2,128,128]{2,1,0:T(8,128)(2,1)S(1)} %get-tuple-element.45), channel_id=1, source_target_pairs={{0,24},{8,0},{16,8},{24,16},{1,25},{9,1},{17,9},{25,17},{2,26},{10... | collective-permute-start | bytes 196616 | tf_op jit(solution)/shard_map/ppermute | solution.py:362
  54.2 9.2 %copy-start.5 = (bf16[512,512]{1,0:T(8,128)(2,1)S(1)}, bf16[512,512]{1,0:T(8,128)(2,1)}, u32[]{:S(2)}) copy-start(bf16[512,512]{1,0:T(8,128)(2,1)} %w0) | copy-start | bytes 1572868
  55.4 8.9 %collective-permute-start.9 = (bf16[128,128]{1,0:T(8,128)(2,1)S(1)}, bf16[128,128]{1,0:T(8,128)(2,1)S(1)}, u32[]{:S(2)}, u32[]{:S(2)}) collective-permute-start(bf16[128,128]{1,0:T(8,128)(2,1)S(1)} %get-tuple-element.46), channel_id=1, source_target_pairs={{0,32},{32,64},{64,96},{96,128},{128,160},{160,192},{192,224},{224... | collective-permute-start | bytes 98312 | tf_op jit(solution)/shard_map/ppermute | solution.py:362
  56.6 11.8 %collective-permute-start.10 = (bf16[128,128]{1,0:T(8,128)(2,1)S(1)}, bf16[128,128]{1,0:T(8,128)(2,1)S(1)}, u32[]{:S(2)}, u32[]{:S(2)}) collective-permute-start(bf16[128,128]{1,0:T(8,128)(2,1)S(1)} %get-tuple-element.47), channel_id=1, source_target_pairs={{0,64},{32,96},{64,128},{96,160},{128,192},{160,224},{192,0},{224,... | collective-permute-start | bytes 98312 | tf_op jit(solution)/shard_map/ppermute | solution.py:362
  59.6 11.2 %collective-permute-start.11 = (bf16[128,128]{1,0:T(8,128)(2,1)S(1)}, bf16[128,128]{1,0:T(8,128)(2,1)S(1)}, u32[]{:S(2)}, u32[]{:S(2)}) collective-permute-start(bf16[128,128]{1,0:T(8,128)(2,1)S(1)} %get-tuple-element.48), channel_id=1, source_target_pairs={{0,96},{32,128},{64,160},{96,192},{128,224},{160,0},{192,32},{224,... | collective-permute-start | bytes 98312 | tf_op jit(solution)/shard_map/ppermute | solution.py:362
  63.4 28.9 %collective-permute-start.27 = (bf16[512,512]{1,0:T(8,128)(2,1)S(1)}, bf16[512,512]{1,0:T(8,128)(2,1)S(1)}, u32[]{:S(2)}, u32[]{:S(2)}) collective-permute-start(bf16[512,512]{1,0:T(8,128)(2,1)S(1)} %copy-done.5), channel_id=1, source_target_pairs={{0,2},{2,4},{4,6},{6,0},{1,3},{3,5},{5,7},{7,1},{8,10},{10,12},{12... | collective-permute-start | bytes 1572872 | tf_op jit(solution)/shard_map/ppermute | solution.py:362
  63.4 8.2 %collective-permute-start.12 = (bf16[128,128]{1,0:T(8,128)(2,1)S(1)}, bf16[128,128]{1,0:T(8,128)(2,1)S(1)}, u32[]{:S(2)}, u32[]{:S(2)}) collective-permute-start(bf16[128,128]{1,0:T(8,128)(2,1)S(1)} %get-tuple-element.49), channel_id=1, source_target_pairs={{0,128},{32,160},{64,192},{96,224},{128,0},{160,32},{192,64},{224,... | collective-permute-start | bytes 98312 | tf_op jit(solution)/shard_map/ppermute | solution.py:362
  64.3 8.3 %collective-permute-start.13 = (bf16[128,128]{1,0:T(8,128)(2,1)S(1)}, bf16[128,128]{1,0:T(8,128)(2,1)S(1)}, u32[]{:S(2)}, u32[]{:S(2)}) collective-permute-start(bf16[128,128]{1,0:T(8,128)(2,1)S(1)} %get-tuple-element.50), channel_id=1, source_target_pairs={{0,160},{32,192},{64,224},{96,0},{128,32},{160,64},{192,96},{224,1... | collective-permute-start | bytes 98312 | tf_op jit(solution)/shard_map/ppermute | solution.py:362
  68.4 6.1 %collective-permute-start.14 = (bf16[128,128]{1,0:T(8,128)(2,1)S(1)}, bf16[128,128]{1,0:T(8,128)(2,1)S(1)}, u32[]{:S(2)}, u32[]{:S(2)}) collective-permute-start(bf16[128,128]{1,0:T(8,128)(2,1)S(1)} %get-tuple-element.51), channel_id=1, source_target_pairs={{0,192},{32,224},{64,0},{96,32},{128,64},{160,96},{192,128},{224,1... | collective-permute-start | bytes 98312 | tf_op jit(solution)/shard_map/ppermute | solution.py:362
  70.8 3.8 %collective-permute-start.15 = (bf16[128,128]{1,0:T(8,128)(2,1)S(1)}, bf16[128,128]{1,0:T(8,128)(2,1)S(1)}, u32[]{:S(2)}, u32[]{:S(2)}) collective-permute-start(bf16[128,128]{1,0:T(8,128)(2,1)S(1)} %get-tuple-element.52), channel_id=1, source_target_pairs={{0,224},{32,0},{64,32},{96,64},{128,96},{160,128},{192,160},{224,1... | collective-permute-start | bytes 98312 | tf_op jit(solution)/shard_map/ppermute | solution.py:362
  71.7 23.5 %collective-permute-start.28 = (bf16[512,512]{1,0:T(8,128)(2,1)S(1)}, bf16[512,512]{1,0:T(8,128)(2,1)S(1)}, u32[]{:S(2)}, u32[]{:S(2)}) collective-permute-start(bf16[512,512]{1,0:T(8,128)(2,1)S(1)} %copy-done.5), channel_id=1, source_target_pairs={{0,4},{2,6},{4,0},{6,2},{1,5},{3,7},{5,1},{7,3},{8,12},{10,14},{12... | collective-permute-start | bytes 1572872 | tf_op jit(solution)/shard_map/ppermute | solution.py:362
  72.6 28.3 %collective-permute-start.29 = (bf16[512,512]{1,0:T(8,128)(2,1)S(1)}, bf16[512,512]{1,0:T(8,128)(2,1)S(1)}, u32[]{:S(2)}, u32[]{:S(2)}) collective-permute-start(bf16[512,512]{1,0:T(8,128)(2,1)S(1)} %copy-done.5), channel_id=1, source_target_pairs={{0,6},{2,0},{4,2},{6,4},{1,7},{3,1},{5,3},{7,5},{8,14},{10,8},{12,... | collective-permute-start | bytes 1572872 | tf_op jit(solution)/shard_map/ppermute | solution.py:362
  74.6 14.7 %copy-start.6 = (bf16[512,512]{1,0:T(8,128)(2,1)S(1)}, bf16[512,512]{1,0:T(8,128)(2,1)}, u32[]{:S(2)}) copy-start(bf16[512,512]{1,0:T(8,128)(2,1)} %w0.1) | copy-start | bytes 1572868
  77.1 12.2 %collective-permute-start.16 = (bf16[128,128]{1,0:T(8,128)(2,1)S(1)}, bf16[128,128]{1,0:T(8,128)(2,1)S(1)}, u32[]{:S(2)}, u32[]{:S(2)}) collective-permute-start(bf16[128,128]{1,0:T(8,128)(2,1)S(1)} %get-tuple-element.55), channel_id=1, source_target_pairs={{0,8},{8,16},{16,24},{24,0},{1,9},{9,17},{17,25},{25,1},{2,10},{10... | collective-permute-start | bytes 98312 | tf_op jit(solution)/shard_map/ppermute | solution.py:362
  77.7 15.2 %copy-start.16 = (bf16[512]{0:T(512)(128)(2,1)S(1)}, bf16[512]{0:T(512)(128)(2,1)}, u32[]{:S(2)}) copy-start(bf16[512]{0:T(512)(128)(2,1)} %param.32) | copy-start | bytes 3076
  77.7 6.9 %collective-permute-start.25 = (bf16[8,512]{1,0:T(8,128)(2,1)S(1)}, bf16[8,512]{1,0:T(8,128)(2,1)S(1)}, u32[]{:S(2)}, u32[]{:S(2)}) collective-permute-start(bf16[8,512]{1,0:T(8,128)(2,1)S(1)} %get-tuple-element.78), channel_id=1, source_target_pairs={{8,0},{16,8},{24,16},{32,24},{40,32},{48,40},{56,48},{64,56},{72,6... | collective-permute-start | bytes 24584 | tf_op jit(solution)/shard_map/ppermute | solution.py:448
  84.6 4.7 %collective-permute-start.26 = (bf16[8,512]{1,0:T(8,128)(2,1)S(1)}, bf16[8,512]{1,0:T(8,128)(2,1)S(1)}, u32[]{:S(2)}, u32[]{:S(2)}) collective-permute-start(bf16[8,512]{1,0:T(8,128)(2,1)S(1)} %get-tuple-element.77), channel_id=1, source_target_pairs={{0,8},{8,16},{16,24},{24,32},{32,40},{40,48},{48,56},{56,64},{64,7... | collective-permute-start | bytes 24584 | tf_op jit(solution)/shard_map/ppermute | solution.py:447
  89.3 15.9 %collective-permute-start.22 = (bf16[512,512]{1,0:T(8,128)(2,1)S(1)}, bf16[512,512]{1,0:T(8,128)(2,1)S(1)}, u32[]{:S(2)}, u32[]{:S(2)}) collective-permute-start(bf16[512,512]{1,0:T(8,128)(2,1)S(1)} %copy-done.6), channel_id=1, source_target_pairs={{0,2},{2,4},{4,6},{6,0},{1,3},{3,5},{5,7},{7,1},{8,10},{10,12},{12... | collective-permute-start | bytes 1572872 | tf_op jit(solution)/shard_map/ppermute | solution.py:362
  89.3 17.7 %collective-permute-start.23 = (bf16[512,512]{1,0:T(8,128)(2,1)S(1)}, bf16[512,512]{1,0:T(8,128)(2,1)S(1)}, u32[]{:S(2)}, u32[]{:S(2)}) collective-permute-start(bf16[512,512]{1,0:T(8,128)(2,1)S(1)} %copy-done.6), channel_id=1, source_target_pairs={{0,4},{2,6},{4,0},{6,2},{1,5},{3,7},{5,1},{7,3},{8,12},{10,14},{12... | collective-permute-start | bytes 1572872 | tf_op jit(solution)/shard_map/ppermute | solution.py:362
  92.3 27.2 %collective-permute-start.24 = (bf16[512,512]{1,0:T(8,128)(2,1)S(1)}, bf16[512,512]{1,0:T(8,128)(2,1)S(1)}, u32[]{:S(2)}, u32[]{:S(2)}) collective-permute-start(bf16[512,512]{1,0:T(8,128)(2,1)S(1)} %copy-done.6), channel_id=1, source_target_pairs={{0,6},{2,0},{4,2},{6,4},{1,7},{3,1},{5,3},{7,5},{8,14},{10,8},{12,... | collective-permute-start | bytes 1572872 | tf_op jit(solution)/shard_map/ppermute | solution.py:362
  92.9 8.9 %copy-start.7 = (bf16[2,256,256]{2,1,0:T(8,128)(2,1)S(1)}, bf16[2,256,256]{2,1,0:T(8,128)(2,1)}, u32[]{:S(2)}) copy-start(bf16[2,256,256]{2,1,0:T(8,128)(2,1)} %mix.1) | copy-start | bytes 786436
  95.1 8.1 %collective-permute-start.17 = (bf16[128,128]{1,0:T(8,128)(2,1)S(1)}, bf16[128,128]{1,0:T(8,128)(2,1)S(1)}, u32[]{:S(2)}, u32[]{:S(2)}) collective-permute-start(bf16[128,128]{1,0:T(8,128)(2,1)S(1)} %get-tuple-element.56), channel_id=1, source_target_pairs={{0,16},{8,24},{16,0},{24,8},{1,17},{9,25},{17,1},{25,9},{2,18},{10... | collective-permute-start | bytes 98312 | tf_op jit(solution)/shard_map/ppermute | solution.py:362
  100.9 4.3 %collective-permute-start.18 = (bf16[128,128]{1,0:T(8,128)(2,1)S(1)}, bf16[128,128]{1,0:T(8,128)(2,1)S(1)}, u32[]{:S(2)}, u32[]{:S(2)}) collective-permute-start(bf16[128,128]{1,0:T(8,128)(2,1)S(1)} %get-tuple-element.57), channel_id=1, source_target_pairs={{0,24},{8,0},{16,8},{24,16},{1,25},{9,1},{17,9},{25,17},{2,26},{10... | collective-permute-start | bytes 98312 | tf_op jit(solution)/shard_map/ppermute | solution.py:362
  122.4 3.2 %collective-permute-start.30 = (bf16[64,2048]{1,0:T(8,128)(2,1)S(1)}, bf16[64,2048]{1,0:T(8,128)(2,1)S(1)}, u32[]{:S(2)}, u32[]{:S(2)}) collective-permute-start(bf16[64,2048]{1,0:T(8,128)(2,1)S(1)} %get-tuple-element.70), channel_id=1, source_target_pairs={{0,1},{1,0},{2,3},{3,2},{4,5},{5,4},{6,7},{7,6},{8,9},{9,8},{10,11... | collective-permute-start | bytes 786440 | tf_op jit(solution)/shard_map/ppermute | solution.py:487

commit v2 on v1

v2 whole, which is shorter than its diff:
```python
import jax
import jax.numpy as jnp
from jax import lax
from jax.experimental import pallas as pl
from jax.experimental.pallas import tpu as pltpu
from jax.sharding import Mesh
from jax.sharding import PartitionSpec as P

SP = ("sp_0", "sp_1")
SP_TP = ("sp_0", "sp_1", "tp")
N_FS, N_X, N_Z = 4, 4, 8
TOK = 128
BLK = 32
N_BLK = TOK // BLK
PAIRS = 4
REACH = 8
LEFT, LEAD, TAIL, OWN = 4, 5, 6, 7

norm_eps = 1e-06
head_eps = 0.00064
unit_eps = 1e-06
half_root = 0.6065306597126334
cap = 80.0

f32 = jnp.float32
bf16 = jnp.bfloat16
highest = lax.Precision.HIGHEST


def in_hbm(array):
    return pltpu.with_memory_space_constraint(array, pltpu.HBM)


def call(body, outs, scratch=(), far=0, same=None):
    def run(scal, *arrays):
        count = len(arrays) - far + len(outs)

        def fetched(at, *refs):
            source, near, held = refs[:far], refs[far : far + count], refs[far + count :]
            buffers, sems, rest = held[:far], held[far], held[far + 1 :]
            copies = [
                pltpu.make_async_copy(a, b, sems.at[k])
                for k, (a, b) in enumerate(zip(source, buffers))
            ]
            for copy in copies:
                copy.start()
            for copy in copies:
                copy.wait()
            body(at, *buffers, *near, *rest)

        extra = []
        if far:
            extra = [pltpu.VMEM(a.shape, a.dtype) for a in arrays[:far]]
            extra.append(pltpu.SemaphoreType.DMA((far,)))
        return pl.pallas_call(
            fetched if far else body,
            out_shape=[jax.ShapeDtypeStruct(s, d) for s, d in outs],
            in_specs=[pl.BlockSpec(memory_space=pltpu.SMEM)]
            + [pl.BlockSpec(memory_space=pltpu.HBM)] * far
            + [pl.BlockSpec(memory_space=pltpu.VMEM)] * (len(arrays) - far),
            out_specs=[pl.BlockSpec(memory_space=pltpu.VMEM)] * len(outs),
            scratch_shapes=extra + list(scratch),
            input_output_aliases=same or {},
            compiler_params=pltpu.CompilerParams(vmem_limit_bytes=20 << 20),
            cost_estimate=pl.CostEstimate(flops=1, transcendentals=0, bytes_accessed=1),
        )(scal, *[in_hbm(a) for a in arrays[:far]], *arrays[far:])

    return run


def seat(scal, axis):
    return scal[("sp_1", "sp_0", "fs", "tp").index(axis)]


def stage_body(scal, *refs):
    count = len(refs) // 2
    sems = refs[-1]
    copies = [pltpu.make_async_copy(refs[k], refs[count + k], sems.at[k]) for k in range(count)]
    for copy in copies:
        copy.start()
    for copy in copies:
        copy.wait()


def stage(scal, *arrays):
    return pl.pallas_call(
        stage_body,
        out_shape=[jax.ShapeDtypeStruct(a.shape, a.dtype) for a in arrays],
        in_specs=[pl.BlockSpec(memory_space=pltpu.SMEM)]
        + [pl.BlockSpec(memory_space=pltpu.HBM)] * len(arrays),
        out_specs=[pl.BlockSpec(memory_space=pltpu.VMEM)] * len(arrays),
        scratch_shapes=[pltpu.SemaphoreType.DMA((len(arrays),))],
        compiler_params=pltpu.CompilerParams(vmem_limit_bytes=4 << 20),
        name="stage",
    )(scal, *[in_hbm(a) for a in arrays])


def cut_body(scal, tokens, *refs):
    outs, sems = refs[:4], refs[4]
    copies = []
    for s, out in enumerate(outs):
        at = pl.multiple_of(((seat(scal, "fs") + s) & 3) * 512, 512)
        copies.append(pltpu.make_async_copy(tokens.at[:, pl.ds(at, 512)], out, sems.at[s]))
        copies[-1].start()
    for copy in copies:
        copy.wait()


def dot(a, b):
    return jnp.dot(a, b, preferred_element_type=f32)


def dot_t(a, b):
    return lax.dot_general(a, b, (((1,), (1,)), ((), ())), preferred_element_type=f32)


def dot_0(a, b):
    return lax.dot_general(a, b, (((0,), (0,)), ((), ())), preferred_element_type=f32)


def iota2(shape):
    return (
        lax.broadcasted_iota(jnp.int32, shape, 0),
        lax.broadcasted_iota(jnp.int32, shape, 1),
    )


def roll64(a):
    return pltpu.roll(a, 64, axis=1)


def summed(own, parts, cols, scale):
    r1, r2, r3 = parts
    got = own + r1[:, cols].astype(f32)
    got = got + r2[:, cols].astype(f32) + r3[:, cols].astype(f32)
    return (got * scale).astype(bf16).astype(f32)


def head_sum(a):
    row, lane = iota2((128, 128))
    same = jnp.where((row // 64) == (lane // 64), 1.0, 0.0).astype(f32)
    return jnp.dot(a, same, precision=highest, preferred_element_type=f32)


def mid_rows(way):
    return [i * BLK + (BLK // 2 - 1 if way == 0 else BLK // 2) for i in range(N_BLK)]


def both_heads(block, lane):
    zero = jnp.zeros_like(block)
    low = lane < 64
    return jnp.concatenate(
        [jnp.where(low, block, zero), jnp.where(low, zero, block)], axis=0
    ).astype(bf16)


def gather_rows(scal, gain, parts):
    at = pl.multiple_of(seat(scal, "fs") * 512, 512)
    rows = jnp.concatenate([part[...] for part in parts], axis=0).astype(f32)
    return (rows * gain[:, pl.ds(at, 512)].astype(f32)).astype(bf16)


def put_parts(got, outs, cols):
    for s in (1, 2, 3):
        outs[s - 1][:, cols] = got[s * TOK : (s + 1) * TOK].astype(bf16)


def project_qp_body(scal, gain, w1, w2, a0, a1, a2, a3, own, *outs):
    rows = gather_rows(scal, gain, (a0, a1, a2, a3))
    for half, w in enumerate((w1, w2)):
        cols = slice(half * 512, (half + 1) * 512)
        got = dot(rows, w[...])
        own[:, cols] = got[:TOK]
        put_parts(got, outs, cols)


def project_kv_body(scal, gain, w1, w2, a0, a1, a2, a3, *outs):
    rows = gather_rows(scal, gain, (a0, a1, a2, a3))
    for half, w in enumerate((w1, w2)):
        put_parts(dot(rows, w[...]), outs, slice(half * 512, (half + 1) * 512))


def decay_body(
    scal,
    tokens, gain, dlow, rlow, draise, dbias, rraise, rbias, tempo_in, sudden_in, wk, wv, mine,
    inv_out, reach_out, out,
):
    rows = gather_rows(scal, gain, (mine,))
    for half, w in enumerate((wk, wv)):
        got = dot(rows, w[...])
        for pair in range(PAIRS):
            out[half * PAIRS + pair, OWN] = got[:, pair * 128 : (pair + 1) * 128].astype(bf16)
    row, lane = iota2((TOK, TOK))
    low = lane < 64
    tempo = tempo_in[...].T
    sudden = sudden_in[...].T
    wide = tokens[...].astype(f32)
    inv = lax.rsqrt(jnp.mean(wide * wide, axis=-1, keepdims=True) + norm_eps)
    inv_out[...] = inv
    normed = (wide * inv * gain[...].astype(f32)).astype(bf16)
    act = jnp.tanh(dot(normed, dlow[...]).astype(bf16).astype(f32)).astype(bf16)
    lat = dot(normed, rlow[...]).astype(bf16)
    for way in range(2):
        mine = (lane // 64) == way
        act_w = jnp.where(mine, act, jnp.zeros_like(act))
        lat_w = jnp.where(mine, lat, jnp.zeros_like(lat))
        tri = jnp.where((row >= lane) if way == 0 else (row <= lane), 1.0, 0.0).astype(f32)
        for pair in range(PAIRS):
            cols = slice(pair * 128, (pair + 1) * 128)
            chain = way * PAIRS + pair
            pre = dbias[way : way + 1, cols] + dot(act_w, draise[:, cols])
            rate = jax.nn.sigmoid(rbias[way : way + 1, cols] + dot(lat_w, rraise[:, cols]))
            at = way * 8 + pair * 2
            pace = jnp.where(low, tempo[:, at : at + 1], tempo[:, at + 1 : at + 2])
            jump = jnp.where(low, sudden[:, at : at + 1], sudden[:, at + 1 : at + 2])
            g = -half_root * jax.nn.sigmoid(pre) * pace + jump
            reach = jnp.dot(tri, g, precision=highest, preferred_element_type=f32)
            reach_out[way, :, cols] = reach
            before = reach - g
            out[chain, LEAD] = jnp.exp(before).astype(bf16)
            for i, mid_row in enumerate(mid_rows(way)):
                mid = reach[mid_row : mid_row + 1, :]
                rows = slice(i * BLK, (i + 1) * BLK)
                out[chain, LEFT, rows] = jnp.exp(before[rows] - mid).astype(bf16)
                out[chain, i] = (rate * jnp.exp(jnp.minimum(mid - reach, cap))).astype(bf16)
            end = reach[TOK - 1 :, :] if way == 0 else reach[:1, :]
            out[chain, TAIL] = (rate * jnp.exp(end - reach)).astype(bf16)


def maps_body(
    scal,
    r1, r2, r3, inv, factors, reach,
    o0, o1, o2, o3, right_out, xy_out, solved, links, inner, ahead_out, tail_out, strong_out, maps,
):
    here = seat(scal, "sp_1")
    row, lane = iota2((TOK, TOK))
    low = lane < 64
    wide_low = (lax.broadcasted_iota(jnp.int32, (TOK, 256), 1) % 128) < 64
    eye = row == lane
    eye_bf = jnp.where(row == lane, 1.0, 0.0).astype(bf16)
    level_masks = []
    for level in range(7):
        size = 2**level
        hit = ((row // (2 * size)) == (lane // (2 * size))) & ((row // size) != (lane // size))
        level_masks.append(jnp.where(hit, 1.0, 0.0).astype(bf16))
    scale = inv[...]
    for pair in range(PAIRS):
        c = slice(pair * 128, (pair + 1) * 128)
        v = slice(512 + pair * 128, 512 + (pair + 1) * 128)
        key = summed(factors[pair, OWN].astype(f32), (r1, r2, r3), c, scale)
        square = head_sum(key * key) + unit_eps
        inverse = lax.rsqrt(square)
        unit = key * inverse
        val = summed(factors[PAIRS + pair, OWN].astype(f32), (r1, r2, r3), v, scale)
        strong_out[pair] = (val * (square * inverse)).astype(bf16)
        for way in range(2):
            chain = way * PAIRS + pair
            pieces = []
            for i in range(N_BLK):
                rows = slice(i * BLK, (i + 1) * BLK)
                side = (unit * factors[chain, i].astype(f32)).astype(bf16)
                right_out[chain, i] = side
                pieces.append(
                    dot_t(both_heads(unit[rows] * factors[chain, LEFT, rows].astype(f32), lane[:BLK]), side)
                )
            strict = (row > lane) if way == 0 else (row < lane)
            for head in range(2):
                link = jnp.concatenate(
                    [piece[head * BLK : (head + 1) * BLK] for piece in pieces], axis=0
                )
                link = jnp.where(strict, link, 0.0).astype(bf16)
                links[2 * chain + head] = link
                solved[2 * chain + head] = eye_bf - link * level_masks[0]
            ahead_out[chain] = (unit * factors[chain, LEAD].astype(f32)).astype(bf16)
            tail_out[chain] = (unit * factors[chain, TAIL].astype(f32)).astype(bf16)
    for level in range(1, 7):
        for k in range(16):
            inner[k] = dot(links[k] * level_masks[level], solved[k]).astype(bf16)
        for k in range(16):
            solved[k] = solved[k] - dot(solved[k], inner[k]).astype(bf16)
    for pair in range(PAIRS):
        c = slice(pair * 128, (pair + 1) * 128)
        for way in range(2):
            chain = way * PAIRS + pair
            side = jnp.concatenate([strong_out[pair], ahead_out[chain]], axis=1)
            first = dot(solved[2 * chain], side)
            second = dot(solved[2 * chain + 1], side)
            xy = jnp.where(wide_low, first, second).astype(bf16)
            xy_out[chain] = xy
            got = dot_0(tail_out[chain], xy)
            carry = got[:, :128]
            end = reach[way, TOK - 1 :, c] if way == 0 else reach[way, :1, c]
            turn = jnp.where(eye, jnp.exp(end) - 1.0, 0.0) - got[:, 128:]
            maps[pair, way] = jnp.where(
                row < 64,
                jnp.where(low, carry, roll64(turn)),
                jnp.where(low, roll64(carry), turn),
            ).astype(bf16)
    for s, out in enumerate((o0, o1, o2, o3)):
        out[...] = maps[(here + s) & 3]


def read_body(scal, own, r1, r2, r3, inv, right, reach_in, xy_in, qeff, local):
    row, lane = iota2((TOK, TOK))
    wide_low = (lax.broadcasted_iota(jnp.int32, (TOK, 256), 1) % 128) < 64
    scale = inv[...]
    for pair in range(PAIRS):
        c = slice(pair * 128, (pair + 1) * 128)
        query = summed(own[:, c], (r1, r2, r3), c, scale)
        base = None
        for way in range(2):
            reach = reach_in[way, :, c]
            pieces = []
            for i, mid_row in enumerate(mid_rows(way)):
                mid = reach[mid_row : mid_row + 1, :]
                rows = slice(i * BLK, (i + 1) * BLK)
                left = query[rows] * jnp.exp(reach[rows] - mid)
                pieces.append(
                    dot_t(both_heads(left, lane[:BLK]), right[way * PAIRS + pair, i])
                )
            within = (row >= lane) if way == 0 else (row <= lane)
            xy = xy_in[way * PAIRS + pair]
            pulls = []
            for head in range(2):
                link = jnp.concatenate(
                    [piece[head * BLK : (head + 1) * BLK] for piece in pieces], axis=0
                )
                pulls.append(dot(jnp.where(within, link, 0.0).astype(bf16), xy))
            pull = jnp.where(wide_low, pulls[0], pulls[1])
            base = pull[:, :128] if base is None else base + pull[:, :128]
            qeff[pair, :, way * 128 : (way + 1) * 128] = (
                query * jnp.exp(reach) - pull[:, 128:]
            ).astype(bf16)
        local[:, c] = base


def spread(packed, row, lane):
    moved = roll64(packed)
    return jnp.where(
        row < 64,
        jnp.where(lane < 64, moved, 0.0),
        jnp.where(lane < 64, 0.0, packed),
    ).astype(bf16)


def compose(state, packed, row, lane):
    return (
        state
        + dot(spread(packed, row, lane), state.astype(bf16))
        + jnp.where(lane < 64, packed, 0.0)
    )


def chain_body(scal, a0, a1, a2, a3, send, before, maps):
    here = seat(scal, "sp_1")
    row, lane = iota2((TOK, TOK))
    ident = jnp.where((lane - 64) == (row % 64), 1.0, 0.0).astype(f32)
    for s, a in enumerate((a0, a1, a2, a3)):
        maps[s] = a[...]
    for way in range(2):
        state = ident
        for step in range(N_X):
            at = step if way == 0 else N_X - 1 - step
            got = maps[(here - at) & 3, way].astype(f32)
            state = got + ident if step == 0 else compose(state, got, row, lane)
            if step < N_X - 1:
                before[step, way] = (state - ident).astype(bf16)
        send[way] = (state - ident).astype(bf16)


def group_body(scal, a0, a1, a2, a3, send, mine, maps):
    level = seat(scal, "sp_0")
    spot = level & 3
    row, lane = iota2((TOK, TOK))
    ident = jnp.where((lane - 64) == (row % 64), 1.0, 0.0).astype(f32)
    for s, a in enumerate((a0, a1, a2, a3)):
        maps[s] = a[...]
    totals = []
    for way in range(2):
        state = ident
        kept = ident
        for step in range(4):
            at = step if way == 0 else 3 - step
            kept = jnp.where(spot == at, state, kept)
            got = maps[(spot - at) & 3, way].astype(f32)
            state = got + ident if step == 0 else compose(state, got, row, lane)
        mine[way] = kept - ident
        totals.append(state)
    send[...] = jnp.where(level < 4, totals[0], totals[1]).astype(bf16)


def enter_body(scal, taken, mine, before, o0, o1, o2, o3, states):
    here, level = seat(scal, "sp_1"), seat(scal, "sp_0")
    row, lane = iota2((TOK, TOK))
    low = lane < 64
    other = jnp.where(low, taken[...].astype(f32), 0.0)
    enter = []
    for way in range(2):
        started = (level >= 4) if way == 0 else (level < 4)
        enter.append(compose(jnp.where(started, other, 0.0), mine[way], row, lane))
    for at in range(N_X):
        f, b = enter
        if at > 0:
            f = compose(f, before[at - 1, 0].astype(f32), row, lane)
        if at < N_X - 1:
            b = compose(b, before[N_X - 2 - at, 1].astype(f32), row, lane)
        states[at] = jnp.where(low, f, roll64(b)).astype(bf16)
    for s, out in enumerate((o0, o1, o2, o3)):
        out[...] = states[(here + s) & 3]


def final_body(
    scal, hgain, wa0, wp0, z0, z1, z2, z3, qeff, local, wa1, wp1, wa2, wp2, wa3, wp3, pool,
    keep, give, states, total,
):
    here, seq, core = seat(scal, "sp_1"), seat(scal, "fs"), seat(scal, "tp")
    row, lane = iota2((TOK, TOK))
    low = lane < 64
    top = row < 64
    for s, z in enumerate((z0, z1, z2, z3)):
        states[s] = z[...]
    cols = []
    for pair in range(PAIRS):
        c = slice(pair * 128, (pair + 1) * 128)
        packed = states[(here - pair) & 3].astype(f32)
        moved = roll64(packed)
        ahead = jnp.where(top, jnp.where(low, packed, 0.0), jnp.where(low, 0.0, moved))
        behind = jnp.where(top, jnp.where(low, moved, 0.0), jnp.where(low, 0.0, packed))
        block = jnp.concatenate([ahead, behind], axis=0).astype(bf16)
        read = dot(qeff[pair], block) + local[:, c]
        centred = read - head_sum(read) * (1.0 / 64.0)
        var = head_sum(centred * centred) * (1.0 / 64.0)
        cols.append(
            (centred * lax.rsqrt(var + head_eps) * hgain[:, c].astype(f32)).astype(bf16)
        )
    attn = jnp.concatenate(cols, axis=1)
    pooled = pool[...]
    weights = (
        (wa0[...], wp0[...]),
        (wa1[...], wp1[...]),
        (wa2[...], wp2[...]),
        (wa3[...], wp3[...]),
    )
    for s, (wa, wp) in enumerate(weights):
        at = pl.multiple_of(((seq - s) & 3) * 512, 512)
        total[:, pl.ds(at, 512)] = dot_t(attn, wa) + dot_t(pooled, wp)
    mine = pl.multiple_of(core * 64, 64)
    other = pl.multiple_of((1 - core) * 64, 64)
    keep[...] = total[pl.ds(mine, 64), :]
    give[...] = total[pl.ds(other, 64), :].astype(bf16)


def pool_body(scal, mix, pool_in, head, tail, out):
    core, span = seat(scal, "tp"), seat(scal, "sp_0") * N_X + seat(scal, "sp_1")
    here = pool_in[...].astype(f32)
    cells = jnp.concatenate([tail[...].astype(f32), here, head[...].astype(f32)], axis=0)
    spot = lax.broadcasted_iota(jnp.int32, (TOK, 256), 0) + span * TOK
    length = TOK * N_X * N_Z
    sums = []
    running = cells
    for level in range(4):
        shift = 2**level
        size = running.shape[0]
        running = running[: size - shift] + running[shift:]
        sums.append(running[REACH - shift : REACH - shift + TOK])
    for member in range(2):
        c = slice(member * 256, (member + 1) * 256)
        upper = core == 1
        chosen = jnp.where(upper, sums[member + 2][:, c], sums[member][:, c])
        half = jnp.where(upper, 2 ** (member + 2), 2**member)
        count = (jnp.minimum(spot + half, length) - jnp.maximum(spot - half, 0)).astype(f32)
        diff = (chosen / count - here[:, c]).astype(bf16)
        out[:, c] = dot(diff, mix[member]).astype(bf16)


def shift_by(a, axis, s, n):
    return lax.ppermute(a, axis, [(i, (i + s) % n) for i in range(n)])


def shards(
    inputs,
    input_norm_gain,
    receptance_matrix,
    key_matrix,
    value_matrix,
    pooling_input_weight,
    decay_lower_matrix,
    decay_raise_matrix,
    decay_offset_bias,
    removal_lower_matrix,
    removal_raise_matrix,
    removal_rate_bias,
    tempo_scale,
    sudden_decay_extra,
    head_norm_gain,
    group_mixing_weight,
    attention_output_matrix,
    pooling_output_matrix,
):
    scal = jnp.stack([lax.axis_index(a) for a in ("sp_1", "sp_0", "fs", "tp")]).astype(jnp.int32)
    return step(
        scal, inputs[0], input_norm_gain.reshape(1, 2048),
        receptance_matrix, key_matrix, value_matrix, pooling_input_weight,
        decay_lower_matrix, decay_raise_matrix.reshape(128, 512), decay_offset_bias,
        removal_lower_matrix, removal_raise_matrix.reshape(128, 512), removal_rate_bias,
        tempo_scale[0].reshape(16, TOK), sudden_decay_extra[0].reshape(16, TOK),
        head_norm_gain.reshape(1, 512), group_mixing_weight,
        attention_output_matrix, pooling_output_matrix,
    )


def step(
    scal, tokens, gain, wq, wk, wv, wp, dlow, draise, dbias, rlow, rraise, rbias,
    tempo, sudden, hgain, mix, attn_own, pool_own,
):
    rows = pl.pallas_call(
        cut_body,
        out_shape=[jax.ShapeDtypeStruct((TOK, 512), bf16)] * 4,
        in_specs=[pl.BlockSpec(memory_space=pltpu.SMEM), pl.BlockSpec(memory_space=pltpu.HBM)],
        out_specs=[pl.BlockSpec(memory_space=pltpu.VMEM)] * 4,
        scratch_shapes=[pltpu.SemaphoreType.DMA((4,))],
        compiler_params=pltpu.CompilerParams(vmem_limit_bytes=4 << 20),
        name="cut",
    )(scal, in_hbm(tokens))
    rows = list(rows)
    for s in (2, 1, 3):
        rows[s] = shift_by(rows[s], "fs", s, N_FS)
    square = (TOK, TOK)
    wk_near, wv_near, gain_near = stage(scal, wk, wv, gain)

    def give_back(got):
        back = [None] * 3
        for s in (2, 1, 3):
            back[s - 1] = shift_by(got[s - 1], "fs", N_FS - s, N_FS)
        return back

    parts = [((TOK, 1024), bf16)] * 3
    got = call(project_kv_body, parts)(
        scal, gain_near, wk_near, wv_near, *rows
    )
    kv = give_back(got)
    own_qp, *got = call(project_qp_body, [((TOK, 1024), f32)] + parts)(
        scal, gain_near, wq, wp, *rows
    )
    qp = [own_qp] + give_back(got)

    attn_w = [attn_own] + [None] * 3
    pool_w = [pool_own] + [None] * 3
    for s in (1, 3):
        attn_w[s] = shift_by(attn_own, "fs", s, N_FS)
        pool_w[s] = shift_by(pool_own, "fs", s, N_FS)
    attn_w[2] = shift_by(attn_w[1], "fs", 1, N_FS)
    pool_w[2] = shift_by(pool_w[3], "fs", 3, N_FS)

    inv, reach, factors = call(
        decay_body, [((TOK, 1), f32), ((2, TOK, 512), f32), ((8, 8, *square), bf16)], far=12
    )(
        scal, tokens, gain, dlow, rlow, draise, dbias, rraise, rbias, tempo, sudden, wk, wv, rows[0]
    )
    outs = call(
        maps_body,
        [((2, *square), bf16)] * 4 + [((8, N_BLK, *square), bf16), ((8, TOK, 256), bf16)],
        scratch=[pltpu.VMEM((16, *square), bf16)] * 3
        + [pltpu.VMEM((8, *square), bf16)] * 2
        + [pltpu.VMEM((PAIRS, *square), bf16), pltpu.VMEM((PAIRS, 2, *square), bf16)],
    )(scal, *kv, inv, factors, reach)
    maps, (right, xy) = outs[:4], outs[4:]
    got = [maps[0]]
    got += [shift_by(maps[s], "sp_1", s, N_X) for s in (1, 2, 3)]

    pool_sum = qp[0][:, 512:]
    for s in (1, 2, 3):
        pool_sum = pool_sum + qp[s][:, 512:].astype(f32)
    pool_in = (pool_sum * inv).astype(bf16)
    n_sp = N_X * N_Z
    below = lax.ppermute(pool_in[TOK - REACH :], SP, [(i, i + 1) for i in range(n_sp - 1)])
    above = lax.ppermute(pool_in[:REACH], SP, [(i + 1, i) for i in range(n_sp - 1)])

    (pooled,) = call(pool_body, [((TOK, 512), bf16)])(
        scal, mix, pool_in, above, below
    )
    qeff, local = call(
        read_body, [((PAIRS, TOK, 256), bf16), ((TOK, 512), f32)]
    )(scal, *qp, inv, right, reach, xy)

    total, before = call(
        chain_body,
        [((2, *square), bf16), ((3, 2, *square), bf16)],
        scratch=[pltpu.VMEM((N_X, 2, *square), bf16)],
    )(scal, *got)
    near = [total]
    for s in (1, 2, 3):
        pairs = [(i, (i // 4) * 4 + (i + s) % 4) for i in range(N_Z)]
        near.append(lax.ppermute(total, "sp_0", pairs))
    half, mine = call(
        group_body,
        [(square, bf16), ((2, *square), f32)],
        scratch=[pltpu.VMEM((4, 2, *square), bf16)],
    )(scal, *near)
    taken = lax.ppermute(half, "sp_0", [(i, i ^ 4) for i in range(N_Z)])
    states = call(
        enter_body, [(square, bf16)] * 4, scratch=[pltpu.VMEM((N_X, *square), bf16)]
    )(scal, taken, mine, before)
    enter = [states[0]]
    enter += [shift_by(states[s], "sp_1", s, N_X) for s in (1, 2, 3)]

    keep, give = call(
        final_body,
        [((64, 2048), f32), ((64, 2048), bf16)],
        scratch=[pltpu.VMEM((N_X, *square), bf16), pltpu.VMEM((TOK, 2048), f32)],
    )(
        scal, hgain, attn_own, pool_own, *enter, qeff, local,
        attn_w[1], pool_w[1], attn_w[2], pool_w[2], attn_w[3], pool_w[3], pooled,
    )
    taken = lax.ppermute(give, "tp", [(0, 1), (1, 0)])
    return (keep + taken.astype(f32)).astype(bf16)[None]


def solution(mesh):
    split = Mesh(
        mesh.devices.reshape(8, 4, mesh.shape["fs"], mesh.shape["tp"]), ("sp_0", "sp_1", "fs", "tp")
    )
    in_specs = (
        P("fs", SP, None),
        P(),
        P("fs", "tp"),
        P("fs", "tp"),
        P("fs", "tp"),
        P("fs", "tp"),
        P(),
        P(None, None, "tp"),
        P(None, "tp"),
        P(),
        P(None, None, "tp"),
        P(None, "tp"),
        P("fs", None, "tp", SP),
        P("fs", None, "tp", SP),
        P("tp"),
        P("tp", None, None),
        P("fs", "tp"),
        P("fs", "tp"),
    )
    out_specs = P("fs", SP_TP, None)
    return jax.shard_map(
        shards, mesh=split, in_specs=in_specs, out_specs=out_specs, check_vma=False
    )
```

time: 128 us -> 110 us (0.86)
  the two profiles are of different devices: /device:TPU:7 before, /device:TPU:105 now
where the time goes in v2:
time: 110 us
  starting transfers between devices  47.7 us (43%)
  Pallas kernels  28.4 us (26%)
  waiting for transfers between devices  27.5 us (25%)
  local copies, waits for them, and re-layouts  4.75 us (4%)
    ppermute x21, starting transfers between devices, shift_by(): return lax.ppermute(a, axis, [(i, (i + s) % n) for i in range(n)])  29.1 us
    pallas_call x10, Pallas kernels, run(): pl.pallas_call(fetched if far else body, out_shape=[jax.ShapeDtypeStruct(...  24.9 us
    ppermute x21, waiting for transfers between devices, shift_by(): return lax.ppermute(a, axis, [(i, (i + s) % n) for i in range(n)])  14.6 us
    ppermute x1, starting transfers between devices, step(): taken = lax.ppermute(give, 'tp', [(0, 1), (1, 0)])  8.24 us
    ppermute x3, waiting for transfers between devices, step(): near.append(lax.ppermute(total, 'sp_0', pairs))  7.52 us
    ppermute x1, starting transfers between devices, step(): taken = lax.ppermute(half, 'sp_0', [(i, i ^ 4) for i in range(N_Z)])  4.66 us
    ppermute x1, starting transfers between devices, step(): lax.ppermute(pool_in[TOK - REACH:], SP, [(i, i + 1) for i in range(n_sp -...  3.54 us
    unnamed x18, local copies, waits for them, and re-layouts  3.46 us
  transfers between devices with their start and end apart: 28, of which 12 were waited for; matrix products, arithmetic and copies ran while one was open for 1% of the time, Pallas kernels for 19%

profile of v2, /device:TPU:105, one launch (start us, length us, event | category | flops | bytes accessed | tf_op | source)
XLA Modules:
  0.0 109.7 jit_solution(5853361906426382980)
XLA Ops:
  0.1 1.7 %cut.1 = (bf16[128,512]{1,0:T(8,128)(2,1)S(1)}, bf16[128,512]{1,0:T(8,128)(2,1)S(1)}, bf16[128,512]{1,0:T(8,128)(2,1)S(1)}, bf16[128,512]{1,0:T(8,128)(2,1)S(1)}) custom-call(s32[4]{0:T(128)S(1)} %pad_add_fusion.scal.at, bf16[128,2048]{1,0:T(8,128)(2,1)} %bitcast.11), custom_call_target="tpu_custom_call" | custom-call | tf_op jit(solution)/shard_map/cut/pallas_call | solution.py:516
  1.8 1.4 %collective-permute-start = (bf16[128,512]{1,0:T(8,128)(2,1)S(1)}, bf16[128,512]{1,0:T(8,128)(2,1)S(1)}, u32[]{:S(2)}, u32[]{:S(2)}) collective-permute-start(bf16[128,512]{1,0:T(8,128)(2,1)S(1)} %get-tuple-element.44), channel_id=1, source_target_pairs={{0,2},{2,4},{4,6},{6,0},{1,3},{3,5},{5,7},{7,1},{8,10},{10,12},{12... | collective-permute-start | bytes 393224 | tf_op jit(solution)/shard_map/ppermute | solution.py:477
  3.1 0.8 collective-permute-start.1
  4.0 2.0 %collective-permute-start.2 = (bf16[128,512]{1,0:T(8,128)(2,1)S(1)}, bf16[128,512]{1,0:T(8,128)(2,1)S(1)}, u32[]{:S(2)}, u32[]{:S(2)}) collective-permute-start(bf16[128,512]{1,0:T(8,128)(2,1)S(1)} %get-tuple-element.46), channel_id=1, source_target_pairs={{0,6},{2,0},{4,2},{6,4},{1,7},{3,1},{5,3},{7,5},{8,14},{10,8},{12,... | collective-permute-start | bytes 393224 | tf_op jit(solution)/shard_map/ppermute | solution.py:477
  5.9 1.3 %reshape.13.refs_2_.refs_1_ = bf16[1,2048]{1,0:T(2,128)(2,1)} reshape(bf16[2048]{0:T(1024)(128)(2,1)} %param.19) | data formatting | bytes 8192 | tf_op jit(solution)/shard_map/reshape | solution.py:502
  7.2 1.8 %stage.1 = (bf16[512,512]{1,0:T(8,128)(2,1)S(1)}, bf16[512,512]{1,0:T(8,128)(2,1)S(1)}, bf16[1,2048]{1,0:T(2,128)(2,1)S(1)}) custom-call(s32[4]{0:T(128)S(1)} %pad_add_fusion.scal.at, bf16[512,512]{1,0:T(8,128)(2,1)} %refs_10_.1, bf16[512,512]{1,0:T(8,128)(2,1)} %refs_11_.1, bf16[1,2048]{1,0:T(2,128)(2,1)} %reshape.13.refs_2_.refs_1_), custom_call_target="tpu_custom_call" | custom-call | tf_op jit(solution)/shard_map/stage/pallas_call | solution.py:86
  9.0 2.4 %collective-permute-done.2.a3 = bf16[128,512]{1,0:T(8,128)(2,1)S(1)} collective-permute-done((bf16[128,512]{1,0:T(8,128)(2,1)S(1)}, bf16[128,512]{1,0:T(8,128)(2,1)S(1)}, u32[]{:S(2)}, u32[]{:S(2)}) %collective-permute-start.2) | collective-permute-done | bytes 131104 | tf_op jit(solution)/shard_map/ppermute | solution.py:477
  11.4 1.2 %shard_map.172 = (bf16[128,1024]{1,0:T(8,128)(2,1)S(1)}, bf16[128,1024]{1,0:T(8,128)(2,1)S(1)}, bf16[128,1024]{1,0:T(8,128)(2,1)S(1)}) custom-call(s32[4]{0:T(128)S(1)} %pad_add_fusion.scal.at, bf16[1,2048]{1,0:T(2,128)(2,1)S(1)} %get-tuple-element.40.gain, bf16[512,512]{1,0:T(8,128)(2,1)S(1)} %get-tuple-element.41.w1, ...), custom_call_target="tpu_custom_call" | custom-call | flops 1 | bytes 1 | tf_op jit(solution)/shard_map/pallas_call | solution.py:55
  13.0 1.4 %collective-permute-start.4 = (bf16[128,1024]{1,0:T(8,128)(2,1)S(1)}, bf16[128,1024]{1,0:T(8,128)(2,1)S(1)}, u32[]{:S(2)}, u32[]{:S(2)}) collective-permute-start(bf16[128,1024]{1,0:T(8,128)(2,1)S(1)} %get-tuple-element.48), channel_id=1, source_target_pairs={{0,4},{2,6},{4,0},{6,2},{1,5},{3,7},{5,1},{7,3},{8,12},{10,14},{12... | collective-permute-start | bytes 786440 | tf_op jit(solution)/shard_map/ppermute | solution.py:477
  14.4 2.0 %collective-permute-start.5 = (bf16[128,1024]{1,0:T(8,128)(2,1)S(1)}, bf16[128,1024]{1,0:T(8,128)(2,1)S(1)}, u32[]{:S(2)}, u32[]{:S(2)}) collective-permute-start(bf16[128,1024]{1,0:T(8,128)(2,1)S(1)} %get-tuple-element.49), channel_id=1, source_target_pairs={{0,2},{2,4},{4,6},{6,0},{1,3},{3,5},{5,7},{7,1},{8,10},{10,12},{12... | collective-permute-start | bytes 786440 | tf_op jit(solution)/shard_map/ppermute | solution.py:477
  16.4 1.4 %collective-permute-start.22 = (bf16[512,512]{1,0:T(8,128)(2,1)}, bf16[512,512]{1,0:T(8,128)(2,1)}, u32[]{:S(2)}, u32[]{:S(2)}) collective-permute-start(bf16[512,512]{1,0:T(8,128)(2,1)} %wp0.1), channel_id=1, source_target_pairs={{0,6},{2,0},{4,2},{6,4},{1,7},{3,1},{5,3},{7,5},{8,14},{10,8},{12,... | collective-permute-start | bytes 1572872 | tf_op jit(solution)/shard_map/ppermute | solution.py:477
  17.9 4.6 %shard_map.173 = (f32[128,1]{1,0:T(8,128)S(1)}, f32[2,128,512]{2,1,0:T(8,128)S(1)}, bf16[8,8,128,128]{3,2,1,0:T(8,128)(2,1)S(1)}) custom-call(s32[4]{0:T(128)S(1)} %pad_add_fusion.scal.at, bf16[128,2048]{1,0:T(8,128)(2,1)} %bitcast.12, bf16[1,2048]{1,0:T(2,128)(2,1)} %reshape.13.refs_2_.refs_1_, bf16[2048,128]{1,0:T(8,128)(2,1)} %refs_2_.1, ...), custom_call_target="tpu_custom_call" | custom-call | flops 1 | bytes 1 | tf_op jit(solution)/shard_map/pallas_call | solution.py:55
  22.5 2.2 %collective-permute-done.4.r2 = bf16[128,1024]{1,0:T(8,128)(2,1)S(1)} collective-permute-done((bf16[128,1024]{1,0:T(8,128)(2,1)S(1)}, bf16[128,1024]{1,0:T(8,128)(2,1)S(1)}, u32[]{:S(2)}, u32[]{:S(2)}) %collective-permute-start.4) | collective-permute-done | bytes 262176 | tf_op jit(solution)/shard_map/ppermute | solution.py:477
  24.7 2.6 %collective-permute-done.5.r3 = bf16[128,1024]{1,0:T(8,128)(2,1)S(1)} collective-permute-done((bf16[128,1024]{1,0:T(8,128)(2,1)S(1)}, bf16[128,1024]{1,0:T(8,128)(2,1)S(1)}, u32[]{:S(2)}, u32[]{:S(2)}) %collective-permute-start.5) | collective-permute-done | bytes 262176 | tf_op jit(solution)/shard_map/ppermute | solution.py:477
  27.4 6.5 %shard_map.174 = (bf16[2,128,128]{2,1,0:T(8,128)(2,1)S(1)}, bf16[2,128,128]{2,1,0:T(8,128)(2,1)S(1)}, bf16[2,128,128]{2,1,0:T(8,128)(2,1)S(1)}, bf16[2,128,128]{...) custom-call(s32[4]{0:T(128)S(1)} %pad_add_fusion.scal.at, ...), custom_call_target="tpu_custom_call" | custom-call | flops 1 | bytes 1 | tf_op jit(solution)/shard_map/pallas_call | solution.py:55
  33.8 0.8 copy-done.3
  34.6 1.2 %collective-permute-start.6 = (bf16[2,128,128]{2,1,0:T(8,128)(2,1)S(1)}, bf16[2,128,128]{2,1,0:T(8,128)(2,1)S(1)}, u32[]{:S(2)}, u32[]{:S(2)}) collective-permute-start(bf16[2,128,128]{2,1,0:T(8,128)(2,1)S(1)} %get-tuple-element.54), channel_id=1, source_target_pairs={{0,8},{8,16},{16,24},{24,0},{1,9},{9,17},{17,25},{25,1},{2,10},{10... | collective-permute-start | bytes 196616 | tf_op jit(solution)/shard_map/ppermute | solution.py:477
  35.9 2.4 %collective-permute-start.7 = (bf16[2,128,128]{2,1,0:T(8,128)(2,1)S(1)}, bf16[2,128,128]{2,1,0:T(8,128)(2,1)S(1)}, u32[]{:S(2)}, u32[]{:S(2)}) collective-permute-start(bf16[2,128,128]{2,1,0:T(8,128)(2,1)S(1)} %get-tuple-element.55), channel_id=1, source_target_pairs={{0,16},{8,24},{16,0},{24,8},{1,17},{9,25},{17,1},{25,9},{2,18},{10... | collective-permute-start | bytes 196616 | tf_op jit(solution)/shard_map/ppermute | solution.py:477
  38.3 1.2 %collective-permute-start.8 = (bf16[2,128,128]{2,1,0:T(8,128)(2,1)S(1)}, bf16[2,128,128]{2,1,0:T(8,128)(2,1)S(1)}, u32[]{:S(2)}, u32[]{:S(2)}) collective-permute-start(bf16[2,128,128]{2,1,0:T(8,128)(2,1)S(1)} %get-tuple-element.56), channel_id=1, source_target_pairs={{0,24},{8,0},{16,8},{24,16},{1,25},{9,1},{17,9},{25,17},{2,26},{10... | collective-permute-start | bytes 196616 | tf_op jit(solution)/shard_map/ppermute | solution.py:477
  39.5 1.2 %shard_map.178 = (f32[128,1024]{1,0:T(8,128)S(1)}, bf16[128,1024]{1,0:T(8,128)(2,1)S(1)}, bf16[128,1024]{1,0:T(8,128)(2,1)S(1)}, bf16[128,1024]{1,0:T(8,128)(2,1)S(1)}) custom-call(s32[4]{0:T(128)S(1)} %pad_add_fusion.scal.at, bf16[1,2048]{1,0:T(2,128)(2,1)S(1)} %get-tuple-element.40.gain, bf16[512,512]{1,0:T(8,128)(2,1)S(1)} %copy-done.1, ...), custom_call_target="tpu_custom_call" | custom-call | flops 1 | bytes 1 | tf_op jit(solution)/shard_map/pallas_call | solution.py:55
  40.7 3.3 %collective-permute-start.16 = (bf16[128,1024]{1,0:T(8,128)(2,1)S(1)}, bf16[128,1024]{1,0:T(8,128)(2,1)S(1)}, u32[]{:S(2)}, u32[]{:S(2)}) collective-permute-start(bf16[128,1024]{1,0:T(8,128)(2,1)S(1)} %get-tuple-element.66), channel_id=1, source_target_pairs={{0,6},{2,0},{4,2},{6,4},{1,7},{3,1},{5,3},{7,5},{8,14},{10,8},{12,... | collective-permute-start | bytes 786440 | tf_op jit(solution)/shard_map/ppermute | solution.py:477
  44.3 1.1 collective-permute-start.18
  45.4 1.2 %shard_map.175 = (bf16[2,128,128]{2,1,0:T(8,128)(2,1)S(1)}, bf16[3,2,128,128]{3,2,1,0:T(8,128)(2,1)S(1)}) custom-call(s32[4]{0:T(128)S(1)} %pad_add_fusion.scal.at, bf16[2,128,128]{2,1,0:T(8,128)(2,1)S(1)} %get-tuple-element.53.a0, bf16[2,128,128]{2,1,0:T(8,128)(2,1)S(1)} %collective-permute-done.6.a1, bf16[2,128,128]{2,1,0:T(8,128)(2,1)S(1)} %collective-permute-done.7.a2, ...), custom_call_target="tpu_custom_call" | custom-call | flops 1 | bytes 1 | tf_op jit(solution)/shard_map/pallas_call | solution.py:55
  46.6 0.7 copy-done.6
  47.3 1.0 collective-permute-done.16.r1
  48.2 5.9 %collective-permute-done.17.r2 = bf16[128,1024]{1,0:T(8,128)(2,1)S(1)} collective-permute-done((bf16[128,1024]{1,0:T(8,128)(2,1)S(1)}, bf16[128,1024]{1,0:T(8,128)(2,1)S(1)}, u32[]{:S(2)}, u32[]{:S(2)}) %collective-permute-start.17) | collective-permute-done | bytes 262176 | tf_op jit(solution)/shard_map/ppermute | solution.py:477
  54.6 3.3 %collective-permute-start.24 = (bf16[512,512]{1,0:T(8,128)(2,1)S(1)}, bf16[512,512]{1,0:T(8,128)(2,1)}, u32[]{:S(2)}, u32[]{:S(2)}) collective-permute-start(bf16[512,512]{1,0:T(8,128)(2,1)S(1)} %copy-done), channel_id=1, source_target_pairs={{0,6},{2,0},{4,2},{6,4},{1,7},{3,1},{5,3},{7,5},{8,14},{10,8},{12,... | collective-permute-start | bytes 1572872 | tf_op jit(solution)/shard_map/ppermute | solution.py:477
  58.2 1.4 %collective-permute-start.23 = (bf16[512,512]{1,0:T(8,128)(2,1)}, bf16[512,512]{1,0:T(8,128)(2,1)S(1)}, u32[]{:S(2)}, u32[]{:S(2)}) collective-permute-start(bf16[512,512]{1,0:T(8,128)(2,1)} %collective-permute-done.22.wp3), channel_id=1, source_target_pairs={{0,6},{2,0},{4,2},{6,4},{1,7},{3,1},{5,3},{7,5},{8,14},{10,8},{12,... | collective-permute-start | bytes 1572872 | tf_op jit(solution)/shard_map/ppermute | solution.py:477
  59.8 2.6 %collective-permute-done.10.a2 = bf16[2,128,128]{2,1,0:T(8,128)(2,1)S(1)} collective-permute-done((bf16[2,128,128]{2,1,0:T(8,128)(2,1)S(1)}, bf16[2,128,128]{2,1,0:T(8,128)(2,1)S(1)}, u32[]{:S(2)}, u32[]{:S(2)}) %collective-permute-start.10) | collective-permute-done | bytes 65568 | tf_op jit(solution)/shard_map/ppermute | solution.py:594
  62.4 4.9 %collective-permute-done.11.a3 = bf16[2,128,128]{2,1,0:T(8,128)(2,1)S(1)} collective-permute-done((bf16[2,128,128]{2,1,0:T(8,128)(2,1)S(1)}, bf16[2,128,128]{2,1,0:T(8,128)(2,1)S(1)}, u32[]{:S(2)}, u32[]{:S(2)}) %collective-permute-start.11) | collective-permute-done | bytes 65568 | tf_op jit(solution)/shard_map/ppermute | solution.py:594
  67.3 2.1 %collective-permute-start.25 = (bf16[8,512]{1,0:T(8,128)(2,1)S(1)}, bf16[8,512]{1,0:T(8,128)(2,1)S(1)}, u32[]{:S(2)}, u32[]{:S(2)}) collective-permute-start(bf16[8,512]{1,0:T(8,128)(2,1)S(1)} %get-tuple-element.76), channel_id=1, source_target_pairs={{8,0},{16,8},{24,16},{32,24},{40,32},{48,40},{56,48},{64,56},{72,6... | collective-permute-start | bytes 24584 | tf_op jit(solution)/shard_map/ppermute | solution.py:577
  69.4 1.5 %shard_map.176 = (bf16[128,128]{1,0:T(8,128)(2,1)S(1)}, f32[2,128,128]{2,1,0:T(8,128)S(1)}) custom-call(s32[4]{0:T(128)S(1)} %pad_add_fusion.scal.at, bf16[2,128,128]{2,1,0:T(8,128)(2,1)S(1)} %get-tuple-element.57.a0, bf16[2,128,128]{2,1,0:T(8,128)(2,1)} %collective-permute-done.9.a1, bf16[2,128,128]{2,1,0:T(8,128)(2,1)S(1)} %collective-permute-done.10.a2, ...), custom_call_target="tpu_custom_call" | custom-call | flops 1 | bytes 1 | tf_op jit(solution)/shard_map/pallas_call | solution.py:55
  70.9 1.2 %collective-permute-done.25.head = bf16[8,512]{1,0:T(8,128)(2,1)S(1)} collective-permute-done((bf16[8,512]{1,0:T(8,128)(2,1)S(1)}, bf16[8,512]{1,0:T(8,128)(2,1)S(1)}, u32[]{:S(2)}, u32[]{:S(2)}) %collective-permute-start.25) | collective-permute-done | bytes 8224 | tf_op jit(solution)/shard_map/ppermute | solution.py:577
  72.1 4.7 %collective-permute-start.12 = (bf16[128,128]{1,0:T(8,128)(2,1)S(1)}, bf16[128,128]{1,0:T(8,128)(2,1)S(1)}, u32[]{:S(2)}, u32[]{:S(2)}) collective-permute-start(bf16[128,128]{1,0:T(8,128)(2,1)S(1)} %get-tuple-element.58), channel_id=1, source_target_pairs={{0,128},{32,160},{64,192},{96,224},{128,0},{160,32},{192,64},{224,... | collective-permute-start | bytes 98312 | tf_op jit(solution)/shard_map/ppermute | solution.py:600
  76.8 2.0 %collective-permute-done.12.taken = bf16[128,128]{1,0:T(8,128)(2,1)S(1)} collective-permute-done((bf16[128,128]{1,0:T(8,128)(2,1)S(1)}, bf16[128,128]{1,0:T(8,128)(2,1)S(1)}, u32[]{:S(2)}, u32[]{:S(2)}) %collective-permute-start.12) | collective-permute-done | bytes 32800 | tf_op jit(solution)/shard_map/ppermute | solution.py:600
  78.8 3.5 %collective-permute-start.26 = (bf16[8,512]{1,0:T(8,128)(2,1)S(1)}, bf16[8,512]{1,0:T(8,128)(2,1)S(1)}, u32[]{:S(2)}, u32[]{:S(2)}) collective-permute-start(bf16[8,512]{1,0:T(8,128)(2,1)S(1)} %get-tuple-element.75), channel_id=1, source_target_pairs={{0,8},{8,16},{16,24},{24,32},{32,40},{40,48},{48,56},{56,64},{64,7... | collective-permute-start | bytes 24584 | tf_op jit(solution)/shard_map/ppermute | solution.py:576
  82.3 0.9 copy-done.7
  83.2 1.0 shard_map.177
  84.3 1.0 collective-permute-done.26.tail
  85.8 3.6 %collective-permute-start.14 = (bf16[128,128]{1,0:T(8,128)(2,1)S(1)}, bf16[128,128]{1,0:T(8,128)(2,1)S(1)}, u32[]{:S(2)}, u32[]{:S(2)}) collective-permute-start(bf16[128,128]{1,0:T(8,128)(2,1)S(1)} %get-tuple-element.63), channel_id=1, source_target_pairs={{0,16},{8,24},{16,0},{24,8},{1,17},{9,25},{17,1},{25,9},{2,18},{10... | collective-permute-start | bytes 98312 | tf_op jit(solution)/shard_map/ppermute | solution.py:477
  89.4 1.3 %collective-permute-start.15 = (bf16[128,128]{1,0:T(8,128)(2,1)S(1)}, bf16[128,128]{1,0:T(8,128)(2,1)S(1)}, u32[]{:S(2)}, u32[]{:S(2)}) collective-permute-start(bf16[128,128]{1,0:T(8,128)(2,1)S(1)} %get-tuple-element.64), channel_id=1, source_target_pairs={{0,24},{8,0},{16,8},{24,16},{1,25},{9,1},{17,9},{25,17},{2,26},{10... | collective-permute-start | bytes 98312 | tf_op jit(solution)/shard_map/ppermute | solution.py:477
  90.8 1.0 copy-done.4
  91.8 2.2 %shard_map.179 = (bf16[4,128,256]{2,1,0:T(8,128)(2,1)S(1)}, f32[128,512]{1,0:T(8,128)S(1)}) custom-call(s32[4]{0:T(128)S(1)} %pad_add_fusion.scal.at, f32[128,1024]{1,0:T(8,128)S(1)} %get-tuple-element.65.own, bf16[128,1024]{1,0:T(8,128)(2,1)S(1)} %collective-permute-done.16.r1, bf16[128,1024]{1,0:T(8,128)(2,1)S(1)} %collective-permute-done.17.r2, ...), custom_call_target="tpu_custom_call" | custom-call | flops 1 | bytes 1 | tf_op jit(solution)/shard_map/pallas_call | solution.py:55
  94.0 0.9 shard_map.180.pool
  95.0 4.6 %shard_map.181 = (f32[64,2048]{1,0:T(8,128)S(1)}, bf16[64,2048]{1,0:T(8,128)(2,1)S(1)}) custom-call(s32[4]{0:T(128)S(1)} %pad_add_fusion.scal.at, bf16[1,512]{1,0:T(2,128)(2,1)S(1)} %reshape.12.hgain, bf16[512,512]{1,0:T(8,128)(2,1)S(1)} %copy-done, bf16[512,512]{1,0:T(8,128)(2,1)} %wp0.1, bf16[128,128]{1,0:T(8,128)(2,1)S(1)} %get-tuple-element.61.z0, ...), custom_call_target="tpu_custom_call" | custom-call | flops 1 | bytes 1 | tf_op jit(solution)/shard_map/pallas_call | solution.py:55
  99.5 8.2 %collective-permute-start.27 = (bf16[64,2048]{1,0:T(8,128)(2,1)S(1)}, bf16[64,2048]{1,0:T(8,128)(2,1)S(1)}, u32[]{:S(2)}, u32[]{:S(2)}) collective-permute-start(bf16[64,2048]{1,0:T(8,128)(2,1)S(1)} %get-tuple-element.74), channel_id=1, source_target_pairs={{0,1},{1,0},{2,3},{3,2},{4,5},{5,4},{6,7},{7,6},{8,9},{9,8},{10,11... | collective-permute-start | bytes 786440 | tf_op jit(solution)/shard_map/ppermute | solution.py:615
  107.8 1.2 %collective-permute-done.27 = bf16[64,2048]{1,0:T(8,128)(2,1)S(1)} collective-permute-done((bf16[64,2048]{1,0:T(8,128)(2,1)S(1)}, bf16[64,2048]{1,0:T(8,128)(2,1)S(1)}, u32[]{:S(2)}, u32[]{:S(2)}) %collective-permute-start.27) | collective-permute-done | bytes 262176 | tf_op jit(solution)/shard_map/ppermute | solution.py:615
  108.9 0.8 fusion
  (45 shorter events, 2.2 us)
Async XLA Ops:
  0.0 16.4 %copy-start = (bf16[512,512]{1,0:T(8,128)(2,1)S(1)}, bf16[512,512]{1,0:T(8,128)(2,1)}, u32[]{:S(2)}) copy-start(bf16[512,512]{1,0:T(8,128)(2,1)} %wa0.1) | copy-start | bytes 1572868
  1.8 7.2 %collective-permute-start = (bf16[128,512]{1,0:T(8,128)(2,1)S(1)}, bf16[128,512]{1,0:T(8,128)(2,1)S(1)}, u32[]{:S(2)}, u32[]{:S(2)}) collective-permute-start(bf16[128,512]{1,0:T(8,128)(2,1)S(1)} %get-tuple-element.44), channel_id=1, source_target_pairs={{0,2},{2,4},{4,6},{6,0},{1,3},{3,5},{5,7},{7,1},{8,10},{10,12},{12... | collective-permute-start | bytes 393224 | tf_op jit(solution)/shard_map/ppermute | solution.py:477
  3.1 5.9 %collective-permute-start.1 = (bf16[128,512]{1,0:T(8,128)(2,1)S(1)}, bf16[128,512]{1,0:T(8,128)(2,1)S(1)}, u32[]{:S(2)}, u32[]{:S(2)}) collective-permute-start(bf16[128,512]{1,0:T(8,128)(2,1)S(1)} %get-tuple-element.45), channel_id=1, source_target_pairs={{0,4},{2,6},{4,0},{6,2},{1,5},{3,7},{5,1},{7,3},{8,12},{10,14},{12... | collective-permute-start | bytes 393224 | tf_op jit(solution)/shard_map/ppermute | solution.py:477
  4.0 7.5 %collective-permute-start.2 = (bf16[128,512]{1,0:T(8,128)(2,1)S(1)}, bf16[128,512]{1,0:T(8,128)(2,1)S(1)}, u32[]{:S(2)}, u32[]{:S(2)}) collective-permute-start(bf16[128,512]{1,0:T(8,128)(2,1)S(1)} %get-tuple-element.46), channel_id=1, source_target_pairs={{0,6},{2,0},{4,2},{6,4},{1,7},{3,1},{5,3},{7,5},{8,14},{10,8},{12,... | collective-permute-start | bytes 393224 | tf_op jit(solution)/shard_map/ppermute | solution.py:477
  12.7 9.8 %collective-permute-start.3 = (bf16[128,1024]{1,0:T(8,128)(2,1)S(1)}, bf16[128,1024]{1,0:T(8,128)(2,1)S(1)}, u32[]{:S(2)}, u32[]{:S(2)}) collective-permute-start(bf16[128,1024]{1,0:T(8,128)(2,1)S(1)} %get-tuple-element.47), channel_id=1, source_target_pairs={{0,6},{2,0},{4,2},{6,4},{1,7},{3,1},{5,3},{7,5},{8,14},{10,8},{12,... | collective-permute-start | bytes 786440 | tf_op jit(solution)/shard_map/ppermute | solution.py:477
  13.0 11.7 %collective-permute-start.4 = (bf16[128,1024]{1,0:T(8,128)(2,1)S(1)}, bf16[128,1024]{1,0:T(8,128)(2,1)S(1)}, u32[]{:S(2)}, u32[]{:S(2)}) collective-permute-start(bf16[128,1024]{1,0:T(8,128)(2,1)S(1)} %get-tuple-element.48), channel_id=1, source_target_pairs={{0,4},{2,6},{4,0},{6,2},{1,5},{3,7},{5,1},{7,3},{8,12},{10,14},{12... | collective-permute-start | bytes 786440 | tf_op jit(solution)/shard_map/ppermute | solution.py:477
  14.4 12.9 %collective-permute-start.5 = (bf16[128,1024]{1,0:T(8,128)(2,1)S(1)}, bf16[128,1024]{1,0:T(8,128)(2,1)S(1)}, u32[]{:S(2)}, u32[]{:S(2)}) collective-permute-start(bf16[128,1024]{1,0:T(8,128)(2,1)S(1)} %get-tuple-element.49), channel_id=1, source_target_pairs={{0,2},{2,4},{4,6},{6,0},{1,3},{3,5},{5,7},{7,1},{8,10},{10,12},{12... | collective-permute-start | bytes 786440 | tf_op jit(solution)/shard_map/ppermute | solution.py:477
  16.4 41.7 %collective-permute-start.19 = (bf16[512,512]{1,0:T(8,128)(2,1)S(1)}, bf16[512,512]{1,0:T(8,128)(2,1)}, u32[]{:S(2)}, u32[]{:S(2)}) collective-permute-start(bf16[512,512]{1,0:T(8,128)(2,1)S(1)} %copy-done), channel_id=1, source_target_pairs={{0,2},{2,4},{4,6},{6,0},{1,3},{3,5},{5,7},{7,1},{8,10},{10,12},{12... | collective-permute-start | bytes 1572872 | tf_op jit(solution)/shard_map/ppermute | solution.py:477
  16.4 41.8 %collective-permute-start.22 = (bf16[512,512]{1,0:T(8,128)(2,1)}, bf16[512,512]{1,0:T(8,128)(2,1)}, u32[]{:S(2)}, u32[]{:S(2)}) collective-permute-start(bf16[512,512]{1,0:T(8,128)(2,1)} %wp0.1), channel_id=1, source_target_pairs={{0,6},{2,0},{4,2},{6,4},{1,7},{3,1},{5,3},{7,5},{8,14},{10,8},{12,... | collective-permute-start | bytes 1572872 | tf_op jit(solution)/shard_map/ppermute | solution.py:477
  22.5 17.0 %copy-start.1 = (bf16[512,512]{1,0:T(8,128)(2,1)S(1)}, bf16[512,512]{1,0:T(8,128)(2,1)}, u32[]{:S(2)}) copy-start(bf16[512,512]{1,0:T(8,128)(2,1)} %w1.1) | copy-start | bytes 1572868
  22.5 17.0 %copy-start.2 = (bf16[512,512]{1,0:T(8,128)(2,1)S(1)}, bf16[512,512]{1,0:T(8,128)(2,1)}, u32[]{:S(2)}) copy-start(bf16[512,512]{1,0:T(8,128)(2,1)} %w2.1) | copy-start | bytes 1572868
  33.8 0.8 copy-start.3
  34.6 56.1 %copy-start.8 = (bf16[512]{0:T(512)(128)(2,1)S(1)}, bf16[512]{0:T(512)(128)(2,1)}, u32[]{:S(2)}) copy-start(bf16[512]{0:T(512)(128)(2,1)} %param.32) | copy-start | bytes 3076
  34.6 6.1 %collective-permute-start.6 = (bf16[2,128,128]{2,1,0:T(8,128)(2,1)S(1)}, bf16[2,128,128]{2,1,0:T(8,128)(2,1)S(1)}, u32[]{:S(2)}, u32[]{:S(2)}) collective-permute-start(bf16[2,128,128]{2,1,0:T(8,128)(2,1)S(1)} %get-tuple-element.54), channel_id=1, source_target_pairs={{0,8},{8,16},{16,24},{24,0},{1,9},{9,17},{17,25},{25,1},{2,10},{10... | collective-permute-start | bytes 196616 | tf_op jit(solution)/shard_map/ppermute | solution.py:477
  35.9 8.2 %collective-permute-start.7 = (bf16[2,128,128]{2,1,0:T(8,128)(2,1)S(1)}, bf16[2,128,128]{2,1,0:T(8,128)(2,1)S(1)}, u32[]{:S(2)}, u32[]{:S(2)}) collective-permute-start(bf16[2,128,128]{2,1,0:T(8,128)(2,1)S(1)} %get-tuple-element.55), channel_id=1, source_target_pairs={{0,16},{8,24},{16,0},{24,8},{1,17},{9,25},{17,1},{25,9},{2,18},{10... | collective-permute-start | bytes 196616 | tf_op jit(solution)/shard_map/ppermute | solution.py:477
  38.3 6.0 %collective-permute-start.8 = (bf16[2,128,128]{2,1,0:T(8,128)(2,1)S(1)}, bf16[2,128,128]{2,1,0:T(8,128)(2,1)S(1)}, u32[]{:S(2)}, u32[]{:S(2)}) collective-permute-start(bf16[2,128,128]{2,1,0:T(8,128)(2,1)S(1)} %get-tuple-element.56), channel_id=1, source_target_pairs={{0,24},{8,0},{16,8},{24,16},{1,25},{9,1},{17,9},{25,17},{2,26},{10... | collective-permute-start | bytes 196616 | tf_op jit(solution)/shard_map/ppermute | solution.py:477
  40.7 7.5 %collective-permute-start.16 = (bf16[128,1024]{1,0:T(8,128)(2,1)S(1)}, bf16[128,1024]{1,0:T(8,128)(2,1)S(1)}, u32[]{:S(2)}, u32[]{:S(2)}) collective-permute-start(bf16[128,1024]{1,0:T(8,128)(2,1)S(1)} %get-tuple-element.66), channel_id=1, source_target_pairs={{0,6},{2,0},{4,2},{6,4},{1,7},{3,1},{5,3},{7,5},{8,14},{10,8},{12,... | collective-permute-start | bytes 786440 | tf_op jit(solution)/shard_map/ppermute | solution.py:477
  44.0 10.2 %collective-permute-start.17 = (bf16[128,1024]{1,0:T(8,128)(2,1)S(1)}, bf16[128,1024]{1,0:T(8,128)(2,1)S(1)}, u32[]{:S(2)}, u32[]{:S(2)}) collective-permute-start(bf16[128,1024]{1,0:T(8,128)(2,1)S(1)} %get-tuple-element.67), channel_id=1, source_target_pairs={{0,4},{2,6},{4,0},{6,2},{1,5},{3,7},{5,1},{7,3},{8,12},{10,14},{12... | collective-permute-start | bytes 786440 | tf_op jit(solution)/shard_map/ppermute | solution.py:477
  44.3 10.3 %collective-permute-start.18 = (bf16[128,1024]{1,0:T(8,128)(2,1)S(1)}, bf16[128,1024]{1,0:T(8,128)(2,1)S(1)}, u32[]{:S(2)}, u32[]{:S(2)}) collective-permute-start(bf16[128,1024]{1,0:T(8,128)(2,1)S(1)} %get-tuple-element.68), channel_id=1, source_target_pairs={{0,2},{2,4},{4,6},{6,0},{1,3},{3,5},{5,7},{7,1},{8,10},{10,12},{12... | collective-permute-start | bytes 786440 | tf_op jit(solution)/shard_map/ppermute | solution.py:477
  46.6 0.7 copy-start.6
  48.2 9.8 %collective-permute-start.9 = (bf16[2,128,128]{2,1,0:T(8,128)(2,1)S(1)}, bf16[2,128,128]{2,1,0:T(8,128)(2,1)}, u32[]{:S(2)}, u32[]{:S(2)}) collective-permute-start(bf16[2,128,128]{2,1,0:T(8,128)(2,1)S(1)} %get-tuple-element.57.a0), channel_id=1, source_target_pairs={{0,32},{32,64},{64,96},{96,0},{128,160},{160,192},{192,224},{224,1... | collective-permute-start | bytes 196616 | tf_op jit(solution)/shard_map/ppermute | solution.py:594
  54.2 31.6 %collective-permute-start.20 = (bf16[512,512]{1,0:T(8,128)(2,1)}, bf16[512,512]{1,0:T(8,128)(2,1)}, u32[]{:S(2)}, u32[]{:S(2)}) collective-permute-start(bf16[512,512]{1,0:T(8,128)(2,1)} %wp0.1), channel_id=1, source_target_pairs={{0,2},{2,4},{4,6},{6,0},{1,3},{3,5},{5,7},{7,1},{8,10},{10,12},{12... | collective-permute-start | bytes 1572872 | tf_op jit(solution)/shard_map/ppermute | solution.py:477
  54.6 34.7 %collective-permute-start.24 = (bf16[512,512]{1,0:T(8,128)(2,1)S(1)}, bf16[512,512]{1,0:T(8,128)(2,1)}, u32[]{:S(2)}, u32[]{:S(2)}) collective-permute-start(bf16[512,512]{1,0:T(8,128)(2,1)S(1)} %copy-done), channel_id=1, source_target_pairs={{0,6},{2,0},{4,2},{6,4},{1,7},{3,1},{5,3},{7,5},{8,14},{10,8},{12,... | collective-permute-start | bytes 1572872 | tf_op jit(solution)/shard_map/ppermute | solution.py:477
  58.0 4.4 %collective-permute-start.10 = (bf16[2,128,128]{2,1,0:T(8,128)(2,1)S(1)}, bf16[2,128,128]{2,1,0:T(8,128)(2,1)S(1)}, u32[]{:S(2)}, u32[]{:S(2)}) collective-permute-start(bf16[2,128,128]{2,1,0:T(8,128)(2,1)S(1)} %get-tuple-element.57.a0), channel_id=1, source_target_pairs={{0,64},{32,96},{64,0},{96,32},{128,192},{160,224},{192,128},{224,1... | collective-permute-start | bytes 196616 | tf_op jit(solution)/shard_map/ppermute | solution.py:594
  58.1 36.8 %collective-permute-start.21 = (bf16[512,512]{1,0:T(8,128)(2,1)}, bf16[512,512]{1,0:T(8,128)(2,1)S(1)}, u32[]{:S(2)}, u32[]{:S(2)}) collective-permute-start(bf16[512,512]{1,0:T(8,128)(2,1)} %collective-permute-done.19.wa1), channel_id=1, source_target_pairs={{0,2},{2,4},{4,6},{6,0},{1,3},{3,5},{5,7},{7,1},{8,10},{10,12},{12... | collective-permute-start | bytes 1572872 | tf_op jit(solution)/shard_map/ppermute | solution.py:477
  58.2 36.7 %collective-permute-start.23 = (bf16[512,512]{1,0:T(8,128)(2,1)}, bf16[512,512]{1,0:T(8,128)(2,1)S(1)}, u32[]{:S(2)}, u32[]{:S(2)}) collective-permute-start(bf16[512,512]{1,0:T(8,128)(2,1)} %collective-permute-done.22.wp3), channel_id=1, source_target_pairs={{0,6},{2,0},{4,2},{6,4},{1,7},{3,1},{5,3},{7,5},{8,14},{10,8},{12,... | collective-permute-start | bytes 1572872 | tf_op jit(solution)/shard_map/ppermute | solution.py:477
  59.8 34.3 %copy-start.5 = (bf16[2,256,256]{2,1,0:T(8,128)(2,1)S(1)}, bf16[2,256,256]{2,1,0:T(8,128)(2,1)}, u32[]{:S(2)}) copy-start(bf16[2,256,256]{2,1,0:T(8,128)(2,1)} %mix.1) | copy-start | bytes 786436
  62.4 4.9 %collective-permute-start.11 = (bf16[2,128,128]{2,1,0:T(8,128)(2,1)S(1)}, bf16[2,128,128]{2,1,0:T(8,128)(2,1)S(1)}, u32[]{:S(2)}, u32[]{:S(2)}) collective-permute-start(bf16[2,128,128]{2,1,0:T(8,128)(2,1)S(1)} %get-tuple-element.57.a0), channel_id=1, source_target_pairs={{0,96},{32,0},{64,32},{96,64},{128,224},{160,128},{192,160},{224,1... | collective-permute-start | bytes 196616 | tf_op jit(solution)/shard_map/ppermute | solution.py:594
  67.3 4.8 %collective-permute-start.25 = (bf16[8,512]{1,0:T(8,128)(2,1)S(1)}, bf16[8,512]{1,0:T(8,128)(2,1)S(1)}, u32[]{:S(2)}, u32[]{:S(2)}) collective-permute-start(bf16[8,512]{1,0:T(8,128)(2,1)S(1)} %get-tuple-element.76), channel_id=1, source_target_pairs={{8,0},{16,8},{24,16},{32,24},{40,32},{48,40},{56,48},{64,56},{72,6... | collective-permute-start | bytes 24584 | tf_op jit(solution)/shard_map/ppermute | solution.py:577
  72.1 6.7 %collective-permute-start.12 = (bf16[128,128]{1,0:T(8,128)(2,1)S(1)}, bf16[128,128]{1,0:T(8,128)(2,1)S(1)}, u32[]{:S(2)}, u32[]{:S(2)}) collective-permute-start(bf16[128,128]{1,0:T(8,128)(2,1)S(1)} %get-tuple-element.58), channel_id=1, source_target_pairs={{0,128},{32,160},{64,192},{96,224},{128,0},{160,32},{192,64},{224,... | collective-permute-start | bytes 98312 | tf_op jit(solution)/shard_map/ppermute | solution.py:600
  78.8 6.5 %collective-permute-start.26 = (bf16[8,512]{1,0:T(8,128)(2,1)S(1)}, bf16[8,512]{1,0:T(8,128)(2,1)S(1)}, u32[]{:S(2)}, u32[]{:S(2)}) collective-permute-start(bf16[8,512]{1,0:T(8,128)(2,1)S(1)} %get-tuple-element.75), channel_id=1, source_target_pairs={{0,8},{8,16},{16,24},{24,32},{32,40},{40,48},{48,56},{56,64},{64,7... | collective-permute-start | bytes 24584 | tf_op jit(solution)/shard_map/ppermute | solution.py:576
  82.3 0.9 copy-start.7
  85.3 9.7 %collective-permute-start.13 = (bf16[128,128]{1,0:T(8,128)(2,1)S(1)}, bf16[128,128]{1,0:T(8,128)(2,1)S(1)}, u32[]{:S(2)}, u32[]{:S(2)}) collective-permute-start(bf16[128,128]{1,0:T(8,128)(2,1)S(1)} %get-tuple-element.62), channel_id=1, source_target_pairs={{0,8},{8,16},{16,24},{24,0},{1,9},{9,17},{17,25},{25,1},{2,10},{10... | collective-permute-start | bytes 98312 | tf_op jit(solution)/shard_map/ppermute | solution.py:477
  85.8 9.1 %collective-permute-start.14 = (bf16[128,128]{1,0:T(8,128)(2,1)S(1)}, bf16[128,128]{1,0:T(8,128)(2,1)S(1)}, u32[]{:S(2)}, u32[]{:S(2)}) collective-permute-start(bf16[128,128]{1,0:T(8,128)(2,1)S(1)} %get-tuple-element.63), channel_id=1, source_target_pairs={{0,16},{8,24},{16,0},{24,8},{1,17},{9,25},{17,1},{25,9},{2,18},{10... | collective-permute-start | bytes 98312 | tf_op jit(solution)/shard_map/ppermute | solution.py:477
  89.4 5.6 %collective-permute-start.15 = (bf16[128,128]{1,0:T(8,128)(2,1)S(1)}, bf16[128,128]{1,0:T(8,128)(2,1)S(1)}, u32[]{:S(2)}, u32[]{:S(2)}) collective-permute-start(bf16[128,128]{1,0:T(8,128)(2,1)S(1)} %get-tuple-element.64), channel_id=1, source_target_pairs={{0,24},{8,0},{16,8},{24,16},{1,25},{9,1},{17,9},{25,17},{2,26},{10... | collective-permute-start | bytes 98312 | tf_op jit(solution)/shard_map/ppermute | solution.py:477
  90.7 1.0 copy-start.4
  99.5 9.4 %collective-permute-start.27 = (bf16[64,2048]{1,0:T(8,128)(2,1)S(1)}, bf16[64,2048]{1,0:T(8,128)(2,1)S(1)}, u32[]{:S(2)}, u32[]{:S(2)}) collective-permute-start(bf16[64,2048]{1,0:T(8,128)(2,1)S(1)} %get-tuple-element.74), channel_id=1, source_target_pairs={{0,1},{1,0},{2,3},{3,2},{4,5},{5,4},{6,7},{7,6},{8,9},{9,8},{10,11... | collective-permute-start | bytes 786440 | tf_op jit(solution)/shard_map/ppermute | solution.py:615

commit v3 on v2

--- a/solution.py
+++ b/solution.py
@@ -31,13 +31,15 @@
     return pltpu.with_memory_space_constraint(array, pltpu.HBM)
 
 
-def call(body, outs, scratch=(), far=0, same=None):
+def call(body, outs, scratch=(), far=0, keep=0):
     def run(scal, *arrays):
         count = len(arrays) - far + len(outs)
 
         def fetched(at, *refs):
             source, near, held = refs[:far], refs[far : far + count], refs[far + count :]
-            buffers, sems, rest = held[:far], held[far], held[far + 1 :]
+            kept = near[count - keep :]
+            buffers, sems, rest = held[: far - keep], held[far - keep], held[far - keep + 1 :]
+            buffers = (*kept, *buffers)
             copies = [
                 pltpu.make_async_copy(a, b, sems.at[k])
                 for k, (a, b) in enumerate(zip(source, buffers))
@@ -46,11 +48,11 @@
                 copy.start()
             for copy in copies:
                 copy.wait()
-            body(at, *buffers, *near, *rest)
+            body(at, *buffers, *near[: count - keep], *rest)
 
         extra = []
         if far:
-            extra = [pltpu.VMEM(a.shape, a.dtype) for a in arrays[:far]]
+            extra = [pltpu.VMEM(a.shape, a.dtype) for a in arrays[keep:far]]
             extra.append(pltpu.SemaphoreType.DMA((far,)))
         return pl.pallas_call(
             fetched if far else body,
@@ -60,7 +62,6 @@
             + [pl.BlockSpec(memory_space=pltpu.VMEM)] * (len(arrays) - far),
             out_specs=[pl.BlockSpec(memory_space=pltpu.VMEM)] * len(outs),
             scratch_shapes=extra + list(scratch),
-            input_output_aliases=same or {},
             compiler_params=pltpu.CompilerParams(vmem_limit_bytes=20 << 20),
             cost_estimate=pl.CostEstimate(flops=1, transcendentals=0, bytes_accessed=1),
         )(scal, *[in_hbm(a) for a in arrays[:far]], *arrays[far:])
@@ -70,29 +71,6 @@
 
 def seat(scal, axis):
     return scal[("sp_1", "sp_0", "fs", "tp").index(axis)]
-
-
-def stage_body(scal, *refs):
-    count = len(refs) // 2
-    sems = refs[-1]
-    copies = [pltpu.make_async_copy(refs[k], refs[count + k], sems.at[k]) for k in range(count)]
-    for copy in copies:
-        copy.start()
-    for copy in copies:
-        copy.wait()
-
-
-def stage(scal, *arrays):
-    return pl.pallas_call(
-        stage_body,
-        out_shape=[jax.ShapeDtypeStruct(a.shape, a.dtype) for a in arrays],
-        in_specs=[pl.BlockSpec(memory_space=pltpu.SMEM)]
-        + [pl.BlockSpec(memory_space=pltpu.HBM)] * len(arrays),
-        out_specs=[pl.BlockSpec(memory_space=pltpu.VMEM)] * len(arrays),
-        scratch_shapes=[pltpu.SemaphoreType.DMA((len(arrays),))],
-        compiler_params=pltpu.CompilerParams(vmem_limit_bytes=4 << 20),
-        name="stage",
-    )(scal, *[in_hbm(a) for a in arrays])
 
 
 def cut_body(scal, tokens, *refs):
@@ -182,7 +160,7 @@
 
 def decay_body(
     scal,
-    tokens, gain, dlow, rlow, draise, dbias, rraise, rbias, tempo_in, sudden_in, wk, wv, mine,
+    wk, wv, gain, tokens, dlow, rlow, draise, rraise, tempo_in, sudden_in, dbias, rbias, mine,
     inv_out, reach_out, out,
 ):
     rows = gather_rows(scal, gain, (mine,))
@@ -197,7 +175,7 @@
     wide = tokens[...].astype(f32)
     inv = lax.rsqrt(jnp.mean(wide * wide, axis=-1, keepdims=True) + norm_eps)
     inv_out[...] = inv
-    normed = (wide * inv * gain[...].astype(f32)).astype(bf16)
+    normed = (wide * inv * gain[:, :2048].astype(f32)).astype(bf16)
     act = jnp.tanh(dot(normed, dlow[...]).astype(bf16).astype(f32)).astype(bf16)
     lat = dot(normed, rlow[...]).astype(bf16)
     for way in range(2):
@@ -300,7 +278,7 @@
         out[...] = maps[(here + s) & 3]
 
 
-def read_body(scal, own, r1, r2, r3, inv, right, reach_in, xy_in, qeff, local):
+def read_body(scal, own, r1, r2, r3, inv, right, reach_in, xy_in, qeff, local, pool, first, last):
     row, lane = iota2((TOK, TOK))
     wide_low = (lax.broadcasted_iota(jnp.int32, (TOK, 256), 1) % 128) < 64
     scale = inv[...]
@@ -332,6 +310,11 @@
                 query * jnp.exp(reach) - pull[:, 128:]
             ).astype(bf16)
         local[:, c] = base
+        v = slice(512 + pair * 128, 512 + (pair + 1) * 128)
+        value = summed(own[:, v], (r1, r2, r3), v, scale)
+        pool[:, c] = value.astype(bf16)
+        first[:, c] = value[:REACH].astype(bf16)
+        last[:, c] = value[TOK - REACH :].astype(bf16)
 
 
 def spread(packed, row, lane):
@@ -410,7 +393,7 @@
 
 
 def final_body(
-    scal, hgain, wa0, wp0, z0, z1, z2, z3, qeff, local, wa1, wp1, wa2, wp2, wa3, wp3, pool,
+    scal, gain, wa0, wp0, z0, z1, z2, z3, qeff, local, wa1, wp1, wa2, wp2, wa3, wp3, pool,
     keep, give, states, total,
 ):
     here, seq, core = seat(scal, "sp_1"), seat(scal, "fs"), seat(scal, "tp")
@@ -422,6 +405,7 @@
     cols = []
     for pair in range(PAIRS):
         c = slice(pair * 128, (pair + 1) * 128)
+        at = slice(2048 + pair * 128, 2048 + (pair + 1) * 128)
         packed = states[(here - pair) & 3].astype(f32)
         moved = roll64(packed)
         ahead = jnp.where(top, jnp.where(low, packed, 0.0), jnp.where(low, 0.0, moved))
@@ -431,7 +415,7 @@
         centred = read - head_sum(read) * (1.0 / 64.0)
         var = head_sum(centred * centred) * (1.0 / 64.0)
         cols.append(
-            (centred * lax.rsqrt(var + head_eps) * hgain[:, c].astype(f32)).astype(bf16)
+            (centred * lax.rsqrt(var + head_eps) * gain[:, at].astype(f32)).astype(bf16)
         )
     attn = jnp.concatenate(cols, axis=1)
     pooled = pool[...]
@@ -499,19 +483,20 @@
 ):
     scal = jnp.stack([lax.axis_index(a) for a in ("sp_1", "sp_0", "fs", "tp")]).astype(jnp.int32)
     return step(
-        scal, inputs[0], input_norm_gain.reshape(1, 2048),
+        scal, inputs[0],
+        jnp.concatenate([input_norm_gain, head_norm_gain]).reshape(1, 2560),
         receptance_matrix, key_matrix, value_matrix, pooling_input_weight,
         decay_lower_matrix, decay_raise_matrix.reshape(128, 512), decay_offset_bias,
         removal_lower_matrix, removal_raise_matrix.reshape(128, 512), removal_rate_bias,
         tempo_scale[0].reshape(16, TOK), sudden_decay_extra[0].reshape(16, TOK),
-        head_norm_gain.reshape(1, 512), group_mixing_weight,
+        group_mixing_weight,
         attention_output_matrix, pooling_output_matrix,
     )
 
 
 def step(
     scal, tokens, gain, wq, wk, wv, wp, dlow, draise, dbias, rlow, rraise, rbias,
-    tempo, sudden, hgain, mix, attn_own, pool_own,
+    tempo, sudden, mix, attn_own, pool_own,
 ):
     rows = pl.pallas_call(
         cut_body,
@@ -526,7 +511,17 @@
     for s in (2, 1, 3):
         rows[s] = shift_by(rows[s], "fs", s, N_FS)
     square = (TOK, TOK)
-    wk_near, wv_near, gain_near = stage(scal, wk, wv, gain)
+    inv, reach, factors, wk_near, wv_near, gain_near = call(
+        decay_body,
+        [
+            ((TOK, 1), f32), ((2, TOK, 512), f32), ((8, 8, *square), bf16),
+            (wk.shape, bf16), (wv.shape, bf16), (gain.shape, bf16),
+        ],
+        far=12,
+        keep=3,
+    )(
+        scal, wk, wv, gain, tokens, dlow, rlow, draise, rraise, tempo, sudden, dbias, rbias, rows[0]
+    )
 
     def give_back(got):
         back = [None] * 3
@@ -546,17 +541,13 @@
 
     attn_w = [attn_own] + [None] * 3
     pool_w = [pool_own] + [None] * 3
-    for s in (1, 3):
-        attn_w[s] = shift_by(attn_own, "fs", s, N_FS)
-        pool_w[s] = shift_by(pool_own, "fs", s, N_FS)
+    attn_w[1] = shift_by(attn_own, "fs", 1, N_FS)
+    pool_w[3] = shift_by(pool_own, "fs", 3, N_FS)
+    attn_w[3] = shift_by(attn_own, "fs", 3, N_FS)
+    pool_w[1] = shift_by(pool_own, "fs", 1, N_FS)
     attn_w[2] = shift_by(attn_w[1], "fs", 1, N_FS)
     pool_w[2] = shift_by(pool_w[3], "fs", 3, N_FS)
 
-    inv, reach, factors = call(
-        decay_body, [((TOK, 1), f32), ((2, TOK, 512), f32), ((8, 8, *square), bf16)], far=12
-    )(
-        scal, tokens, gain, dlow, rlow, draise, dbias, rraise, rbias, tempo, sudden, wk, wv, rows[0]
-    )
     outs = call(
         maps_body,
         [((2, *square), bf16)] * 4 + [((8, N_BLK, *square), bf16), ((8, TOK, 256), bf16)],
@@ -568,21 +559,19 @@
     got = [maps[0]]
     got += [shift_by(maps[s], "sp_1", s, N_X) for s in (1, 2, 3)]
 
-    pool_sum = qp[0][:, 512:]
-    for s in (1, 2, 3):
-        pool_sum = pool_sum + qp[s][:, 512:].astype(f32)
-    pool_in = (pool_sum * inv).astype(bf16)
+    qeff, local, pool_in, first, last = call(
+        read_body,
+        [
+            ((PAIRS, TOK, 256), bf16), ((TOK, 512), f32),
+            ((TOK, 512), bf16), ((REACH, 512), bf16), ((REACH, 512), bf16),
+        ],
+    )(scal, *qp, inv, right, reach, xy)
     n_sp = N_X * N_Z
-    below = lax.ppermute(pool_in[TOK - REACH :], SP, [(i, i + 1) for i in range(n_sp - 1)])
-    above = lax.ppermute(pool_in[:REACH], SP, [(i + 1, i) for i in range(n_sp - 1)])
-
+    below = lax.ppermute(last, SP, [(i, i + 1) for i in range(n_sp - 1)])
+    above = lax.ppermute(first, SP, [(i + 1, i) for i in range(n_sp - 1)])
     (pooled,) = call(pool_body, [((TOK, 512), bf16)])(
         scal, mix, pool_in, above, below
     )
-    qeff, local = call(
-        read_body, [((PAIRS, TOK, 256), bf16), ((TOK, 512), f32)]
-    )(scal, *qp, inv, right, reach, xy)
-
     total, before = call(
         chain_body,
         [((2, *square), bf16), ((3, 2, *square), bf16)],
@@ -609,7 +598,7 @@
         [((64, 2048), f32), ((64, 2048), bf16)],
         scratch=[pltpu.VMEM((N_X, *square), bf16), pltpu.VMEM((TOK, 2048), f32)],
     )(
-        scal, hgain, attn_own, pool_own, *enter, qeff, local,
+        scal, gain_near, attn_own, pool_own, *enter, qeff, local,
         attn_w[1], pool_w[1], attn_w[2], pool_w[2], attn_w[3], pool_w[3], pooled,
     )
     taken = lax.ppermute(give, "tp", [(0, 1), (1, 0)])

time: 110 us -> 129 us (1.17)
  the two profiles are of different devices: /device:TPU:105 before, /device:TPU:7 now
where the time goes in v3:
time: 129 us; the launch traced here: 127 us
  waiting for transfers between devices  50.1 us (39%)
  starting transfers between devices  49.3 us (38%)
  Pallas kernels  25.3 us (20%)
  other arithmetic  1.55 us (1%)
    ppermute x21, waiting for transfers between devices, shift_by(): return lax.ppermute(a, axis, [(i, (i + s) % n) for i in range(n)])  36.1 us
    pallas_call x10, Pallas kernels, run(): pl.pallas_call(fetched if far else body, out_shape=[jax.ShapeDtypeStruct(...  23.6 us
    ppermute x21, starting transfers between devices, shift_by(): return lax.ppermute(a, axis, [(i, (i + s) % n) for i in range(n)])  22.2 us
    ppermute x1, starting transfers between devices, step(): taken = lax.ppermute(give, 'tp', [(0, 1), (1, 0)])  12.3 us
    ppermute x3, waiting for transfers between devices, step(): near.append(lax.ppermute(total, 'sp_0', pairs))  8.36 us
    ppermute x1, starting transfers between devices, step(): taken = lax.ppermute(half, 'sp_0', [(i, i ^ 4) for i in range(N_Z)])  4.93 us
    ppermute x3, starting transfers between devices, step(): near.append(lax.ppermute(total, 'sp_0', pairs))  3.95 us
    ppermute x1, starting transfers between devices, step(): above = lax.ppermute(first, SP, [(i + 1, i) for i in range(n_sp - 1)])  3.25 us
  transfers between devices with their start and end apart: 28, of which 14 were waited for; matrix products, arithmetic and copies ran while one was open for 1% of the time, Pallas kernels for 15%

profile of v3, /device:TPU:7, one launch (start us, length us, event | category | flops | bytes accessed | tf_op | source)
XLA Modules:
  0.0 127.0 jit_solution(17744214176087296824)
XLA Ops:
  0.1 1.7 %cut.1 = (bf16[128,512]{1,0:T(8,128)(2,1)S(1)}, bf16[128,512]{1,0:T(8,128)(2,1)S(1)}, bf16[128,512]{1,0:T(8,128)(2,1)S(1)}, bf16[128,512]{1,0:T(8,128)(2,1)S(1)}) custom-call(s32[4]{0:T(128)S(1)} %pad_add_fusion.scal.at, bf16[128,2048]{1,0:T(8,128)(2,1)} %bitcast.11), custom_call_target="tpu_custom_call" | custom-call | tf_op jit(solution)/shard_map/cut/pallas_call | solution.py:501
  1.8 1.4 %collective-permute-start = (bf16[128,512]{1,0:T(8,128)(2,1)S(1)}, bf16[128,512]{1,0:T(8,128)(2,1)S(1)}, u32[]{:S(2)}, u32[]{:S(2)}) collective-permute-start(bf16[128,512]{1,0:T(8,128)(2,1)S(1)} %get-tuple-element.47), channel_id=1, source_target_pairs={{0,2},{2,4},{4,6},{6,0},{1,3},{3,5},{5,7},{7,1},{8,10},{10,12},{12... | collective-permute-start | bytes 393224 | tf_op jit(solution)/shard_map/ppermute | solution.py:461
  3.1 2.6 %collective-permute-start.1 = (bf16[128,512]{1,0:T(8,128)(2,1)S(1)}, bf16[128,512]{1,0:T(8,128)(2,1)S(1)}, u32[]{:S(2)}, u32[]{:S(2)}) collective-permute-start(bf16[128,512]{1,0:T(8,128)(2,1)S(1)} %get-tuple-element.48), channel_id=1, source_target_pairs={{0,4},{2,6},{4,0},{6,2},{1,5},{3,7},{5,1},{7,3},{8,12},{10,14},{12... | collective-permute-start | bytes 393224 | tf_op jit(solution)/shard_map/ppermute | solution.py:461
  5.8 1.1 collective-permute-start.2
  6.8 0.7 pad_maximum_fusion
  7.5 0.6 reshape.9.refs_2_
  8.2 4.6 %shard_map.172 = (f32[128,1]{1,0:T(8,128)S(1)}, f32[2,128,512]{2,1,0:T(8,128)S(1)}, bf16[8,8,128,128]{3,2,1,0:T(8,128)(2,1)S(1)}, bf16[512,512]{1,0:T(8,128)(2,1...) custom-call(s32[4]{0:T(128)S(1)} %pad_add_fusion.scal.at, bf16[512,512]{1,0:T(8,128)(2,1)} %refs_0_.1, ...), custom_call_target="tpu_custom_call" | custom-call | flops 1 | bytes 1 | tf_op jit(solution)/shard_map/pallas_call | solution.py:57
  12.8 1.3 shard_map.173
  14.1 1.0 collective-permute-start.3
  15.0 1.3 %collective-permute-start.4 = (bf16[128,1024]{1,0:T(8,128)(2,1)S(1)}, bf16[128,1024]{1,0:T(8,128)(2,1)S(1)}, u32[]{:S(2)}, u32[]{:S(2)}) collective-permute-start(bf16[128,1024]{1,0:T(8,128)(2,1)S(1)} %get-tuple-element.51), channel_id=1, source_target_pairs={{0,4},{2,6},{4,0},{6,2},{1,5},{3,7},{5,1},{7,3},{8,12},{10,14},{12... | collective-permute-start | bytes 786440 | tf_op jit(solution)/shard_map/ppermute | solution.py:461
  16.4 2.7 %collective-permute-start.22 = (bf16[512,512]{1,0:T(8,128)(2,1)S(1)}, bf16[512,512]{1,0:T(8,128)(2,1)S(1)}, u32[]{:S(2)}, u32[]{:S(2)}) collective-permute-start(bf16[512,512]{1,0:T(8,128)(2,1)S(1)} %copy-done.3), channel_id=1, source_target_pairs={{0,6},{2,0},{4,2},{6,4},{1,7},{3,1},{5,3},{7,5},{8,14},{10,8},{12,... | collective-permute-start | bytes 1572872 | tf_op jit(solution)/shard_map/ppermute | solution.py:461
  19.0 1.3 shard_map.178
  20.5 2.5 %collective-permute-start.16 = (bf16[128,1024]{1,0:T(8,128)(2,1)S(1)}, bf16[128,1024]{1,0:T(8,128)(2,1)S(1)}, u32[]{:S(2)}, u32[]{:S(2)}) collective-permute-start(bf16[128,1024]{1,0:T(8,128)(2,1)S(1)} %get-tuple-element.69), channel_id=1, source_target_pairs={{0,6},{2,0},{4,2},{6,4},{1,7},{3,1},{5,3},{7,5},{8,14},{10,8},{12,... | collective-permute-start | bytes 786440 | tf_op jit(solution)/shard_map/ppermute | solution.py:461
  23.1 0.9 collective-permute-start.17
  24.0 19.4 %collective-permute-done.5.r3 = bf16[128,1024]{1,0:T(8,128)(2,1)S(1)} collective-permute-done((bf16[128,1024]{1,0:T(8,128)(2,1)S(1)}, bf16[128,1024]{1,0:T(8,128)(2,1)S(1)}, u32[]{:S(2)}, u32[]{:S(2)}) %collective-permute-start.5) | collective-permute-done | bytes 262176 | tf_op jit(solution)/shard_map/ppermute | solution.py:461
  43.4 6.5 %shard_map.174 = (bf16[2,128,128]{2,1,0:T(8,128)(2,1)S(1)}, bf16[2,128,128]{2,1,0:T(8,128)(2,1)S(1)}, bf16[2,128,128]{2,1,0:T(8,128)(2,1)S(1)}, bf16[2,128,128]{...) custom-call(s32[4]{0:T(128)S(1)} %pad_add_fusion.scal.at, ...), custom_call_target="tpu_custom_call" | custom-call | flops 1 | bytes 1 | tf_op jit(solution)/shard_map/pallas_call | solution.py:57
  50.0 2.3 %collective-permute-start.7 = (bf16[2,128,128]{2,1,0:T(8,128)(2,1)S(1)}, bf16[2,128,128]{2,1,0:T(8,128)(2,1)S(1)}, u32[]{:S(2)}, u32[]{:S(2)}) collective-permute-start(bf16[2,128,128]{2,1,0:T(8,128)(2,1)S(1)} %get-tuple-element.58), channel_id=1, source_target_pairs={{0,16},{8,24},{16,0},{24,8},{1,17},{9,25},{17,1},{25,9},{2,18},{10... | collective-permute-start | bytes 196616 | tf_op jit(solution)/shard_map/ppermute | solution.py:461
  52.3 0.8 collective-permute-done.6.a1
  53.1 1.6 %collective-permute-done.7.a2 = bf16[2,128,128]{2,1,0:T(8,128)(2,1)S(1)} collective-permute-done((bf16[2,128,128]{2,1,0:T(8,128)(2,1)S(1)}, bf16[2,128,128]{2,1,0:T(8,128)(2,1)S(1)}, u32[]{:S(2)}, u32[]{:S(2)}) %collective-permute-start.7) | collective-permute-done | bytes 65568 | tf_op jit(solution)/shard_map/ppermute | solution.py:461
  54.7 1.1 collective-permute-start.24
  55.8 1.2 collective-permute-done.8.a3
  57.0 0.9 collective-permute-start.21
  57.9 1.8 %collective-permute-start.23 = (bf16[512,512]{1,0:T(8,128)(2,1)S(1)}, bf16[512,512]{1,0:T(8,128)(2,1)S(1)}, u32[]{:S(2)}, u32[]{:S(2)}) collective-permute-start(bf16[512,512]{1,0:T(8,128)(2,1)S(1)} %collective-permute-done.22.wp3), channel_id=1, source_target_pairs={{0,6},{2,0},{4,2},{6,4},{1,7},{3,1},{5,3},{7,5},{8,14},{10,8},{12,... | collective-permute-start | bytes 1572872 | tf_op jit(solution)/shard_map/ppermute | solution.py:461
  59.7 1.2 shard_map.175
  60.9 10.4 %collective-permute-done.18.r3 = bf16[128,1024]{1,0:T(8,128)(2,1)S(1)} collective-permute-done((bf16[128,1024]{1,0:T(8,128)(2,1)S(1)}, bf16[128,1024]{1,0:T(8,128)(2,1)S(1)}, u32[]{:S(2)}, u32[]{:S(2)}) %collective-permute-start.18) | collective-permute-done | bytes 262176 | tf_op jit(solution)/shard_map/ppermute | solution.py:461
  71.3 1.6 %collective-permute-start.9 = (bf16[2,128,128]{2,1,0:T(8,128)(2,1)S(1)}, bf16[2,128,128]{2,1,0:T(8,128)(2,1)S(1)}, u32[]{:S(2)}, u32[]{:S(2)}) collective-permute-start(bf16[2,128,128]{2,1,0:T(8,128)(2,1)S(1)} %get-tuple-element.60.a0), channel_id=1, source_target_pairs={{0,32},{32,64},{64,96},{96,0},{128,160},{160,192},{192,224},{224,1... | collective-permute-start | bytes 196616 | tf_op jit(solution)/shard_map/ppermute | solution.py:583
  72.9 4.4 %collective-permute-done.9.a1 = bf16[2,128,128]{2,1,0:T(8,128)(2,1)S(1)} collective-permute-done((bf16[2,128,128]{2,1,0:T(8,128)(2,1)S(1)}, bf16[2,128,128]{2,1,0:T(8,128)(2,1)S(1)}, u32[]{:S(2)}, u32[]{:S(2)}) %collective-permute-start.9) | collective-permute-done | bytes 65568 | tf_op jit(solution)/shard_map/ppermute | solution.py:583
  77.7 4.0 %collective-permute-done.10.a2 = bf16[2,128,128]{2,1,0:T(8,128)(2,1)S(1)} collective-permute-done((bf16[2,128,128]{2,1,0:T(8,128)(2,1)S(1)}, bf16[2,128,128]{2,1,0:T(8,128)(2,1)S(1)}, u32[]{:S(2)}, u32[]{:S(2)}) %collective-permute-start.10) | collective-permute-done | bytes 65568 | tf_op jit(solution)/shard_map/ppermute | solution.py:583
  81.7 1.9 %collective-permute-start.11 = (bf16[2,128,128]{2,1,0:T(8,128)(2,1)S(1)}, bf16[2,128,128]{2,1,0:T(8,128)(2,1)S(1)}, u32[]{:S(2)}, u32[]{:S(2)}) collective-permute-start(bf16[2,128,128]{2,1,0:T(8,128)(2,1)S(1)} %get-tuple-element.60.a0), channel_id=1, source_target_pairs={{0,96},{32,0},{64,32},{96,64},{128,224},{160,128},{192,160},{224,1... | collective-permute-start | bytes 196616 | tf_op jit(solution)/shard_map/ppermute | solution.py:583
  83.6 2.3 %shard_map.179 = (bf16[4,128,256]{2,1,0:T(8,128)(2,1)S(1)}, f32[128,512]{1,0:T(8,128)S(1)}, bf16[128,512]{1,0:T(8,128)(2,1)S(1)}, bf16[8,512]{1,0:T(8,128)(2,1)S(1)}, bf16[8,512]{1,0:T(8,128)(2,1)S(1)}) custom-call(s32[4]{0:T(128)S(1)} %pad_add_fusion.scal.at, f32[128,1024]{1,0:T(8,128)S(1)} %get-tuple-element.68.own, ...), custom_call_target="tpu_custom_call" | custom-call | flops 1 | bytes 1 | tf_op jit(solution)/shard_map/pallas_call | solution.py:57
  85.9 3.2 %collective-permute-start.25 = (bf16[8,512]{1,0:T(8,128)(2,1)S(1)}, bf16[8,512]{1,0:T(8,128)(2,1)S(1)}, u32[]{:S(2)}, u32[]{:S(2)}) collective-permute-start(bf16[8,512]{1,0:T(8,128)(2,1)S(1)} %get-tuple-element.77), channel_id=1, source_target_pairs={{8,0},{16,8},{24,16},{32,24},{40,32},{48,40},{56,48},{64,56},{72,6... | collective-permute-start | bytes 24584 | tf_op jit(solution)/shard_map/ppermute | solution.py:571
  89.2 1.2 shard_map.176
  90.3 2.1 %collective-permute-done.25.head = bf16[8,512]{1,0:T(8,128)(2,1)S(1)} collective-permute-done((bf16[8,512]{1,0:T(8,128)(2,1)S(1)}, bf16[8,512]{1,0:T(8,128)(2,1)S(1)}, u32[]{:S(2)}, u32[]{:S(2)}) %collective-permute-start.25) | collective-permute-done | bytes 8224 | tf_op jit(solution)/shard_map/ppermute | solution.py:571
  92.4 4.9 %collective-permute-start.12 = (bf16[128,128]{1,0:T(8,128)(2,1)S(1)}, bf16[128,128]{1,0:T(8,128)(2,1)S(1)}, u32[]{:S(2)}, u32[]{:S(2)}) collective-permute-start(bf16[128,128]{1,0:T(8,128)(2,1)S(1)} %get-tuple-element.61), channel_id=1, source_target_pairs={{0,128},{32,160},{64,192},{96,224},{128,0},{160,32},{192,64},{224,... | collective-permute-start | bytes 98312 | tf_op jit(solution)/shard_map/ppermute | solution.py:589
  97.3 1.7 %collective-permute-done.12.taken = bf16[128,128]{1,0:T(8,128)(2,1)S(1)} collective-permute-done((bf16[128,128]{1,0:T(8,128)(2,1)S(1)}, bf16[128,128]{1,0:T(8,128)(2,1)S(1)}, u32[]{:S(2)}, u32[]{:S(2)}) %collective-permute-start.12) | collective-permute-done | bytes 32800 | tf_op jit(solution)/shard_map/ppermute | solution.py:589
  99.1 2.7 %collective-permute-start.26 = (bf16[8,512]{1,0:T(8,128)(2,1)S(1)}, bf16[8,512]{1,0:T(8,128)(2,1)S(1)}, u32[]{:S(2)}, u32[]{:S(2)}) collective-permute-start(bf16[8,512]{1,0:T(8,128)(2,1)S(1)} %get-tuple-element.78), channel_id=1, source_target_pairs={{0,8},{8,16},{16,24},{24,32},{32,40},{40,48},{48,56},{56,64},{64,7... | collective-permute-start | bytes 24584 | tf_op jit(solution)/shard_map/ppermute | solution.py:570
  101.8 1.0 shard_map.177
  102.8 0.7 collective-permute-done.26.tail
  103.5 0.6 collective-permute-start.13
  104.0 1.3 %collective-permute-start.14 = (bf16[128,128]{1,0:T(8,128)(2,1)S(1)}, bf16[128,128]{1,0:T(8,128)(2,1)S(1)}, u32[]{:S(2)}, u32[]{:S(2)}) collective-permute-start(bf16[128,128]{1,0:T(8,128)(2,1)S(1)} %get-tuple-element.66), channel_id=1, source_target_pairs={{0,16},{8,24},{16,0},{24,8},{1,17},{9,25},{17,1},{25,9},{2,18},{10... | collective-permute-start | bytes 98312 | tf_op jit(solution)/shard_map/ppermute | solution.py:461
  105.4 0.6 collective-permute-start.15
  106.0 0.9 shard_map.180.pool
  106.9 1.7 %collective-permute-done.14.z2 = bf16[128,128]{1,0:T(8,128)(2,1)S(1)} collective-permute-done((bf16[128,128]{1,0:T(8,128)(2,1)S(1)}, bf16[128,128]{1,0:T(8,128)(2,1)S(1)}, u32[]{:S(2)}, u32[]{:S(2)}) %collective-permute-start.14) | collective-permute-done | bytes 32800 | tf_op jit(solution)/shard_map/ppermute | solution.py:461
  108.6 0.7 collective-permute-done.15.z3
  109.4 3.4 %shard_map.181 = (f32[64,2048]{1,0:T(8,128)S(1)}, bf16[64,2048]{1,0:T(8,128)(2,1)S(1)}) custom-call(s32[4]{0:T(128)S(1)} %pad_add_fusion.scal.at, bf16[1,2560]{1,0:T(2,128)(2,1)S(1)} %get-tuple-element.44.gain, bf16[512,512]{1,0:T(8,128)(2,1)S(1)} %copy-done.2, bf16[512,512]{1,0:T(8,128)(2,1)S(1)} %copy-done.3, bf16[128,128]{1,0:T(8,128)(2,1)S(1)} %get-tuple-element.64.z0, ...), custom_call_target="tpu_custom_call" | custom-call | flops 1 | bytes 1 | tf_op jit(solution)/shard_map/pallas_call | solution.py:57
  112.8 12.3 %collective-permute-start.27 = (bf16[64,2048]{1,0:T(8,128)(2,1)S(1)}, bf16[64,2048]{1,0:T(8,128)(2,1)S(1)}, u32[]{:S(2)}, u32[]{:S(2)}) collective-permute-start(bf16[64,2048]{1,0:T(8,128)(2,1)S(1)} %get-tuple-element.80), channel_id=1, source_target_pairs={{0,1},{1,0},{2,3},{3,2},{4,5},{5,4},{6,7},{7,6},{8,9},{9,8},{10,11... | collective-permute-start | bytes 786440 | tf_op jit(solution)/shard_map/ppermute | solution.py:604
  125.1 1.2 collective-permute-done.27
  126.2 0.8 fusion
  (33 shorter events, 0.9 us)
Async XLA Ops:
  1.8 11.0 %collective-permute-start = (bf16[128,512]{1,0:T(8,128)(2,1)S(1)}, bf16[128,512]{1,0:T(8,128)(2,1)S(1)}, u32[]{:S(2)}, u32[]{:S(2)}) collective-permute-start(bf16[128,512]{1,0:T(8,128)(2,1)S(1)} %get-tuple-element.47), channel_id=1, source_target_pairs={{0,2},{2,4},{4,6},{6,0},{1,3},{3,5},{5,7},{7,1},{8,10},{10,12},{12... | collective-permute-start | bytes 393224 | tf_op jit(solution)/shard_map/ppermute | solution.py:461
  3.1 9.7 %collective-permute-start.1 = (bf16[128,512]{1,0:T(8,128)(2,1)S(1)}, bf16[128,512]{1,0:T(8,128)(2,1)S(1)}, u32[]{:S(2)}, u32[]{:S(2)}) collective-permute-start(bf16[128,512]{1,0:T(8,128)(2,1)S(1)} %get-tuple-element.48), channel_id=1, source_target_pairs={{0,4},{2,6},{4,0},{6,2},{1,5},{3,7},{5,1},{7,3},{8,12},{10,14},{12... | collective-permute-start | bytes 393224 | tf_op jit(solution)/shard_map/ppermute | solution.py:461
  5.8 7.1 %collective-permute-start.2 = (bf16[128,512]{1,0:T(8,128)(2,1)S(1)}, bf16[128,512]{1,0:T(8,128)(2,1)S(1)}, u32[]{:S(2)}, u32[]{:S(2)}) collective-permute-start(bf16[128,512]{1,0:T(8,128)(2,1)S(1)} %get-tuple-element.49), channel_id=1, source_target_pairs={{0,6},{2,0},{4,2},{6,4},{1,7},{3,1},{5,3},{7,5},{8,14},{10,8},{12,... | collective-permute-start | bytes 393224 | tf_op jit(solution)/shard_map/ppermute | solution.py:461
  8.1 8.2 %copy-start.2 = (bf16[512,512]{1,0:T(8,128)(2,1)S(1)}, bf16[512,512]{1,0:T(8,128)(2,1)}, u32[]{:S(2)}) copy-start(bf16[512,512]{1,0:T(8,128)(2,1)} %wa0.1) | copy-start | bytes 1572868
  8.1 8.2 %copy-start.3 = (bf16[512,512]{1,0:T(8,128)(2,1)S(1)}, bf16[512,512]{1,0:T(8,128)(2,1)}, u32[]{:S(2)}) copy-start(bf16[512,512]{1,0:T(8,128)(2,1)} %wp0.1) | copy-start | bytes 1572868
  8.1 10.9 %copy-start = (bf16[512,512]{1,0:T(8,128)(2,1)S(1)}, bf16[512,512]{1,0:T(8,128)(2,1)}, u32[]{:S(2)}) copy-start(bf16[512,512]{1,0:T(8,128)(2,1)} %w1.1) | copy-start | bytes 1572868
  8.1 10.9 %copy-start.1 = (bf16[512,512]{1,0:T(8,128)(2,1)S(1)}, bf16[512,512]{1,0:T(8,128)(2,1)}, u32[]{:S(2)}) copy-start(bf16[512,512]{1,0:T(8,128)(2,1)} %w2.1) | copy-start | bytes 1572868
  14.1 6.4 %collective-permute-start.3 = (bf16[128,1024]{1,0:T(8,128)(2,1)S(1)}, bf16[128,1024]{1,0:T(8,128)(2,1)S(1)}, u32[]{:S(2)}, u32[]{:S(2)}) collective-permute-start(bf16[128,1024]{1,0:T(8,128)(2,1)S(1)} %get-tuple-element.50), channel_id=1, source_target_pairs={{0,6},{2,0},{4,2},{6,4},{1,7},{3,1},{5,3},{7,5},{8,14},{10,8},{12,... | collective-permute-start | bytes 786440 | tf_op jit(solution)/shard_map/ppermute | solution.py:461
  15.0 8.0 %collective-permute-start.4 = (bf16[128,1024]{1,0:T(8,128)(2,1)S(1)}, bf16[128,1024]{1,0:T(8,128)(2,1)S(1)}, u32[]{:S(2)}, u32[]{:S(2)}) collective-permute-start(bf16[128,1024]{1,0:T(8,128)(2,1)S(1)} %get-tuple-element.51), channel_id=1, source_target_pairs={{0,4},{2,6},{4,0},{6,2},{1,5},{3,7},{5,1},{7,3},{8,12},{10,14},{12... | collective-permute-start | bytes 786440 | tf_op jit(solution)/shard_map/ppermute | solution.py:461
  16.4 40.6 %collective-permute-start.19 = (bf16[512,512]{1,0:T(8,128)(2,1)S(1)}, bf16[512,512]{1,0:T(8,128)(2,1)S(1)}, u32[]{:S(2)}, u32[]{:S(2)}) collective-permute-start(bf16[512,512]{1,0:T(8,128)(2,1)S(1)} %copy-done.2), channel_id=1, source_target_pairs={{0,2},{2,4},{4,6},{6,0},{1,3},{3,5},{5,7},{7,1},{8,10},{10,12},{12... | collective-permute-start | bytes 1572872 | tf_op jit(solution)/shard_map/ppermute | solution.py:461
  16.4 41.5 %collective-permute-start.22 = (bf16[512,512]{1,0:T(8,128)(2,1)S(1)}, bf16[512,512]{1,0:T(8,128)(2,1)S(1)}, u32[]{:S(2)}, u32[]{:S(2)}) collective-permute-start(bf16[512,512]{1,0:T(8,128)(2,1)S(1)} %copy-done.3), channel_id=1, source_target_pairs={{0,6},{2,0},{4,2},{6,4},{1,7},{3,1},{5,3},{7,5},{8,14},{10,8},{12,... | collective-permute-start | bytes 1572872 | tf_op jit(solution)/shard_map/ppermute | solution.py:461
  19.0 24.4 %collective-permute-start.5 = (bf16[128,1024]{1,0:T(8,128)(2,1)S(1)}, bf16[128,1024]{1,0:T(8,128)(2,1)S(1)}, u32[]{:S(2)}, u32[]{:S(2)}) collective-permute-start(bf16[128,1024]{1,0:T(8,128)(2,1)S(1)} %get-tuple-element.52), channel_id=1, source_target_pairs={{0,2},{2,4},{4,6},{6,0},{1,3},{3,5},{5,7},{7,1},{8,10},{10,12},{12... | collective-permute-start | bytes 786440 | tf_op jit(solution)/shard_map/ppermute | solution.py:461
  20.5 29.4 %collective-permute-start.16 = (bf16[128,1024]{1,0:T(8,128)(2,1)S(1)}, bf16[128,1024]{1,0:T(8,128)(2,1)S(1)}, u32[]{:S(2)}, u32[]{:S(2)}) collective-permute-start(bf16[128,1024]{1,0:T(8,128)(2,1)S(1)} %get-tuple-element.69), channel_id=1, source_target_pairs={{0,6},{2,0},{4,2},{6,4},{1,7},{3,1},{5,3},{7,5},{8,14},{10,8},{12,... | collective-permute-start | bytes 786440 | tf_op jit(solution)/shard_map/ppermute | solution.py:461
  23.1 29.2 %collective-permute-start.17 = (bf16[128,1024]{1,0:T(8,128)(2,1)S(1)}, bf16[128,1024]{1,0:T(8,128)(2,1)S(1)}, u32[]{:S(2)}, u32[]{:S(2)}) collective-permute-start(bf16[128,1024]{1,0:T(8,128)(2,1)S(1)} %get-tuple-element.70), channel_id=1, source_target_pairs={{0,4},{2,6},{4,0},{6,2},{1,5},{3,7},{5,1},{7,3},{8,12},{10,14},{12... | collective-permute-start | bytes 786440 | tf_op jit(solution)/shard_map/ppermute | solution.py:461
  49.9 3.2 %collective-permute-start.6 = (bf16[2,128,128]{2,1,0:T(8,128)(2,1)S(1)}, bf16[2,128,128]{2,1,0:T(8,128)(2,1)S(1)}, u32[]{:S(2)}, u32[]{:S(2)}) collective-permute-start(bf16[2,128,128]{2,1,0:T(8,128)(2,1)S(1)} %get-tuple-element.57), channel_id=1, source_target_pairs={{0,8},{8,16},{16,24},{24,0},{1,9},{9,17},{17,25},{25,1},{2,10},{10... | collective-permute-start | bytes 196616 | tf_op jit(solution)/shard_map/ppermute | solution.py:461
  50.0 4.7 %collective-permute-start.7 = (bf16[2,128,128]{2,1,0:T(8,128)(2,1)S(1)}, bf16[2,128,128]{2,1,0:T(8,128)(2,1)S(1)}, u32[]{:S(2)}, u32[]{:S(2)}) collective-permute-start(bf16[2,128,128]{2,1,0:T(8,128)(2,1)S(1)} %get-tuple-element.58), channel_id=1, source_target_pairs={{0,16},{8,24},{16,0},{24,8},{1,17},{9,25},{17,1},{25,9},{2,18},{10... | collective-permute-start | bytes 196616 | tf_op jit(solution)/shard_map/ppermute | solution.py:461
  52.3 4.7 %collective-permute-start.8 = (bf16[2,128,128]{2,1,0:T(8,128)(2,1)S(1)}, bf16[2,128,128]{2,1,0:T(8,128)(2,1)S(1)}, u32[]{:S(2)}, u32[]{:S(2)}) collective-permute-start(bf16[2,128,128]{2,1,0:T(8,128)(2,1)S(1)} %get-tuple-element.59), channel_id=1, source_target_pairs={{0,24},{8,0},{16,8},{24,16},{1,25},{9,1},{17,9},{25,17},{2,26},{10... | collective-permute-start | bytes 196616 | tf_op jit(solution)/shard_map/ppermute | solution.py:461
  53.1 51.0 %collective-permute-start.20 = (bf16[512,512]{1,0:T(8,128)(2,1)S(1)}, bf16[512,512]{1,0:T(8,128)(2,1)S(1)}, u32[]{:S(2)}, u32[]{:S(2)}) collective-permute-start(bf16[512,512]{1,0:T(8,128)(2,1)S(1)} %copy-done.3), channel_id=1, source_target_pairs={{0,2},{2,4},{4,6},{6,0},{1,3},{3,5},{5,7},{7,1},{8,10},{10,12},{12... | collective-permute-start | bytes 1572872 | tf_op jit(solution)/shard_map/ppermute | solution.py:461
  54.7 50.7 %collective-permute-start.24 = (bf16[512,512]{1,0:T(8,128)(2,1)S(1)}, bf16[512,512]{1,0:T(8,128)(2,1)S(1)}, u32[]{:S(2)}, u32[]{:S(2)}) collective-permute-start(bf16[512,512]{1,0:T(8,128)(2,1)S(1)} %copy-done.2), channel_id=1, source_target_pairs={{0,6},{2,0},{4,2},{6,4},{1,7},{3,1},{5,3},{7,5},{8,14},{10,8},{12,... | collective-permute-start | bytes 1572872 | tf_op jit(solution)/shard_map/ppermute | solution.py:461
  57.0 14.3 %collective-permute-start.18 = (bf16[128,1024]{1,0:T(8,128)(2,1)S(1)}, bf16[128,1024]{1,0:T(8,128)(2,1)S(1)}, u32[]{:S(2)}, u32[]{:S(2)}) collective-permute-start(bf16[128,1024]{1,0:T(8,128)(2,1)S(1)} %get-tuple-element.71), channel_id=1, source_target_pairs={{0,2},{2,4},{4,6},{6,0},{1,3},{3,5},{5,7},{7,1},{8,10},{10,12},{12... | collective-permute-start | bytes 786440 | tf_op jit(solution)/shard_map/ppermute | solution.py:461
  57.0 52.4 %collective-permute-start.21 = (bf16[512,512]{1,0:T(8,128)(2,1)S(1)}, bf16[512,512]{1,0:T(8,128)(2,1)S(1)}, u32[]{:S(2)}, u32[]{:S(2)}) collective-permute-start(bf16[512,512]{1,0:T(8,128)(2,1)S(1)} %collective-permute-done.19.wa1), channel_id=1, source_target_pairs={{0,2},{2,4},{4,6},{6,0},{1,3},{3,5},{5,7},{7,1},{8,10},{10,12},{12... | collective-permute-start | bytes 1572872 | tf_op jit(solution)/shard_map/ppermute | solution.py:461
  57.9 51.4 %collective-permute-start.23 = (bf16[512,512]{1,0:T(8,128)(2,1)S(1)}, bf16[512,512]{1,0:T(8,128)(2,1)S(1)}, u32[]{:S(2)}, u32[]{:S(2)}) collective-permute-start(bf16[512,512]{1,0:T(8,128)(2,1)S(1)} %collective-permute-done.22.wp3), channel_id=1, source_target_pairs={{0,6},{2,0},{4,2},{6,4},{1,7},{3,1},{5,3},{7,5},{8,14},{10,8},{12,... | collective-permute-start | bytes 1572872 | tf_op jit(solution)/shard_map/ppermute | solution.py:461
  60.9 45.1 %copy-start.4 = (bf16[2,256,256]{2,1,0:T(8,128)(2,1)S(1)}, bf16[2,256,256]{2,1,0:T(8,128)(2,1)}, u32[]{:S(2)}) copy-start(bf16[2,256,256]{2,1,0:T(8,128)(2,1)} %mix.1) | copy-start | bytes 786436
  71.3 6.0 %collective-permute-start.9 = (bf16[2,128,128]{2,1,0:T(8,128)(2,1)S(1)}, bf16[2,128,128]{2,1,0:T(8,128)(2,1)S(1)}, u32[]{:S(2)}, u32[]{:S(2)}) collective-permute-start(bf16[2,128,128]{2,1,0:T(8,128)(2,1)S(1)} %get-tuple-element.60.a0), channel_id=1, source_target_pairs={{0,32},{32,64},{64,96},{96,0},{128,160},{160,192},{192,224},{224,1... | collective-permute-start | bytes 196616 | tf_op jit(solution)/shard_map/ppermute | solution.py:583
  77.3 4.4 %collective-permute-start.10 = (bf16[2,128,128]{2,1,0:T(8,128)(2,1)S(1)}, bf16[2,128,128]{2,1,0:T(8,128)(2,1)S(1)}, u32[]{:S(2)}, u32[]{:S(2)}) collective-permute-start(bf16[2,128,128]{2,1,0:T(8,128)(2,1)S(1)} %get-tuple-element.60.a0), channel_id=1, source_target_pairs={{0,64},{32,96},{64,0},{96,32},{128,192},{160,224},{192,128},{224,1... | collective-permute-start | bytes 196616 | tf_op jit(solution)/shard_map/ppermute | solution.py:583
  81.7 4.2 %collective-permute-start.11 = (bf16[2,128,128]{2,1,0:T(8,128)(2,1)S(1)}, bf16[2,128,128]{2,1,0:T(8,128)(2,1)S(1)}, u32[]{:S(2)}, u32[]{:S(2)}) collective-permute-start(bf16[2,128,128]{2,1,0:T(8,128)(2,1)S(1)} %get-tuple-element.60.a0), channel_id=1, source_target_pairs={{0,96},{32,0},{64,32},{96,64},{128,224},{160,128},{192,160},{224,1... | collective-permute-start | bytes 196616 | tf_op jit(solution)/shard_map/ppermute | solution.py:583
  85.9 6.5 %collective-permute-start.25 = (bf16[8,512]{1,0:T(8,128)(2,1)S(1)}, bf16[8,512]{1,0:T(8,128)(2,1)S(1)}, u32[]{:S(2)}, u32[]{:S(2)}) collective-permute-start(bf16[8,512]{1,0:T(8,128)(2,1)S(1)} %get-tuple-element.77), channel_id=1, source_target_pairs={{8,0},{16,8},{24,16},{32,24},{40,32},{48,40},{56,48},{64,56},{72,6... | collective-permute-start | bytes 24584 | tf_op jit(solution)/shard_map/ppermute | solution.py:571
  92.4 6.7 %collective-permute-start.12 = (bf16[128,128]{1,0:T(8,128)(2,1)S(1)}, bf16[128,128]{1,0:T(8,128)(2,1)S(1)}, u32[]{:S(2)}, u32[]{:S(2)}) collective-permute-start(bf16[128,128]{1,0:T(8,128)(2,1)S(1)} %get-tuple-element.61), channel_id=1, source_target_pairs={{0,128},{32,160},{64,192},{96,224},{128,0},{160,32},{192,64},{224,... | collective-permute-start | bytes 98312 | tf_op jit(solution)/shard_map/ppermute | solution.py:589
  99.1 4.4 %collective-permute-start.26 = (bf16[8,512]{1,0:T(8,128)(2,1)S(1)}, bf16[8,512]{1,0:T(8,128)(2,1)S(1)}, u32[]{:S(2)}, u32[]{:S(2)}) collective-permute-start(bf16[8,512]{1,0:T(8,128)(2,1)S(1)} %get-tuple-element.78), channel_id=1, source_target_pairs={{0,8},{8,16},{16,24},{24,32},{32,40},{40,48},{48,56},{56,64},{64,7... | collective-permute-start | bytes 24584 | tf_op jit(solution)/shard_map/ppermute | solution.py:570
  103.5 3.4 %collective-permute-start.13 = (bf16[128,128]{1,0:T(8,128)(2,1)S(1)}, bf16[128,128]{1,0:T(8,128)(2,1)S(1)}, u32[]{:S(2)}, u32[]{:S(2)}) collective-permute-start(bf16[128,128]{1,0:T(8,128)(2,1)S(1)} %get-tuple-element.65), channel_id=1, source_target_pairs={{0,8},{8,16},{16,24},{24,0},{1,9},{9,17},{17,25},{25,1},{2,10},{10... | collective-permute-start | bytes 98312 | tf_op jit(solution)/shard_map/ppermute | solution.py:461
  104.0 4.6 %collective-permute-start.14 = (bf16[128,128]{1,0:T(8,128)(2,1)S(1)}, bf16[128,128]{1,0:T(8,128)(2,1)S(1)}, u32[]{:S(2)}, u32[]{:S(2)}) collective-permute-start(bf16[128,128]{1,0:T(8,128)(2,1)S(1)} %get-tuple-element.66), channel_id=1, source_target_pairs={{0,16},{8,24},{16,0},{24,8},{1,17},{9,25},{17,1},{25,9},{2,18},{10... | collective-permute-start | bytes 98312 | tf_op jit(solution)/shard_map/ppermute | solution.py:461
  105.4 4.0 %collective-permute-start.15 = (bf16[128,128]{1,0:T(8,128)(2,1)S(1)}, bf16[128,128]{1,0:T(8,128)(2,1)S(1)}, u32[]{:S(2)}, u32[]{:S(2)}) collective-permute-start(bf16[128,128]{1,0:T(8,128)(2,1)S(1)} %get-tuple-element.67), channel_id=1, source_target_pairs={{0,24},{8,0},{16,8},{24,16},{1,25},{9,1},{17,9},{25,17},{2,26},{10... | collective-permute-start | bytes 98312 | tf_op jit(solution)/shard_map/ppermute | solution.py:461
  112.8 13.5 %collective-permute-start.27 = (bf16[64,2048]{1,0:T(8,128)(2,1)S(1)}, bf16[64,2048]{1,0:T(8,128)(2,1)S(1)}, u32[]{:S(2)}, u32[]{:S(2)}) collective-permute-start(bf16[64,2048]{1,0:T(8,128)(2,1)S(1)} %get-tuple-element.80), channel_id=1, source_target_pairs={{0,1},{1,0},{2,3},{3,2},{4,5},{5,4},{6,7},{7,6},{8,9},{9,8},{10,11... | collective-permute-start | bytes 786440 | tf_op jit(solution)/shard_map/ppermute | solution.py:604
